TPU v7x, 512 devices: a whole 4x4x16 slice. The times are simulated.
512 devices in a mesh: gr: 2 (over z_hi), fs: 32 (over z_lo, y), tp: 8 (over x, core).
Axes of the slice: x: 4, y: 4, z: 16 (z_hi: 2, z_lo: 8; z = z_hi * 8 + z_lo), core: 2. Of those that a mesh axis runs over, the one named last changes fastest.
Arguments:
- prompt: bfloat16 [8192, 2048], P(('gr', 'tp'), 'fs'), may hold values from -2.5 to 2.5
- gain_pre: float32 [2048], P(('gr', 'fs')), may hold values from 0.1 to 1.9
- gate_pre: float32 [2048, 5632], P(('gr', 'fs'), 'tp'), may hold values from -6 to 6
- up_pre: float32 [2048, 5632], P(('gr', 'fs'), 'tp'), may hold values from -6 to 6
- down_pre: float32 [2048, 5632], P(('gr', 'fs'), 'tp'), may hold values from -16 to 16
- gain_post: float32 [2048], P(('gr', 'fs')), may hold values from 0.1 to 1.9
- gate_post: float32 [2048, 5632], P(('gr', 'fs'), 'tp'), may hold values from -6 to 6
- up_post: float32 [2048, 5632], P(('gr', 'fs'), 'tp'), may hold values from -6 to 6
- down_post: float32 [2048, 5632], P(('gr', 'fs'), 'tp'), may hold values from -16 to 16
Outputs:
- result: bfloat16 [8192, 2048], P(('gr', 'tp'), 'fs')
- gate_first: bfloat16 [5632, 2048], P('fs')
- up_first: bfloat16 [5632, 2048], P('fs')
- down_first: bfloat16 [5632, 2048], P('fs')
- gate_second: bfloat16 [5632, 2048], P('fs')
- up_second: bfloat16 [5632, 2048], P('fs')
- down_second: bfloat16 [5632, 2048], P('fs')
All inputs are finite; a program needn't handle non-finite values.
Results may differ from a plain program's by a relative error of at most 0.028.
Values may be sent and summed in bfloat16 or wider, within the bound.
No kernel may reach another device: no remote copies, remote signals or barrier semaphores. Data moves between devices by JAX's collectives and lax.ppermute only.
A program may use at most 64 MiB of HBM per device.

v0:
```python
import jax
import jax.numpy as jnp
from jax import lax
from jax.experimental import pallas as pl
from jax.experimental.pallas import tpu as pltpu
from jax.sharding import Mesh
from jax.sharding import PartitionSpec as P

D = 2048
FF = 5632
NORM_EPS = 1e-06
GR, ZQ, B, Y, X, CORE = 2, 4, 2, 4, 4, 2
AXES = ("gr", "zq", "b", "y", "x", "core")
ZL, TP = ZQ * B, X * CORE
F32, BF16 = jnp.float32, jnp.bfloat16
BLOCK = FF // (ZL * Y)
ROWS = D // (GR * ZL * Y)
PART = BLOCK // TP
PADDED = 24
LANES = Y * ROWS
SPANS = GR * ZL
OWN = 2 * PADDED
FEATS = D // (ZL * Y)
AT_ONCE = 4


def swap(blocks, axis):
    return lax.all_to_all(blocks, axis, split_axis=0, concat_axis=0, tiled=True)


def share(block, axis, size):
    return swap(jnp.broadcast_to(block[None], (size, *block.shape)), axis)


def from_peer(block, axis, size, flip):
    return lax.ppermute(block, axis, [(i, i ^ flip) for i in range(size)])


def after(value, *others):
    return lax.optimization_barrier((value, *others))[0]


def by_block(layers):
    cols = jnp.stack([jnp.stack(matrices) for matrices in layers])
    n = cols.shape[0] * 3
    to_y = cols.reshape(n, ROWS, Y, BLOCK).transpose(2, 1, 0, 3).reshape(Y, ROWS, n * BLOCK)
    turned = swap(to_y, "y").reshape(LANES, n * BLOCK).T
    parts = turned.reshape(n, TP, PART, LANES).transpose(1, 0, 2, 3)
    return jnp.pad(parts, ((0, 0), (0, 0), (0, PADDED - PART), (0, 0))).reshape(TP, n * PADDED, LANES)


def by_span(parts):
    to_z = jnp.broadcast_to(parts.reshape(1, ZQ, -1, LANES), (GR, ZQ, B * parts.shape[1], LANES))
    here = swap(to_z.reshape(GR * ZQ, B * parts.shape[1], LANES), ("gr", "zq"))
    here = here.reshape(GR * ZQ, B, -1, 3, PADDED, LANES).transpose(2, 0, 3, 1, 4, 5)
    return here.reshape(-1, GR * ZQ, 3 * OWN, LANES)


def paired(piece):
    near = from_peer(piece, "b", B, 1)
    low = lax.axis_index("b") == 0
    both = jnp.stack([jnp.where(low, piece, near), jnp.where(low, near, piece)], axis=1)
    return both.reshape(SPANS, 3 * OWN, LANES)


def over_x(pair):
    return [from_peer(pair, "x", X, k) for k in range(1, X)]


def widened(pair, pieces):
    mine = jnp.stack([pair, *pieces])
    return mine, from_peer(mine, "core", CORE, 1)


def slot(zl, zq):
    k = (zl // B) ^ zq
    return ((k & 1) << 1) | (k >> 1), zl % B


def half_kernel(at_ref, x_ref, mine_ref, other_ref, out_ref, acc_ref, sq_ref):
    width = x_ref.shape[-1]
    pieces = 2 * X
    zq = at_ref[0]

    def rows(span, lo, hi):
        a = mine_ref[:, span, lo:hi, :].reshape(X * (hi - lo), LANES)
        b = other_ref[:, span, lo:hi, :].reshape(X * (hi - lo), LANES)
        return jnp.concatenate([a, b], axis=0)

    def both(zl, lo, hi):
        return jnp.concatenate([rows(2 * zl, lo, hi), rows(2 * zl + 1, lo, hi)], axis=1)

    acc_ref[...] = jnp.zeros_like(acc_ref)
    sq_ref[...] = jnp.zeros_like(sq_ref)

    def inward(zl, _):
        k, b = slot(zl, zq)
        tokens = x_ref[:, k, b].reshape(Y * FEATS, width)
        wide = tokens.astype(F32)
        sq_ref[...] += jnp.sum((wide * wide).reshape(Y * FEATS // 8, 8, width), axis=0)
        acc_ref[...] += jnp.dot(both(zl, 0, 2 * OWN), tokens, preferred_element_type=F32)
        return 0

    lax.fori_loop(0, ZL, inward, 0)
    squares = jnp.sum(sq_ref[...], axis=0, keepdims=True)
    scale = lax.rsqrt(squares / D + NORM_EPS) * D ** (-0.5)
    sums = acc_ref[...].reshape(pieces, 2 * OWN, width)
    gate = sums[:, :OWN].reshape(pieces * OWN, width) * scale
    up = sums[:, OWN:].reshape(pieces * OWN, width) * scale
    hidden = (gate / (1.0 + jnp.exp(-gate)) * up).astype(BF16)

    def outward(zl, _):
        part = lax.dot_general(
            both(zl, 2 * OWN, 3 * OWN), hidden, (((0,), (0,)), ((), ())), preferred_element_type=F32
        )
        k, b = slot(zl, zq)
        out_ref[:, k, b] = part.astype(BF16).reshape(Y, FEATS, width)
        return 0

    lax.fori_loop(0, ZL, outward, 0)


def half_partial(tokens, mine, other):
    width = tokens.shape[-1]
    vmem = pl.BlockSpec(memory_space=pltpu.VMEM)
    flops = 2 * 3 * 2 * X * OWN * D * width
    return pl.pallas_call(
        half_kernel,
        out_shape=jax.ShapeDtypeStruct(tokens.shape, BF16),
        in_specs=[pl.BlockSpec(memory_space=pltpu.SMEM)] + [vmem] * 3,
        out_specs=vmem,
        scratch_shapes=[pltpu.VMEM((2 * X * 2 * OWN, width), F32), pltpu.VMEM((8, width), F32)],
        cost_estimate=pl.CostEstimate(
            flops=flops, bytes_accessed=2 * (2 * tokens.size + 2 * mine.size), transcendentals=0
        ),
        name="half_step",
    )(place("zq"), tokens, mine, other)


def serve_kernel(at_ref, mine_ref, other_ref, gate_ref, up_ref, down_ref, rows_ref):
    x, core, b = at_ref[0], at_ref[1], at_ref[2]
    for span in range(AT_ONCE):
        for m, out_ref in enumerate((gate_ref, up_ref, down_ref)):
            for xs in range(X):
                k = x ^ xs
                own = pl.ds(pl.multiple_of(m * OWN + b * PADDED, 8), PADDED)
                north = mine_ref[k, span, own, :].astype(F32)
                south = other_ref[k, span, own, :].astype(F32)
                for c in range(CORE):
                    at = (xs * CORE + c) * PART
                    rows_ref[m, at : at + PART, :] = jnp.where(core == c, north, south)[:PART]
            out_ref[:, span * LANES : (span + 1) * LANES] = rows_ref[m].astype(BF16)


def served(mine, other):
    piece = pl.BlockSpec((X, AT_ONCE, 3 * OWN, LANES), lambda j, at: (0, j, 0, 0))
    out = pl.BlockSpec((BLOCK, AT_ONCE * LANES), lambda j, at: (0, j))
    return pl.pallas_call(
        serve_kernel,
        out_shape=[jax.ShapeDtypeStruct((BLOCK, D), BF16)] * 3,
        grid_spec=pltpu.PrefetchScalarGridSpec(
            num_scalar_prefetch=1,
            grid=(SPANS // AT_ONCE,),
            in_specs=[piece, piece],
            out_specs=[out] * 3,
            scratch_shapes=[pltpu.VMEM((3, BLOCK, LANES), F32)],
        ),
        cost_estimate=pl.CostEstimate(flops=10**8, bytes_accessed=2 * (2 * mine.size + 3 * BLOCK * D), transcendentals=0),
        name="serve",
    )(place("x", "core", "b"), mine, other)


def place(*axes):
    return jnp.stack([lax.axis_index(axis) for axis in axes]).astype(jnp.int32)


def traded(first, second):
    low = lax.axis_index("b") == 0
    keep, send = jnp.where(low, first, second), jnp.where(low, second, first)
    got = from_peer(send, "b", B, 1)
    return jnp.where(low, keep, got), jnp.where(low, got, keep)


def over_zq(tokens):
    two = jnp.stack([tokens, from_peer(tokens, "zq", ZQ, 2)])
    return jnp.concatenate([two, from_peer(two, "zq", ZQ, 1)])


def summed(by_y):
    send = jnp.sum(by_y[:, ZQ // 2 :].astype(F32), axis=0).astype(BF16)
    got = from_peer(send, "zq", ZQ, 1)
    kept = jnp.sum(by_y[:, : ZQ // 2].astype(F32), axis=0) + got.astype(F32)
    return kept[0] + from_peer(kept[1].astype(BF16), "zq", ZQ, 2).astype(F32)


def stepped(tokens, total):
    return (tokens.astype(F32) + 0.5 * FF ** (-0.5) * total).astype(BF16)


def local(prompt, gain_pre, gate_pre, up_pre, down_pre, gain_post, gate_post, up_post, down_post):
    half = prompt.shape[0] // B
    turned = prompt.T
    parts = by_block(
        [
            ((gain_pre[:, None] * gate_pre).astype(BF16), (gain_pre[:, None] * up_pre).astype(BF16), down_pre.astype(BF16)),
            ((gain_post[:, None] * gate_post).astype(BF16), (gain_post[:, None] * up_post).astype(BF16), down_post.astype(BF16)),
        ]
    )
    to_z = swap(parts, ("x", "core"))
    tokens = jnp.stack(traded(turned[:, :half], turned[:, half:]))
    wide = over_zq(after(tokens, to_z))
    one, two = by_span(to_z)
    one, two, wide = lax.optimization_barrier((one, two, wide))
    one = paired(one)
    pieces = over_x(one)
    two = paired(after(two, one))
    wide = share(after(wide, one), "y", Y)
    *pieces, two, wide = lax.optimization_barrier((*pieces, two, wide))
    mine, other = widened(one, pieces)
    partial = half_partial(wide, mine, other)
    partial, mine, other, two = lax.optimization_barrier((partial, mine, other, two))
    first = served(mine, other)
    pieces = over_x(two)
    by_y = swap(partial, "y")
    total, *first = lax.optimization_barrier((summed(by_y), *first))
    *pieces, total = lax.optimization_barrier((*pieces, total))
    mine, other = widened(two, pieces)
    middle = stepped(tokens, total)

    partial = half_partial(share(over_zq(middle), "y", Y), mine, other)
    partial, mine, other = lax.optimization_barrier((partial, mine, other))
    second = served(mine, other)
    by_y, *second = lax.optimization_barrier((swap(partial, "y"), *second))
    result = stepped(middle, summed(by_y))
    back = jnp.concatenate(traded(result[0], result[1]), axis=1)
    return (back.T, *first, *second)


def solution(mesh):
    fine = Mesh(mesh.devices.reshape(GR, ZQ, B, Y, X, CORE), AXES)
    tokens = P(("gr", "x", "core"), ("zq", "b", "y"))
    gain = P(("gr", "zq", "b", "y"))
    trained = P(("gr", "zq", "b", "y"), ("x", "core"))
    rows = P(("zq", "b", "y"), None)
    return jax.shard_map(
        local,
        mesh=fine,
        in_specs=(tokens, gain, trained, trained, trained, gain, trained, trained, trained),
        out_specs=(tokens,) + (rows,) * 6,
        check_vma=False,
    )
```

profile of v0, /device:TPU:6, one launch (start us, length us, event | category | flops | bytes accessed | tf_op | source)
XLA Modules:
  0.0 297.8 jit_solution(8431516820488458176)
XLA Ops:
  3.8 11.3 %all_to_all.35 = bf16[4,32,1056]{2,1,0:T(8,128)(2,1)S(1)} all-to-all(bf16[4,32,1056]{2,1,0:T(8,128)(2,1)S(1)} %reshape.59), channel_id=1, replica_groups=mesh['gr'=2,'zq'=4,'b'=2,'y'=4,'x'=4,'core'=2] {'y'}, dimensions={0} | all-to-all | bytes 540672 | tf_op jit(solution)/shard_map/all_to_all | solution.py:28
  15.5 11.9 %all_to_all.36 = bf16[8,144,128]{2,1,0:T(8,128)(2,1)S(1)} all-to-all(bf16[8,144,128]{2,1,0:T(8,128)(2,1)S(1)} %bitcast.102), channel_id=1, replica_groups=mesh['gr'=2,'zq'=4,'b'=2,'y'=4,'x'=4,'core'=2] {'x','core'}, dimensions={0} | all-to-all | bytes 589824 | tf_op jit(solution)/shard_map/all_to_all | solution.py:28
  28.3 13.5 %all-to-all-start.2 = ((bf16[8,288,128]{2,1,0:T(8,128)(2,1)}), bf16[8,288,128]{2,1,0:T(8,128)(2,1)S(1)}, u32[]{:S(2)}, u32[]{:S(2)}) async-start(bf16[8,288,128]{2,1,0:T(8,128)(2,1)} %bitcast.18), calls=%async_computation.2 | async-start | bytes 1179648 | tf_op jit(solution)/shard_map/all_to_all | solution.py:28
  41.9 2.9 collective-permute-start
  44.8 22.1 %collective-permute-done = bf16[64,256]{1,0:T(8,128)(2,1)S(1)} collective-permute-done((bf16[64,256]{1,0:T(8,128)(2,1)S(1)}, bf16[64,256]{1,0:T(8,128)(2,1)S(1)}, u32[]{:S(2)}, u32[]{:S(2)}) %collective-permute-start) | collective-permute-done | bytes 32800 | tf_op jit(solution)/shard_map/ppermute | solution.py:36
  66.9 8.1 %collective-permute-start.1 = (bf16[2,64,256]{2,1,0:T(8,128)(2,1)S(1)}, bf16[2,64,256]{2,1,0:T(8,128)(2,1)S(1)}, u32[]{:S(2)}, u32[]{:S(2)}) collective-permute-start(bf16[2,64,256]{2,1,0:T(8,128)(2,1)S(1)} %pad_maximum_fusion.9), channel_id=1, source_target_pairs={{0,128},{64,192},{128,0},{192,64},{1,129},{65,193},{129,1},{193,65... | collective-permute-start | bytes 196616 | tf_op jit(solution)/shard_map/ppermute | solution.py:36
  75.0 7.6 %collective-permute-done.1 = bf16[2,64,256]{2,1,0:T(8,128)(2,1)S(1)} collective-permute-done((bf16[2,64,256]{2,1,0:T(8,128)(2,1)S(1)}, bf16[2,64,256]{2,1,0:T(8,128)(2,1)S(1)}, u32[]{:S(2)}, u32[]{:S(2)}) %collective-permute-start.1) | collective-permute-done | bytes 65568 | tf_op jit(solution)/shard_map/ppermute | solution.py:36
  82.6 1.9 collective-permute-start.2
  84.5 8.0 %collective-permute-done.2 = bf16[2,2,64,256]{3,2,1,0:T(8,128)(2,1)S(1)} collective-permute-done((bf16[2,2,64,256]{3,2,1,0:T(8,128)(2,1)S(1)}, bf16[2,2,64,256]{3,2,1,0:T(8,128)(2,1)S(1)}, u32[]{:S(2)}, u32[]{:S(2)}) %collective-permute-start.2) | collective-permute-done | bytes 131104 | tf_op jit(solution)/shard_map/ppermute | solution.py:36
  92.7 1.9 collective-permute-start.3
  94.7 8.9 %collective-permute-done.3 = bf16[8,144,128]{2,1,0:T(8,128)(2,1)S(1)} collective-permute-done((bf16[8,144,128]{2,1,0:T(8,128)(2,1)S(1)}, bf16[8,144,128]{2,1,0:T(8,128)(2,1)S(1)}, u32[]{:S(2)}, u32[]{:S(2)}) %collective-permute-start.3) | collective-permute-done | bytes 294944 | tf_op jit(solution)/shard_map/ppermute | solution.py:36
  103.7 1.2 broadcast_in_dim.10
  104.9 3.5 %all-to-all-start.3 = ((bf16[4,4,2,64,256]{4,3,2,1,0:T(8,128)(2,1)}), bf16[4,4,2,64,256]{4,3,2,1,0:T(8,128)(2,1)S(1)}, u32[]{:S(2)}, u32[]{:S(2)}) async-start(bf16[4,4,2,64,256]{4,3,2,1,0:T(8,128)(2,1)} %broadcast_in_dim.10), calls=%async_computation.3 | async-start | bytes 2097152 | tf_op jit(solution)/shard_map/all_to_all | solution.py:28
  108.4 2.2 collective-permute-start.7
  110.6 4.0 %collective-permute-start.6 = (bf16[16,144,128]{2,1,0:T(8,128)(2,1)S(1)}, bf16[16,144,128]{2,1,0:T(8,128)(2,1)S(1)}, u32[]{:S(2)}, u32[]{:S(2)}) collective-permute-start(bf16[16,144,128]{2,1,0:T(8,128)(2,1)S(1)} %bitcast.93), channel_id=1, source_target_pairs={{0,6},{2,4},{4,2},{6,0},{1,7},{3,5},{5,3},{7,1},{8,14},{10,12},{12... | collective-permute-start | bytes 1769480 | tf_op jit(solution)/shard_map/ppermute | solution.py:36
  114.6 1.9 collective-permute-start.5
  116.5 3.9 %collective-permute-start.4 = (bf16[16,144,128]{2,1,0:T(8,128)(2,1)S(1)}, bf16[16,144,128]{2,1,0:T(8,128)(2,1)}, u32[]{:S(2)}, u32[]{:S(2)}) collective-permute-start(bf16[16,144,128]{2,1,0:T(8,128)(2,1)S(1)} %bitcast.95), channel_id=1, source_target_pairs={{0,2},{2,0},{4,6},{6,4},{1,3},{3,1},{5,7},{7,5},{8,10},{10,8},{12,... | collective-permute-start | bytes 1769480 | tf_op jit(solution)/shard_map/ppermute | solution.py:36
  121.4 19.3 %collective-permute-done.6 = bf16[16,144,128]{2,1,0:T(8,128)(2,1)S(1)} collective-permute-done((bf16[16,144,128]{2,1,0:T(8,128)(2,1)S(1)}, bf16[16,144,128]{2,1,0:T(8,128)(2,1)S(1)}, u32[]{:S(2)}, u32[]{:S(2)}) %collective-permute-start.6) | collective-permute-done | bytes 589856 | tf_op jit(solution)/shard_map/ppermute | solution.py:36
  140.8 2.6 collective-permute-done.4
  143.4 2.3 pad_maximum_fusion.mine_ref
  145.7 1.9 collective-permute-start.8
  147.7 4.6 %collective-permute-done.8.other_ref = bf16[4,16,144,128]{3,2,1,0:T(8,128)(2,1)} collective-permute-done((bf16[4,16,144,128]{3,2,1,0:T(8,128)(2,1)S(1)}, bf16[4,16,144,128]{3,2,1,0:T(8,128)(2,1)}, u32[]{:S(2)}, u32[]{:S(2)}) %collective-permute-start.8) | collective-permute-done | bytes 2359328 | tf_op jit(solution)/shard_map/ppermute | solution.py:36
  152.3 8.2 %half_step.2 = bf16[4,4,2,64,256]{4,3,2,1,0:T(8,128)(2,1)} custom-call(s32[1]{0:T(128)} %bitcast.3.at_ref, bf16[4,4,2,64,256]{4,3,2,1,0:T(8,128)(2,1)} %copy-done.2, bf16[4,16,144,128]{3,2,1,0:T(8,128)(2,1)} %copy-done, bf16[4,16,144,128]{3,2,1,0:T(8,128)(2,1)} %collective-permute-done.8.other_ref), custom_call_target="tpu_custom_call" | custom-call | flops 1207959552 | bytes 6815744 | tf_op jit(solution)/shard_map/half_step/pallas_call | solution.py:127
  160.5 4.5 %all-to-all-start.4 = ((bf16[4,4,2,64,256]{4,3,2,1,0:T(8,128)(2,1)}), bf16[4,4,2,64,256]{4,3,2,1,0:T(8,128)(2,1)S(1)}, u32[]{:S(2)}, u32[]{:S(2)}) async-start(bf16[4,4,2,64,256]{4,3,2,1,0:T(8,128)(2,1)} %half_step.2), calls=%async_computation.4 | async-start | bytes 2097152 | tf_op jit(solution)/shard_map/all_to_all | solution.py:28
  165.0 4.0 %collective-permute-start.11 = (bf16[16,144,128]{2,1,0:T(8,128)(2,1)}, bf16[16,144,128]{2,1,0:T(8,128)(2,1)S(1)}, u32[]{:S(2)}, u32[]{:S(2)}) collective-permute-start(bf16[16,144,128]{2,1,0:T(8,128)(2,1)} %bitcast.89), channel_id=1, source_target_pairs={{0,6},{2,4},{4,2},{6,0},{1,7},{3,5},{5,3},{7,1},{8,14},{10,12},{12... | collective-permute-start | bytes 1769480 | tf_op jit(solution)/shard_map/ppermute | solution.py:36
  168.9 2.2 collective-permute-start.10
  171.1 3.7 %collective-permute-start.9 = (bf16[16,144,128]{2,1,0:T(8,128)(2,1)}, bf16[16,144,128]{2,1,0:T(8,128)(2,1)S(1)}, u32[]{:S(2)}, u32[]{:S(2)}) collective-permute-start(bf16[16,144,128]{2,1,0:T(8,128)(2,1)} %bitcast.91), channel_id=1, source_target_pairs={{0,2},{2,0},{4,6},{6,4},{1,3},{3,1},{5,7},{7,5},{8,10},{10,8},{12,... | collective-permute-start | bytes 1769480 | tf_op jit(solution)/shard_map/ppermute | solution.py:36
  174.8 5.6 %all-to-all-done.4 = bf16[4,4,2,64,256]{4,3,2,1,0:T(8,128)(2,1)S(1)} async-done(((bf16[4,4,2,64,256]{4,3,2,1,0:T(8,128)(2,1)}), bf16[4,4,2,64,256]{4,3,2,1,0:T(8,128)(2,1)S(1)}, u32[]{:S(2)}, u32[]{:S(2)}) %all-to-all-start.4) | async-done | bytes 1048608 | tf_op jit(solution)/shard_map/all_to_all | solution.py:28
  180.4 1.9 collective-permute-start.12
  182.4 8.0 %collective-permute-done.12 = bf16[2,2,64,256]{3,2,1,0:T(8,128)(2,1)S(1)} collective-permute-done((bf16[2,2,64,256]{3,2,1,0:T(8,128)(2,1)S(1)}, bf16[2,2,64,256]{3,2,1,0:T(8,128)(2,1)S(1)}, u32[]{:S(2)}, u32[]{:S(2)}) %collective-permute-start.12) | collective-permute-done | bytes 131104 | tf_op jit(solution)/shard_map/ppermute | solution.py:36
  190.5 5.4 %collective-permute-start.13 = (bf16[2,64,256]{2,1,0:T(8,128)(2,1)S(1)}, bf16[2,64,256]{2,1,0:T(8,128)(2,1)S(1)}, u32[]{:S(2)}, u32[]{:S(2)}) collective-permute-start(bf16[2,64,256]{2,1,0:T(8,128)(2,1)S(1)} %fusion.5), channel_id=1, source_target_pairs={{0,128},{64,192},{128,0},{192,64},{1,129},{65,193},{129,1},{193,65... | collective-permute-start | bytes 196616 | tf_op jit(solution)/shard_map/ppermute | solution.py:36
  196.6 5.2 %serve.2 = (bf16[176,2048]{1,0:T(8,128)(2,1)}, bf16[176,2048]{1,0:T(8,128)(2,1)}, bf16[176,2048]{1,0:T(8,128)(2,1)}) custom-call(s32[3]{0:T(128)} %pad_add_fusion.at_ref, bf16[4,16,144,128]{3,2,1,0:T(8,128)(2,1)} %copy-done, bf16[4,16,144,128]{3,2,1,0:T(8,128)(2,1)} %collective-permute-done.8.other_ref), custom_call_target="tpu_custom_call" | custom-call | flops 100000000 | bytes 6881280 | tf_op jit(solution)/shard_map/serve/pallas_call | solution.py:158
  202.5 1.9 collective-permute-start.16
  204.5 3.9 %collective-permute-start.14 = (bf16[2,64,256]{2,1,0:T(8,128)(2,1)S(1)}, bf16[2,64,256]{2,1,0:T(8,128)(2,1)S(1)}, u32[]{:S(2)}, u32[]{:S(2)}) collective-permute-start(bf16[2,64,256]{2,1,0:T(8,128)(2,1)S(1)} %add_convert_fusion), channel_id=1, source_target_pairs={{0,128},{64,192},{128,0},{192,64},{1,129},{65,193},{129,1},{193,65... | collective-permute-start | bytes 196616 | tf_op jit(solution)/shard_map/ppermute | solution.py:36
  208.5 9.9 %collective-permute-done.14 = bf16[2,64,256]{2,1,0:T(8,128)(2,1)S(1)} collective-permute-done((bf16[2,64,256]{2,1,0:T(8,128)(2,1)S(1)}, bf16[2,64,256]{2,1,0:T(8,128)(2,1)S(1)}, u32[]{:S(2)}, u32[]{:S(2)}) %collective-permute-start.14) | collective-permute-done | bytes 65568 | tf_op jit(solution)/shard_map/ppermute | solution.py:36
  218.4 1.9 collective-permute-start.15
  220.3 7.5 %collective-permute-done.15 = bf16[2,2,64,256]{3,2,1,0:T(8,128)(2,1)S(1)} collective-permute-done((bf16[2,2,64,256]{3,2,1,0:T(8,128)(2,1)S(1)}, bf16[2,2,64,256]{3,2,1,0:T(8,128)(2,1)S(1)}, u32[]{:S(2)}, u32[]{:S(2)}) %collective-permute-start.15) | collective-permute-done | bytes 131104 | tf_op jit(solution)/shard_map/ppermute | solution.py:36
  228.0 18.7 %all_to_all.37.x_ref = bf16[4,4,2,64,256]{4,3,2,1,0:T(8,128)(2,1)} all-to-all(bf16[4,4,2,64,256]{4,3,2,1,0:T(8,128)(2,1)S(1)} %broadcast_in_dim.11), channel_id=1, replica_groups=mesh['gr'=2,'zq'=4,'b'=2,'y'=4,'x'=4,'core'=2] {'y'}, dimensions={0} | all-to-all | bytes 2097152 | tf_op jit(solution)/shard_map/all_to_all | solution.py:28
  246.7 8.2 %half_step.3 = bf16[4,4,2,64,256]{4,3,2,1,0:T(8,128)(2,1)} custom-call(s32[1]{0:T(128)} %bitcast.3.at_ref, bf16[4,4,2,64,256]{4,3,2,1,0:T(8,128)(2,1)} %all_to_all.37.x_ref, bf16[4,16,144,128]{3,2,1,0:T(8,128)(2,1)} %copy-done.1, bf16[4,16,144,128]{3,2,1,0:T(8,128)(2,1)} %collective-permute-done.16.other_ref), custom_call_target="tpu_custom_call" | custom-call | flops 1207959552 | bytes 6815744 | tf_op jit(solution)/shard_map/half_step/pallas_call | solution.py:127
  254.9 3.5 %all-to-all-start.6 = ((bf16[4,4,2,64,256]{4,3,2,1,0:T(8,128)(2,1)}), bf16[4,4,2,64,256]{4,3,2,1,0:T(8,128)(2,1)S(1)}, u32[]{:S(2)}, u32[]{:S(2)}) async-start(bf16[4,4,2,64,256]{4,3,2,1,0:T(8,128)(2,1)} %half_step.3), calls=%async_computation.6 | async-start | bytes 2097152 | tf_op jit(solution)/shard_map/all_to_all | solution.py:28
  258.4 5.1 %serve.3 = (bf16[176,2048]{1,0:T(8,128)(2,1)}, bf16[176,2048]{1,0:T(8,128)(2,1)}, bf16[176,2048]{1,0:T(8,128)(2,1)}) custom-call(s32[3]{0:T(128)} %pad_add_fusion.at_ref, bf16[4,16,144,128]{3,2,1,0:T(8,128)(2,1)} %copy-done.1, bf16[4,16,144,128]{3,2,1,0:T(8,128)(2,1)} %collective-permute-done.16.other_ref), custom_call_target="tpu_custom_call" | custom-call | flops 100000000 | bytes 6881280 | tf_op jit(solution)/shard_map/serve/pallas_call | solution.py:158
  263.5 9.6 %all-to-all-done.6 = bf16[4,4,2,64,256]{4,3,2,1,0:T(8,128)(2,1)S(1)} async-done(((bf16[4,4,2,64,256]{4,3,2,1,0:T(8,128)(2,1)}), bf16[4,4,2,64,256]{4,3,2,1,0:T(8,128)(2,1)S(1)}, u32[]{:S(2)}, u32[]{:S(2)}) %all-to-all-start.6) | async-done | bytes 1048608 | tf_op jit(solution)/shard_map/all_to_all | solution.py:28
  273.2 1.9 collective-permute-start.17
  275.2 5.8 %collective-permute-done.17 = bf16[2,2,64,256]{3,2,1,0:T(8,128)(2,1)S(1)} collective-permute-done((bf16[2,2,64,256]{3,2,1,0:T(8,128)(2,1)S(1)}, bf16[2,2,64,256]{3,2,1,0:T(8,128)(2,1)S(1)}, u32[]{:S(2)}, u32[]{:S(2)}) %collective-permute-start.17) | collective-permute-done | bytes 131104 | tf_op jit(solution)/shard_map/ppermute | solution.py:36
  281.0 1.9 collective-permute-start.18
  282.9 8.4 %collective-permute-done.18 = bf16[2,64,256]{2,1,0:T(8,128)(2,1)S(1)} collective-permute-done((bf16[2,64,256]{2,1,0:T(8,128)(2,1)S(1)}, bf16[2,64,256]{2,1,0:T(8,128)(2,1)S(1)}, u32[]{:S(2)}, u32[]{:S(2)}) %collective-permute-start.18) | collective-permute-done | bytes 65568 | tf_op jit(solution)/shard_map/ppermute | solution.py:36
  291.4 1.9 collective-permute-start.19
  293.3 3.9 %collective-permute-done.19 = bf16[64,256]{1,0:T(8,128)(2,1)S(1)} collective-permute-done((bf16[64,256]{1,0:T(8,128)(2,1)S(1)}, bf16[64,256]{1,0:T(8,128)(2,1)S(1)}, u32[]{:S(2)}, u32[]{:S(2)}) %collective-permute-start.19) | collective-permute-done | bytes 32800 | tf_op jit(solution)/shard_map/ppermute | solution.py:36
  (72 shorter events, 8.4 us)
Async XLA Ops:
  15.1 26.7 %copy-start.7 = (bf16[512,64]{0,1:T(8,128)(2,1)S(1)}, bf16[512,64]{0,1:T(8,128)(2,1)}, u32[]{:S(2)}) copy-start(bf16[512,64]{0,1:T(8,128)(2,1)} %param.9) | copy-start | bytes 196612
  28.3 64.3 %all-to-all-start.2 = ((bf16[8,288,128]{2,1,0:T(8,128)(2,1)}), bf16[8,288,128]{2,1,0:T(8,128)(2,1)S(1)}, u32[]{:S(2)}, u32[]{:S(2)}) async-start(bf16[8,288,128]{2,1,0:T(8,128)(2,1)} %bitcast.18), calls=%async_computation.2 | async-start | bytes 1179648 | tf_op jit(solution)/shard_map/all_to_all | solution.py:28
  41.9 25.0 %collective-permute-start = (bf16[64,256]{1,0:T(8,128)(2,1)S(1)}, bf16[64,256]{1,0:T(8,128)(2,1)S(1)}, u32[]{:S(2)}, u32[]{:S(2)}) collective-permute-start(bf16[64,256]{1,0:T(8,128)(2,1)S(1)} %broadcast_select_fusion.1), channel_id=1, source_target_pairs={{0,32},{32,0},{1,33},{33,1},{2,34},{34,2},{3,35},{35,3},{4,36},{36... | collective-permute-start | bytes 98312 | tf_op jit(solution)/shard_map/ppermute | solution.py:36
  66.9 15.7 %collective-permute-start.1 = (bf16[2,64,256]{2,1,0:T(8,128)(2,1)S(1)}, bf16[2,64,256]{2,1,0:T(8,128)(2,1)S(1)}, u32[]{:S(2)}, u32[]{:S(2)}) collective-permute-start(bf16[2,64,256]{2,1,0:T(8,128)(2,1)S(1)} %pad_maximum_fusion.9), channel_id=1, source_target_pairs={{0,128},{64,192},{128,0},{192,64},{1,129},{65,193},{129,1},{193,65... | collective-permute-start | bytes 196616 | tf_op jit(solution)/shard_map/ppermute | solution.py:36
  82.6 10.0 %collective-permute-start.2 = (bf16[2,2,64,256]{3,2,1,0:T(8,128)(2,1)S(1)}, bf16[2,2,64,256]{3,2,1,0:T(8,128)(2,1)S(1)}, u32[]{:S(2)}, u32[]{:S(2)}) collective-permute-start(bf16[2,2,64,256]{3,2,1,0:T(8,128)(2,1)S(1)} %pad_maximum_fusion.7), channel_id=1, source_target_pairs={{0,64},{64,0},{128,192},{192,128},{1,65},{65,1},{129,193},{193,129... | collective-permute-start | bytes 393224 | tf_op jit(solution)/shard_map/ppermute | solution.py:36
  92.7 10.8 %collective-permute-start.3 = (bf16[8,144,128]{2,1,0:T(8,128)(2,1)S(1)}, bf16[8,144,128]{2,1,0:T(8,128)(2,1)S(1)}, u32[]{:S(2)}, u32[]{:S(2)}) collective-permute-start(bf16[8,144,128]{2,1,0:T(8,128)(2,1)S(1)} %bitcast.105), channel_id=1, source_target_pairs={{0,32},{32,0},{1,33},{33,1},{2,34},{34,2},{3,35},{35,3},{4,36},{36... | collective-permute-start | bytes 884744 | tf_op jit(solution)/shard_map/ppermute | solution.py:36
  103.7 16.9 %copy-start.4 = (bf16[8,2,144,128]{3,2,1,0:T(8,128)(2,1)}, bf16[8,2,144,128]{3,2,1,0:T(8,128)(2,1)S(1)}, u32[]{:S(2)}) copy-start(bf16[8,2,144,128]{3,2,1,0:T(8,128)(2,1)S(1)} %copy.30) | copy-start | bytes 1769476
  104.9 38.5 %all-to-all-start.3 = ((bf16[4,4,2,64,256]{4,3,2,1,0:T(8,128)(2,1)}), bf16[4,4,2,64,256]{4,3,2,1,0:T(8,128)(2,1)S(1)}, u32[]{:S(2)}, u32[]{:S(2)}) async-start(bf16[4,4,2,64,256]{4,3,2,1,0:T(8,128)(2,1)} %broadcast_in_dim.10), calls=%async_computation.3 | async-start | bytes 2097152 | tf_op jit(solution)/shard_map/all_to_all | solution.py:28
  108.4 12.1 %collective-permute-start.7 = (bf16[8,144,128]{2,1,0:T(8,128)(2,1)S(1)}, bf16[8,144,128]{2,1,0:T(8,128)(2,1)S(1)}, u32[]{:S(2)}, u32[]{:S(2)}) collective-permute-start(bf16[8,144,128]{2,1,0:T(8,128)(2,1)S(1)} %bitcast.103), channel_id=1, source_target_pairs={{0,32},{32,0},{1,33},{33,1},{2,34},{34,2},{3,35},{35,3},{4,36},{36... | collective-permute-start | bytes 884744 | tf_op jit(solution)/shard_map/ppermute | solution.py:36
  110.6 30.1 %collective-permute-start.6 = (bf16[16,144,128]{2,1,0:T(8,128)(2,1)S(1)}, bf16[16,144,128]{2,1,0:T(8,128)(2,1)S(1)}, u32[]{:S(2)}, u32[]{:S(2)}) collective-permute-start(bf16[16,144,128]{2,1,0:T(8,128)(2,1)S(1)} %bitcast.93), channel_id=1, source_target_pairs={{0,6},{2,4},{4,2},{6,0},{1,7},{3,5},{5,3},{7,1},{8,14},{10,12},{12... | collective-permute-start | bytes 1769480 | tf_op jit(solution)/shard_map/ppermute | solution.py:36
  114.6 26.2 %collective-permute-start.5 = (bf16[16,144,128]{2,1,0:T(8,128)(2,1)S(1)}, bf16[16,144,128]{2,1,0:T(8,128)(2,1)S(1)}, u32[]{:S(2)}, u32[]{:S(2)}) collective-permute-start(bf16[16,144,128]{2,1,0:T(8,128)(2,1)S(1)} %bitcast.94), channel_id=1, source_target_pairs={{0,4},{2,6},{4,0},{6,2},{1,5},{3,7},{5,1},{7,3},{8,12},{10,14},{12... | collective-permute-start | bytes 1769480 | tf_op jit(solution)/shard_map/ppermute | solution.py:36
  116.5 26.9 %collective-permute-start.4 = (bf16[16,144,128]{2,1,0:T(8,128)(2,1)S(1)}, bf16[16,144,128]{2,1,0:T(8,128)(2,1)}, u32[]{:S(2)}, u32[]{:S(2)}) collective-permute-start(bf16[16,144,128]{2,1,0:T(8,128)(2,1)S(1)} %bitcast.95), channel_id=1, source_target_pairs={{0,2},{2,0},{4,6},{6,4},{1,3},{3,1},{5,7},{7,5},{8,10},{10,8},{12,... | collective-permute-start | bytes 1769480 | tf_op jit(solution)/shard_map/ppermute | solution.py:36
  140.8 2.7 copy-start.5
  140.8 2.7 copy-start.6
  143.4 2.3 copy-start.2
  145.7 6.6 %copy-start = (bf16[4,16,144,128]{3,2,1,0:T(8,128)(2,1)}, bf16[4,16,144,128]{3,2,1,0:T(8,128)(2,1)S(1)}, u32[]{:S(2)}) copy-start(bf16[4,16,144,128]{3,2,1,0:T(8,128)(2,1)S(1)} %pad_maximum_fusion.mine_ref) | copy-start | bytes 7077892
  145.7 6.6 %collective-permute-start.8 = (bf16[4,16,144,128]{3,2,1,0:T(8,128)(2,1)S(1)}, bf16[4,16,144,128]{3,2,1,0:T(8,128)(2,1)}, u32[]{:S(2)}, u32[]{:S(2)}) collective-permute-start(bf16[4,16,144,128]{3,2,1,0:T(8,128)(2,1)S(1)} %pad_maximum_fusion.mine_ref), channel_id=1, source_target_pairs={{0,1},{1,0},{2,3},{3,2},{4,5},{5,4},{6,7},{7,6},{8,9},{9,8},{10,11... | collective-permute-start | bytes 7077896 | tf_op jit(solution)/shard_map/ppermute | solution.py:36
  160.5 19.9 %all-to-all-start.4 = ((bf16[4,4,2,64,256]{4,3,2,1,0:T(8,128)(2,1)}), bf16[4,4,2,64,256]{4,3,2,1,0:T(8,128)(2,1)S(1)}, u32[]{:S(2)}, u32[]{:S(2)}) async-start(bf16[4,4,2,64,256]{4,3,2,1,0:T(8,128)(2,1)} %half_step.2), calls=%async_computation.4 | async-start | bytes 2097152 | tf_op jit(solution)/shard_map/all_to_all | solution.py:28
  165.0 37.2 %collective-permute-start.11 = (bf16[16,144,128]{2,1,0:T(8,128)(2,1)}, bf16[16,144,128]{2,1,0:T(8,128)(2,1)S(1)}, u32[]{:S(2)}, u32[]{:S(2)}) collective-permute-start(bf16[16,144,128]{2,1,0:T(8,128)(2,1)} %bitcast.89), channel_id=1, source_target_pairs={{0,6},{2,4},{4,2},{6,0},{1,7},{3,5},{5,3},{7,1},{8,14},{10,12},{12... | collective-permute-start | bytes 1769480 | tf_op jit(solution)/shard_map/ppermute | solution.py:36
  168.9 33.3 %collective-permute-start.10 = (bf16[16,144,128]{2,1,0:T(8,128)(2,1)}, bf16[16,144,128]{2,1,0:T(8,128)(2,1)S(1)}, u32[]{:S(2)}, u32[]{:S(2)}) collective-permute-start(bf16[16,144,128]{2,1,0:T(8,128)(2,1)} %bitcast.90), channel_id=1, source_target_pairs={{0,4},{2,6},{4,0},{6,2},{1,5},{3,7},{5,1},{7,3},{8,12},{10,14},{12... | collective-permute-start | bytes 1769480 | tf_op jit(solution)/shard_map/ppermute | solution.py:36
  171.1 31.1 %collective-permute-start.9 = (bf16[16,144,128]{2,1,0:T(8,128)(2,1)}, bf16[16,144,128]{2,1,0:T(8,128)(2,1)S(1)}, u32[]{:S(2)}, u32[]{:S(2)}) collective-permute-start(bf16[16,144,128]{2,1,0:T(8,128)(2,1)} %bitcast.91), channel_id=1, source_target_pairs={{0,2},{2,0},{4,6},{6,4},{1,3},{3,1},{5,7},{7,5},{8,10},{10,8},{12,... | collective-permute-start | bytes 1769480 | tf_op jit(solution)/shard_map/ppermute | solution.py:36
  180.4 10.0 %collective-permute-start.12 = (bf16[2,2,64,256]{3,2,1,0:T(8,128)(2,1)S(1)}, bf16[2,2,64,256]{3,2,1,0:T(8,128)(2,1)S(1)}, u32[]{:S(2)}, u32[]{:S(2)}) collective-permute-start(bf16[2,2,64,256]{3,2,1,0:T(8,128)(2,1)S(1)} %slice_reduce_fusion), channel_id=1, source_target_pairs={{0,64},{64,0},{128,192},{192,128},{1,65},{65,1},{129,193},{193,129... | collective-permute-start | bytes 393224 | tf_op jit(solution)/shard_map/ppermute | solution.py:36
  190.5 11.7 %collective-permute-start.13 = (bf16[2,64,256]{2,1,0:T(8,128)(2,1)S(1)}, bf16[2,64,256]{2,1,0:T(8,128)(2,1)S(1)}, u32[]{:S(2)}, u32[]{:S(2)}) collective-permute-start(bf16[2,64,256]{2,1,0:T(8,128)(2,1)S(1)} %fusion.5), channel_id=1, source_target_pairs={{0,128},{64,192},{128,0},{192,64},{1,129},{65,193},{129,1},{193,65... | collective-permute-start | bytes 196616 | tf_op jit(solution)/shard_map/ppermute | solution.py:36
  196.6 5.7 %copy-start.3 = (bf16[8,2,144,128]{3,2,1,0:T(8,128)(2,1)S(1)}, bf16[8,2,144,128]{3,2,1,0:T(8,128)(2,1)}, u32[]{:S(2)}) copy-start(bf16[8,2,144,128]{3,2,1,0:T(8,128)(2,1)} %copy.31) | copy-start | bytes 1769476
  202.5 44.2 %copy-start.1 = (bf16[4,16,144,128]{3,2,1,0:T(8,128)(2,1)}, bf16[4,16,144,128]{3,2,1,0:T(8,128)(2,1)S(1)}, u32[]{:S(2)}) copy-start(bf16[4,16,144,128]{3,2,1,0:T(8,128)(2,1)S(1)} %pad_maximum_fusion.1.mine_ref) | copy-start | bytes 7077892
  202.5 44.2 %collective-permute-start.16 = (bf16[4,16,144,128]{3,2,1,0:T(8,128)(2,1)S(1)}, bf16[4,16,144,128]{3,2,1,0:T(8,128)(2,1)}, u32[]{:S(2)}, u32[]{:S(2)}) collective-permute-start(bf16[4,16,144,128]{3,2,1,0:T(8,128)(2,1)S(1)} %pad_maximum_fusion.1.mine_ref), channel_id=1, source_target_pairs={{0,1},{1,0},{2,3},{3,2},{4,5},{5,4},{6,7},{7,6},{8,9},{9,8},{10,11... | collective-permute-start | bytes 7077896 | tf_op jit(solution)/shard_map/ppermute | solution.py:36
  204.5 13.9 %collective-permute-start.14 = (bf16[2,64,256]{2,1,0:T(8,128)(2,1)S(1)}, bf16[2,64,256]{2,1,0:T(8,128)(2,1)S(1)}, u32[]{:S(2)}, u32[]{:S(2)}) collective-permute-start(bf16[2,64,256]{2,1,0:T(8,128)(2,1)S(1)} %add_convert_fusion), channel_id=1, source_target_pairs={{0,128},{64,192},{128,0},{192,64},{1,129},{65,193},{129,1},{193,65... | collective-permute-start | bytes 196616 | tf_op jit(solution)/shard_map/ppermute | solution.py:36
  218.4 9.5 %collective-permute-start.15 = (bf16[2,2,64,256]{3,2,1,0:T(8,128)(2,1)S(1)}, bf16[2,2,64,256]{3,2,1,0:T(8,128)(2,1)S(1)}, u32[]{:S(2)}, u32[]{:S(2)}) collective-permute-start(bf16[2,2,64,256]{3,2,1,0:T(8,128)(2,1)S(1)} %pad_maximum_fusion.8), channel_id=1, source_target_pairs={{0,64},{64,0},{128,192},{192,128},{1,65},{65,1},{129,193},{193,129... | collective-permute-start | bytes 393224 | tf_op jit(solution)/shard_map/ppermute | solution.py:36
  254.9 18.2 %all-to-all-start.6 = ((bf16[4,4,2,64,256]{4,3,2,1,0:T(8,128)(2,1)}), bf16[4,4,2,64,256]{4,3,2,1,0:T(8,128)(2,1)S(1)}, u32[]{:S(2)}, u32[]{:S(2)}) async-start(bf16[4,4,2,64,256]{4,3,2,1,0:T(8,128)(2,1)} %half_step.3), calls=%async_computation.6 | async-start | bytes 2097152 | tf_op jit(solution)/shard_map/all_to_all | solution.py:28
  273.2 7.8 %collective-permute-start.17 = (bf16[2,2,64,256]{3,2,1,0:T(8,128)(2,1)S(1)}, bf16[2,2,64,256]{3,2,1,0:T(8,128)(2,1)S(1)}, u32[]{:S(2)}, u32[]{:S(2)}) collective-permute-start(bf16[2,2,64,256]{3,2,1,0:T(8,128)(2,1)S(1)} %slice_reduce_fusion.1), channel_id=1, source_target_pairs={{0,64},{64,0},{128,192},{192,128},{1,65},{65,1},{129,193},{193,129... | collective-permute-start | bytes 393224 | tf_op jit(solution)/shard_map/ppermute | solution.py:36
  281.0 10.3 %collective-permute-start.18 = (bf16[2,64,256]{2,1,0:T(8,128)(2,1)S(1)}, bf16[2,64,256]{2,1,0:T(8,128)(2,1)S(1)}, u32[]{:S(2)}, u32[]{:S(2)}) collective-permute-start(bf16[2,64,256]{2,1,0:T(8,128)(2,1)S(1)} %fusion.6), channel_id=1, source_target_pairs={{0,128},{64,192},{128,0},{192,64},{1,129},{65,193},{129,1},{193,65... | collective-permute-start | bytes 196616 | tf_op jit(solution)/shard_map/ppermute | solution.py:36
  291.4 5.8 %collective-permute-start.19 = (bf16[64,256]{1,0:T(8,128)(2,1)S(1)}, bf16[64,256]{1,0:T(8,128)(2,1)S(1)}, u32[]{:S(2)}, u32[]{:S(2)}) collective-permute-start(bf16[64,256]{1,0:T(8,128)(2,1)S(1)} %select_bitcast_fusion.4), channel_id=1, source_target_pairs={{0,32},{32,0},{1,33},{33,1},{2,34},{34,2},{3,35},{35,3},{4,36},{36... | collective-permute-start | bytes 98312 | tf_op jit(solution)/shard_map/ppermute | solution.py:36
where the time goes:
time: 300 us; the launch traced here: 298 us
  waiting for transfers between devices  132 us (44%)
  starting transfers between devices  84.5 us (28%)
  blocking collectives  41.9 us (14%)
  Pallas kernels  26.7 us (9%)
  other arithmetic  6.89 us (2%)
  local copies, waits for them, and re-layouts  4.46 us (1%)
    ppermute x20, waiting for transfers between devices, from_peer(): return lax.ppermute(block, axis, [(i, i ^ flip) for i in range(size)])  117 us
    ppermute x20, starting transfers between devices, from_peer(): return lax.ppermute(block, axis, [(i, i ^ flip) for i in range(size)])  59.5 us
    all_to_all x3, blocking collectives, swap(): return lax.all_to_all(blocks, axis, split_axis=0, concat_axis=0, tiled=True)  41.9 us
    all_to_all x4, starting transfers between devices, swap(): return lax.all_to_all(blocks, axis, split_axis=0, concat_axis=0, tiled=True)  25 us
    pallas_call x2, Pallas kernels, half_partial(): pl.pallas_call(half_kernel, out_shape=jax.ShapeDtypeStruct(tokens.shape,...  16.4 us
    all_to_all x4, waiting for transfers between devices, swap(): return lax.all_to_all(blocks, axis, split_axis=0, concat_axis=0, tiled=True)  15.2 us
    pallas_call x2, Pallas kernels, served(): pl.pallas_call(serve_kernel, out_shape=[jax.ShapeDtypeStruct((BLOCK, D),...  10.3 us
  transfers between devices with their start and end apart: 24, of which 16 were waited for; matrix products, arithmetic and copies ran while one was open for 1% of the time, Pallas kernels for 3%

commit v1 on v0

v1 whole, which is shorter than its diff:
```python
import jax
import jax.numpy as jnp
from jax import lax
from jax.experimental import pallas as pl
from jax.experimental.pallas import tpu as pltpu
from jax.sharding import Mesh
from jax.sharding import PartitionSpec as P

D = 2048
FF = 5632
NORM_EPS = 1e-06
GR, ZQ, B, Y, X, CORE = 2, 4, 2, 4, 4, 2
AXES = ("gr", "zq", "b", "y", "x", "core")
ZL = ZQ * B
F32, BF16 = jnp.float32, jnp.bfloat16
BLOCK = FF // (ZL * Y)
ROWS = D // (GR * ZL * Y)
PART = BLOCK // X
PADDED = 48
LANES = Y * ROWS
SPANS = GR * ZL
PIECE = 3 * PADDED
FEATS = D // (ZL * Y)
AT_ONCE = 4


def swap(blocks, axis):
    return lax.all_to_all(blocks, axis, split_axis=0, concat_axis=0, tiled=True)


def share(block, axis, size):
    return swap(jnp.broadcast_to(block[None], (size, *block.shape)), axis)


def from_peer(block, axis, size, flip):
    return lax.ppermute(block, axis, [(i, i ^ flip) for i in range(size)])


def after(value, *others):
    return lax.optimization_barrier((value, *others))[0]


def by_block(layers):
    cols = jnp.stack([matrix for matrices in layers for matrix in matrices])
    n = cols.shape[0]
    to_yx = cols.reshape(n, ROWS, Y * X, PART).transpose(2, 1, 0, 3).reshape(Y * X, ROWS, n * PART)
    here = swap(to_yx, ("y", "x")).reshape(Y, X, ROWS, n * PART)
    turned = here.transpose(1, 3, 0, 2).reshape(X, n, PART, LANES)
    return jnp.pad(turned, ((0, 0), (0, 0), (0, PADDED - PART), (0, 0))).reshape(X, n * PADDED, LANES)


def by_span(parts):
    to_z = jnp.broadcast_to(parts[None], (GR, *parts.shape)).reshape(GR * ZQ, *parts.shape[1:])
    here = swap(to_z, ("gr", "zq"))
    return [here[:, i : i + PIECE] for i in range(0, here.shape[1], PIECE)]


def paired(piece):
    near = from_peer(piece, "b", B, 1)
    low = lax.axis_index("b") == 0
    both = jnp.stack([jnp.where(low, piece, near), jnp.where(low, near, piece)], axis=1)
    return both.reshape(SPANS, PIECE, LANES)


def over_x(pair):
    return [pair] + [from_peer(pair, "x", X, k) for k in range(1, X)]


def over_core(pieces):
    return [from_peer(piece, "core", CORE, 1) for piece in pieces]


def slot(zl, zq):
    k = (zl // B) ^ zq
    return ((k & 1) << 1) | (k >> 1), zl % B


def half_kernel(at_ref, x_ref, *refs):
    piece_refs, (out_ref, acc_ref, sq_ref) = refs[: 2 * X], refs[2 * X :]
    width = x_ref.shape[-1]
    pieces = 2 * X
    zq = at_ref[0]

    def rows(span, lo, hi):
        return jnp.concatenate([ref[span, lo:hi, :] for ref in piece_refs], axis=0)

    def both(zl, lo, hi):
        return jnp.concatenate([rows(2 * zl, lo, hi), rows(2 * zl + 1, lo, hi)], axis=1)

    acc_ref[...] = jnp.zeros_like(acc_ref)
    sq_ref[...] = jnp.zeros_like(sq_ref)

    def inward(zl, _):
        k, b = slot(zl, zq)
        tokens = x_ref[:, k, b].reshape(Y * FEATS, width)
        wide = tokens.astype(F32)
        sq_ref[...] += jnp.sum((wide * wide).reshape(Y * FEATS // 8, 8, width), axis=0)
        acc_ref[...] += jnp.dot(both(zl, 0, 2 * PADDED), tokens, preferred_element_type=F32)
        return 0

    lax.fori_loop(0, ZL, inward, 0)
    squares = jnp.sum(sq_ref[...], axis=0, keepdims=True)
    scale = lax.rsqrt(squares / D + NORM_EPS) * D ** (-0.5)
    sums = acc_ref[...].reshape(pieces, 2 * PADDED, width)
    gate = sums[:, :PADDED].reshape(pieces * PADDED, width) * scale
    up = sums[:, PADDED:].reshape(pieces * PADDED, width) * scale
    hidden = (gate / (1.0 + jnp.exp(-gate)) * up).astype(BF16)

    def outward(zl, _):
        part = lax.dot_general(
            both(zl, 2 * PADDED, PIECE), hidden, (((0,), (0,)), ((), ())), preferred_element_type=F32
        )
        k, b = slot(zl, zq)
        out_ref[:, k, b] = part.astype(BF16).reshape(Y, FEATS, width)
        return 0

    lax.fori_loop(0, ZL, outward, 0)


def half_partial(tokens, pieces):
    width = tokens.shape[-1]
    vmem = pl.BlockSpec(memory_space=pltpu.VMEM)
    flops = 2 * 3 * 2 * X * PADDED * D * width
    return pl.pallas_call(
        half_kernel,
        out_shape=jax.ShapeDtypeStruct(tokens.shape, BF16),
        in_specs=[pl.BlockSpec(memory_space=pltpu.SMEM)] + [vmem] * (1 + 2 * X),
        out_specs=vmem,
        scratch_shapes=[pltpu.VMEM((2 * X * 2 * PADDED, width), F32), pltpu.VMEM((8, width), F32)],
        cost_estimate=pl.CostEstimate(
            flops=flops, bytes_accessed=2 * (2 * tokens.size + 2 * X * pieces[0].size), transcendentals=0
        ),
        name="half_step",
    )(place("zq"), tokens, *pieces)


def serve_kernel(at_ref, *refs):
    piece_refs, out_refs, rows_ref = refs[: 2 * X], refs[2 * X : -1], refs[-1]
    x, here = at_ref[0], at_ref[1] == at_ref[2]
    odd, high = (x & 1) == 1, (x & 2) == 2
    for span in range(AT_ONCE):
        for m, out_ref in enumerate(out_refs):
            lo, hi = m * PADDED, (m + 1) * PADDED
            mine = [ref[span, lo:hi, :].astype(F32) for ref in piece_refs[:X]]
            other = [ref[span, lo:hi, :].astype(F32) for ref in piece_refs[X:]]
            p = [jnp.where(here, a, b) for a, b in zip(mine, other)]
            p = [jnp.where(odd, p[k ^ 1], p[k]) for k in range(X)]
            p = [jnp.where(high, p[k ^ 2], p[k]) for k in range(X)]
            for k in range(X):
                rows_ref[m, k * PART : (k + 1) * PART, :] = p[k][:PART]
            out_ref[:, span * LANES : (span + 1) * LANES] = rows_ref[m].astype(BF16)


def served(pieces):
    piece = pl.BlockSpec((AT_ONCE, PIECE, LANES), lambda j, at: (j, 0, 0))
    out = pl.BlockSpec((BLOCK, AT_ONCE * LANES), lambda j, at: (0, j))
    return pl.pallas_call(
        serve_kernel,
        out_shape=[jax.ShapeDtypeStruct((BLOCK, D), BF16)] * 3,
        grid_spec=pltpu.PrefetchScalarGridSpec(
            num_scalar_prefetch=1,
            grid=(SPANS // AT_ONCE,),
            in_specs=[piece] * (2 * X),
            out_specs=[out] * 3,
            scratch_shapes=[pltpu.VMEM((3, BLOCK, LANES), F32)],
        ),
        cost_estimate=pl.CostEstimate(
            flops=10**8, bytes_accessed=2 * (2 * X * pieces[0].size + 3 * BLOCK * D), transcendentals=0
        ),
        name="serve",
    )(place("x", "core", "b"), *pieces)


def place(*axes):
    return jnp.stack([lax.axis_index(axis) for axis in axes]).astype(jnp.int32)


def traded(first, second):
    low = lax.axis_index("b") == 0
    keep, send = jnp.where(low, first, second), jnp.where(low, second, first)
    got = from_peer(send, "b", B, 1)
    return jnp.where(low, keep, got), jnp.where(low, got, keep)


def far_zq(tokens):
    return jnp.stack([tokens, from_peer(tokens, "zq", ZQ, 2)])


def near_zq(two):
    return jnp.concatenate([two, from_peer(two, "zq", ZQ, 1)])


def summed(by_y):
    send = jnp.sum(by_y[:, ZQ // 2 :].astype(F32), axis=0).astype(BF16)
    got = from_peer(send, "zq", ZQ, 1)
    kept = jnp.sum(by_y[:, : ZQ // 2].astype(F32), axis=0) + got.astype(F32)
    return kept[0] + from_peer(kept[1].astype(BF16), "zq", ZQ, 2).astype(F32)


def stepped(tokens, total):
    return (tokens.astype(F32) + 0.5 * FF ** (-0.5) * total).astype(BF16)


def local(prompt, gain_pre, gate_pre, up_pre, down_pre, gain_post, gate_post, up_post, down_post):
    half = prompt.shape[0] // B
    turned = prompt.T
    parts = by_block(
        [
            ((gain_pre[:, None] * gate_pre).astype(BF16), (gain_pre[:, None] * up_pre).astype(BF16), down_pre.astype(BF16)),
            ((gain_post[:, None] * gate_post).astype(BF16), (gain_post[:, None] * up_post).astype(BF16), down_post.astype(BF16)),
        ]
    )
    tokens = jnp.stack(traded(turned[:, :half], turned[:, half:]))
    parts, wide = lax.optimization_barrier((parts, far_zq(tokens)))
    one, two = by_span(parts)
    one = paired(one)
    pieces = over_x(one)
    wide = near_zq(after(wide, one))
    wide = share(wide, "y", Y)
    two = paired(after(two, one))
    pieces += over_core(pieces)
    wide, two, *pieces = lax.optimization_barrier((wide, two, *pieces))
    partial = half_partial(wide, pieces)
    partial, two, *pieces = lax.optimization_barrier((partial, two, *pieces))
    first = served(pieces)
    pieces = over_x(two)
    by_y = swap(partial, "y")
    total, *first = lax.optimization_barrier((summed(by_y), *first))
    total, *pieces = lax.optimization_barrier((total, *pieces))
    middle = stepped(tokens, total)
    pieces += over_core(pieces)

    partial = half_partial(share(near_zq(far_zq(middle)), "y", Y), pieces)
    partial, *pieces = lax.optimization_barrier((partial, *pieces))
    second = served(pieces)
    by_y, *second = lax.optimization_barrier((swap(partial, "y"), *second))
    result = stepped(middle, summed(by_y))
    back = jnp.concatenate(traded(result[0], result[1]), axis=1)
    return (back.T, *first, *second)


def solution(mesh):
    fine = Mesh(mesh.devices.reshape(GR, ZQ, B, Y, X, CORE), AXES)
    tokens = P(("gr", "x", "core"), ("zq", "b", "y"))
    gain = P(("gr", "zq", "b", "y"))
    trained = P(("gr", "zq", "b", "y"), ("x", "core"))
    rows = P(("zq", "b", "y"), None)
    return jax.shard_map(
        local,
        mesh=fine,
        in_specs=(tokens, gain, trained, trained, trained, gain, trained, trained, trained),
        out_specs=(tokens,) + (rows,) * 6,
        check_vma=False,
    )
```

time: 300 us -> 276 us (0.920)
  waiting for transfers between devices: 132 us -> 75.8 us
  starting transfers between devices: 84.5 us -> 104 us
  local copies, waits for them, and re-layouts: 4.46 us -> 13.5 us
  blocking collectives: 41.9 us -> 45 us
    ppermute x20 -> x26, waiting for transfers between devices: 117 us -> 58.1 us  [from_peer(): return lax.ppermute(block, axis, [(i, i ^ flip) for i in range(size)])]
    ppermute x20 -> x26, starting transfers between devices: 59.5 us -> 80.7 us  [from_peer(): return lax.ppermute(block, axis, [(i, i ^ flip) for i in range(size)])]
    another operation x3 -> x13, local copies, waits for them, and re-layouts: 0.12 us -> 5.27 us  [by_block(): cols = jnp.stack([matrix for matrices in layers for matrix in matrices])]
    another operation x10 -> x4, other arithmetic: 4.86 us -> 0.06 us  [far_zq(): return jnp.stack([tokens, from_peer(tokens, 'zq', ZQ, 2)])]
    convert_element_type x0 -> x4, other arithmetic: none -> 3.88 us  [the longest x1 1.04 us: local(): (gain_pre[:, None] * up_pre).astype(BF16)]
    all_to_all x3 -> x1, blocking collectives: 41.9 us -> 45 us  [swap(): return lax.all_to_all(blocks, axis, split_axis=0, concat_axis=0, tiled=True)]
    all_to_all x4 -> x5, waiting for transfers between devices: 15.2 us -> 17.7 us  [swap(): return lax.all_to_all(blocks, axis, split_axis=0, concat_axis=0, tiled=True)]
    all_to_all x4 -> x5, starting transfers between devices: 25 us -> 23 us  [swap(): return lax.all_to_all(blocks, axis, split_axis=0, concat_axis=0, tiled=True)]
  transfers between devices with their start and end apart: 24 -> 31, of which waited for: 16 -> 15; matrix products, arithmetic and copies ran while one was open for 1% -> 5% of each run, Pallas kernels for 3% -> 4%
where the time goes in v1:
time: 276 us; the launch traced here: 273 us
  starting transfers between devices  104 us (38%)
  waiting for transfers between devices  75.8 us (27%)
  blocking collectives  45 us (16%)
  Pallas kernels  26.9 us (10%)
  local copies, waits for them, and re-layouts  13.5 us (5%)
  other arithmetic  6.74 us (2%)
    ppermute x26, starting transfers between devices, from_peer(): return lax.ppermute(block, axis, [(i, i ^ flip) for i in range(size)])  80.7 us
    ppermute x26, waiting for transfers between devices, from_peer(): return lax.ppermute(block, axis, [(i, i ^ flip) for i in range(size)])  58.1 us
    all_to_all x1, blocking collectives, swap(): return lax.all_to_all(blocks, axis, split_axis=0, concat_axis=0, tiled=True)  45 us
    all_to_all x5, starting transfers between devices, swap(): return lax.all_to_all(blocks, axis, split_axis=0, concat_axis=0, tiled=True)  23 us
    all_to_all x5, waiting for transfers between devices, swap(): return lax.all_to_all(blocks, axis, split_axis=0, concat_axis=0, tiled=True)  17.7 us
    pallas_call x2, Pallas kernels, half_partial(): pl.pallas_call(half_kernel, out_shape=jax.ShapeDtypeStruct(tokens.shape,...  16.3 us
    pallas_call x2, Pallas kernels, served(): pl.pallas_call(serve_kernel, out_shape=[jax.ShapeDtypeStruct((BLOCK, D),...  10.7 us
  transfers between devices with their start and end apart: 31, of which 15 were waited for; matrix products, arithmetic and copies ran while one was open for 5% of the time, Pallas kernels for 4%

profile of v1, /device:TPU:6, one launch (start us, length us, event | category | flops | bytes accessed | tf_op | source)
XLA Modules:
  0.0 273.1 jit_solution(18049656465714724881)
XLA Ops:
  1.4 3.8 %collective-permute-start = (bf16[64,256]{1,0:T(8,128)(2,1)S(1)}, bf16[64,256]{1,0:T(8,128)(2,1)S(1)}, u32[]{:S(2)}, u32[]{:S(2)}) collective-permute-start(bf16[64,256]{1,0:T(8,128)(2,1)S(1)} %broadcast_select_fusion.1), channel_id=1, source_target_pairs={{0,32},{32,0},{1,33},{33,1},{2,34},{34,2},{3,35},{35,3},{4,36},{36... | collective-permute-start | bytes 98312 | tf_op jit(solution)/shard_map/ppermute | solution.py:36
  12.0 2.5 stack.96
  15.9 7.4 %all-to-all-start = ((bf16[16,32,264]{2,1,0:T(8,128)(2,1)}), bf16[16,32,264]{2,1,0:T(8,128)(2,1)S(1)}, u32[]{:S(2)}, u32[]{:S(2)}) async-start(bf16[16,32,264]{2,1,0:T(8,128)(2,1)} %reshape.59), calls=%async_computation | async-start | bytes 786432 | tf_op jit(solution)/shard_map/all_to_all | solution.py:28
  23.4 9.1 %collective-permute-start.1 = (bf16[2,64,256]{2,1,0:T(8,128)(2,1)S(1)}, bf16[2,64,256]{2,1,0:T(8,128)(2,1)S(1)}, u32[]{:S(2)}, u32[]{:S(2)}) collective-permute-start(bf16[2,64,256]{2,1,0:T(8,128)(2,1)S(1)} %get-tuple-element.121), channel_id=1, source_target_pairs={{0,128},{64,192},{128,0},{192,64},{1,129},{65,193},{129,1},{193,65... | collective-permute-start | bytes 196616 | tf_op jit(solution)/shard_map/ppermute | solution.py:36
  32.5 5.7 %collective-permute-done.1 = bf16[2,64,256]{2,1,0:T(8,128)(2,1)S(1)} collective-permute-done((bf16[2,64,256]{2,1,0:T(8,128)(2,1)S(1)}, bf16[2,64,256]{2,1,0:T(8,128)(2,1)S(1)}, u32[]{:S(2)}, u32[]{:S(2)}) %collective-permute-start.1) | collective-permute-done | bytes 65568 | tf_op jit(solution)/shard_map/ppermute | solution.py:36
  39.9 45.0 %all_to_all.30 = bf16[8,288,128]{2,1,0:T(8,128)(2,1)S(1)} all-to-all(bf16[8,288,128]{2,1,0:T(8,128)(2,1)S(1)} %bitcast.73), channel_id=1, replica_groups=mesh['gr'=2,'zq'=4,'b'=2,'y'=4,'x'=4,'core'=2] {'gr','zq'}, dimensions={0} | all-to-all | bytes 1179648 | tf_op jit(solution)/shard_map/all_to_all | solution.py:28
  85.0 2.4 collective-permute-start.2
  87.4 8.1 %collective-permute-done.2 = bf16[8,144,128]{2,1,0:T(8,128)(2,1)S(1)} collective-permute-done((bf16[8,144,128]{2,1,0:T(8,128)(2,1)S(1)}, bf16[8,144,128]{2,1,0:T(8,128)(2,1)S(1)}, u32[]{:S(2)}, u32[]{:S(2)}) %collective-permute-start.2) | collective-permute-done | bytes 294944 | tf_op jit(solution)/shard_map/ppermute | solution.py:36
  95.7 1.9 collective-permute-start.7
  97.6 4.8 %collective-permute-start.6 = (bf16[16,144,128]{2,1,0:T(8,128)(2,1)S(1)}, bf16[16,144,128]{2,1,0:T(8,128)(2,1)S(1)}, u32[]{:S(2)}, u32[]{:S(2)}) collective-permute-start(bf16[16,144,128]{2,1,0:T(8,128)(2,1)S(1)} %bitcast.67), channel_id=1, source_target_pairs={{0,4},{2,6},{4,0},{6,2},{1,5},{3,7},{5,1},{7,3},{8,12},{10,14},{12... | collective-permute-start | bytes 1769480 | tf_op jit(solution)/shard_map/ppermute | solution.py:36
  102.4 3.1 %collective-permute-start.5 = (bf16[16,144,128]{2,1,0:T(8,128)(2,1)S(1)}, bf16[16,144,128]{2,1,0:T(8,128)(2,1)}, u32[]{:S(2)}, u32[]{:S(2)}) collective-permute-start(bf16[16,144,128]{2,1,0:T(8,128)(2,1)S(1)} %bitcast.68), channel_id=1, source_target_pairs={{0,2},{2,0},{4,6},{6,4},{1,3},{3,1},{5,7},{7,5},{8,10},{10,8},{12,... | collective-permute-start | bytes 1769480 | tf_op jit(solution)/shard_map/ppermute | solution.py:36
  105.5 3.9 %collective-permute-start.3 = (bf16[2,2,64,256]{3,2,1,0:T(8,128)(2,1)S(1)}, bf16[2,2,64,256]{3,2,1,0:T(8,128)(2,1)S(1)}, u32[]{:S(2)}, u32[]{:S(2)}) collective-permute-start(bf16[2,2,64,256]{3,2,1,0:T(8,128)(2,1)S(1)} %pad_maximum_fusion.4), channel_id=1, source_target_pairs={{0,64},{64,0},{128,192},{192,128},{1,65},{65,1},{129,193},{193,129... | collective-permute-start | bytes 393224 | tf_op jit(solution)/shard_map/ppermute | solution.py:36
  109.5 5.0 %collective-permute-done.3 = bf16[2,2,64,256]{3,2,1,0:T(8,128)(2,1)S(1)} collective-permute-done((bf16[2,2,64,256]{3,2,1,0:T(8,128)(2,1)S(1)}, bf16[2,2,64,256]{3,2,1,0:T(8,128)(2,1)S(1)}, u32[]{:S(2)}, u32[]{:S(2)}) %collective-permute-start.3) | collective-permute-done | bytes 131104 | tf_op jit(solution)/shard_map/ppermute | solution.py:36
  115.6 4.2 %all-to-all-start.2 = ((bf16[4,4,2,64,256]{4,3,2,1,0:T(8,128)(2,1)}), bf16[4,4,2,64,256]{4,3,2,1,0:T(8,128)(2,1)S(1)}, u32[]{:S(2)}, u32[]{:S(2)}) async-start(bf16[4,4,2,64,256]{4,3,2,1,0:T(8,128)(2,1)} %broadcast_in_dim.7), calls=%async_computation.2 | async-start | bytes 2097152 | tf_op jit(solution)/shard_map/all_to_all | solution.py:28
  121.7 1.9 collective-permute-start.8
  127.5 2.4 collective-permute-start.10
  129.9 1.9 collective-permute-start.9
  132.0 2.1 collective-permute-done.9.refs_5_
  134.1 8.1 %half_step.2 = bf16[4,4,2,64,256]{4,3,2,1,0:T(8,128)(2,1)} custom-call(s32[1]{0:T(128)} %bitcast.3.at_ref, bf16[4,4,2,64,256]{4,3,2,1,0:T(8,128)(2,1)} %copy-done.2, bf16[16,144,128]{2,1,0:T(8,128)(2,1)} %bitcast.70, bf16[16,144,128]{2,1,0:T(8,128)(2,1)} %collective-permute-done.5.refs_1_, bf16[16,144,128]{2,1,0:T(8,128)(2,1)} %copy-done.5, ...), custom_call_target="tpu_custom_call" | custom-call | flops 1207959552 | bytes 6815744 | tf_op jit(solution)/shard_map/half_step/pallas_call | solution.py:124
  142.3 4.2 %all-to-all-start.3 = ((bf16[4,4,2,64,256]{4,3,2,1,0:T(8,128)(2,1)}), bf16[4,4,2,64,256]{4,3,2,1,0:T(8,128)(2,1)S(1)}, u32[]{:S(2)}, u32[]{:S(2)}) async-start(bf16[4,4,2,64,256]{4,3,2,1,0:T(8,128)(2,1)} %half_step.2), calls=%async_computation.3 | async-start | bytes 2097152 | tf_op jit(solution)/shard_map/all_to_all | solution.py:28
  146.5 2.4 collective-permute-start.16
  149.0 3.1 %collective-permute-start.15 = (bf16[16,144,128]{2,1,0:T(8,128)(2,1)S(1)}, bf16[16,144,128]{2,1,0:T(8,128)(2,1)S(1)}, u32[]{:S(2)}, u32[]{:S(2)}) collective-permute-start(bf16[16,144,128]{2,1,0:T(8,128)(2,1)S(1)} %bitcast.61), channel_id=1, source_target_pairs={{0,4},{2,6},{4,0},{6,2},{1,5},{3,7},{5,1},{7,3},{8,12},{10,14},{12... | collective-permute-start | bytes 1769480 | tf_op jit(solution)/shard_map/ppermute | solution.py:36
  152.1 4.2 %collective-permute-start.14 = (bf16[16,144,128]{2,1,0:T(8,128)(2,1)S(1)}, bf16[16,144,128]{2,1,0:T(8,128)(2,1)S(1)}, u32[]{:S(2)}, u32[]{:S(2)}) collective-permute-start(bf16[16,144,128]{2,1,0:T(8,128)(2,1)S(1)} %bitcast.62), channel_id=1, source_target_pairs={{0,2},{2,0},{4,6},{6,4},{1,3},{3,1},{5,7},{7,5},{8,10},{10,8},{12,... | collective-permute-start | bytes 1769480 | tf_op jit(solution)/shard_map/ppermute | solution.py:36
  156.3 5.6 %all-to-all-done.3 = bf16[4,4,2,64,256]{4,3,2,1,0:T(8,128)(2,1)S(1)} async-done(((bf16[4,4,2,64,256]{4,3,2,1,0:T(8,128)(2,1)}), bf16[4,4,2,64,256]{4,3,2,1,0:T(8,128)(2,1)S(1)}, u32[]{:S(2)}, u32[]{:S(2)}) %all-to-all-start.3) | async-done | bytes 1048608 | tf_op jit(solution)/shard_map/all_to_all | solution.py:28
  162.0 3.7 %collective-permute-start.12 = (bf16[2,2,64,256]{3,2,1,0:T(8,128)(2,1)S(1)}, bf16[2,2,64,256]{3,2,1,0:T(8,128)(2,1)S(1)}, u32[]{:S(2)}, u32[]{:S(2)}) collective-permute-start(bf16[2,2,64,256]{3,2,1,0:T(8,128)(2,1)S(1)} %slice_reduce_fusion), channel_id=1, source_target_pairs={{0,64},{64,0},{128,192},{192,128},{1,65},{65,1},{129,193},{193,129... | collective-permute-start | bytes 393224 | tf_op jit(solution)/shard_map/ppermute | solution.py:36
  165.7 6.3 %collective-permute-done.12 = bf16[2,2,64,256]{3,2,1,0:T(8,128)(2,1)S(1)} collective-permute-done((bf16[2,2,64,256]{3,2,1,0:T(8,128)(2,1)S(1)}, bf16[2,2,64,256]{3,2,1,0:T(8,128)(2,1)S(1)}, u32[]{:S(2)}, u32[]{:S(2)}) %collective-permute-start.12) | collective-permute-done | bytes 131104 | tf_op jit(solution)/shard_map/ppermute | solution.py:36
  172.0 3.2 %collective-permute-start.13 = (bf16[2,64,256]{2,1,0:T(8,128)(2,1)S(1)}, bf16[2,64,256]{2,1,0:T(8,128)(2,1)S(1)}, u32[]{:S(2)}, u32[]{:S(2)}) collective-permute-start(bf16[2,64,256]{2,1,0:T(8,128)(2,1)S(1)} %fusion.5), channel_id=1, source_target_pairs={{0,128},{64,192},{128,0},{192,64},{1,129},{65,193},{129,1},{193,65... | collective-permute-start | bytes 196616 | tf_op jit(solution)/shard_map/ppermute | solution.py:36
  175.8 5.4 %serve.2 = (bf16[176,2048]{1,0:T(8,128)(2,1)}, bf16[176,2048]{1,0:T(8,128)(2,1)}, bf16[176,2048]{1,0:T(8,128)(2,1)}) custom-call(s32[3]{0:T(128)} %pad_add_fusion.at_ref, bf16[16,144,128]{2,1,0:T(8,128)(2,1)} %bitcast.71, bf16[16,144,128]{2,1,0:T(8,128)(2,1)} %collective-permute-done.5.refs_1_, bf16[16,144,128]{2,1,0:T(8,128)(2,1)} %copy-done.5, ...), custom_call_target="tpu_custom_call" | custom-call | flops 100000000 | bytes 6881280 | tf_op jit(solution)/shard_map/serve/pallas_call | solution.py:157
  181.3 2.6 collective-permute-done.13
  184.0 4.0 %collective-permute-start.17 = (bf16[2,64,256]{2,1,0:T(8,128)(2,1)S(1)}, bf16[2,64,256]{2,1,0:T(8,128)(2,1)S(1)}, u32[]{:S(2)}, u32[]{:S(2)}) collective-permute-start(bf16[2,64,256]{2,1,0:T(8,128)(2,1)S(1)} %add_convert_fusion), channel_id=1, source_target_pairs={{0,128},{64,192},{128,0},{192,64},{1,129},{65,193},{129,1},{193,65... | collective-permute-start | bytes 196616 | tf_op jit(solution)/shard_map/ppermute | solution.py:36
  188.0 6.4 %collective-permute-done.17 = bf16[2,64,256]{2,1,0:T(8,128)(2,1)S(1)} collective-permute-done((bf16[2,64,256]{2,1,0:T(8,128)(2,1)S(1)}, bf16[2,64,256]{2,1,0:T(8,128)(2,1)S(1)}, u32[]{:S(2)}, u32[]{:S(2)}) %collective-permute-start.17) | collective-permute-done | bytes 65568 | tf_op jit(solution)/shard_map/ppermute | solution.py:36
  194.4 1.9 collective-permute-start.18
  196.3 5.8 %collective-permute-done.18 = bf16[2,2,64,256]{3,2,1,0:T(8,128)(2,1)S(1)} collective-permute-done((bf16[2,2,64,256]{3,2,1,0:T(8,128)(2,1)S(1)}, bf16[2,2,64,256]{3,2,1,0:T(8,128)(2,1)S(1)}, u32[]{:S(2)}, u32[]{:S(2)}) %collective-permute-start.18) | collective-permute-done | bytes 131104 | tf_op jit(solution)/shard_map/ppermute | solution.py:36
  203.3 3.6 %all-to-all-start.4 = ((bf16[4,4,2,64,256]{4,3,2,1,0:T(8,128)(2,1)}), bf16[4,4,2,64,256]{4,3,2,1,0:T(8,128)(2,1)S(1)}, u32[]{:S(2)}, u32[]{:S(2)}) async-start(bf16[4,4,2,64,256]{4,3,2,1,0:T(8,128)(2,1)} %broadcast_in_dim.8), calls=%async_computation.4 | async-start | bytes 2097152 | tf_op jit(solution)/shard_map/all_to_all | solution.py:28
  208.8 2.4 collective-permute-start.20
  211.3 1.9 collective-permute-start.21
  213.2 2.4 collective-permute-start.22
  217.5 3.8 %all-to-all-done.4.x_ref = bf16[4,4,2,64,256]{4,3,2,1,0:T(8,128)(2,1)S(1)} async-done(((bf16[4,4,2,64,256]{4,3,2,1,0:T(8,128)(2,1)}), bf16[4,4,2,64,256]{4,3,2,1,0:T(8,128)(2,1)S(1)}, u32[]{:S(2)}, u32[]{:S(2)}) %all-to-all-start.4) | async-done | bytes 1048608 | tf_op jit(solution)/shard_map/all_to_all | solution.py:28
  222.3 8.1 %half_step.3 = bf16[4,4,2,64,256]{4,3,2,1,0:T(8,128)(2,1)} custom-call(s32[1]{0:T(128)} %bitcast.3.at_ref, bf16[4,4,2,64,256]{4,3,2,1,0:T(8,128)(2,1)} %copy-done.3, bf16[16,144,128]{2,1,0:T(8,128)(2,1)} %bitcast.64, bf16[16,144,128]{2,1,0:T(8,128)(2,1)} %copy-done.8, bf16[16,144,128]{2,1,0:T(8,128)(2,1)} %copy-done.7, bf16[16,144,128]{2,1,0:T(8,128)(2,1)} %copy-done.6, ...), custom_call_target="tpu_custom_call" | custom-call | flops 1207959552 | bytes 6815744 | tf_op jit(solution)/shard_map/half_step/pallas_call | solution.py:124
  230.4 3.5 %all-to-all-start.5 = ((bf16[4,4,2,64,256]{4,3,2,1,0:T(8,128)(2,1)}), bf16[4,4,2,64,256]{4,3,2,1,0:T(8,128)(2,1)S(1)}, u32[]{:S(2)}, u32[]{:S(2)}) async-start(bf16[4,4,2,64,256]{4,3,2,1,0:T(8,128)(2,1)} %half_step.3), calls=%async_computation.5 | async-start | bytes 2097152 | tf_op jit(solution)/shard_map/all_to_all | solution.py:28
  234.0 5.3 %serve.3 = (bf16[176,2048]{1,0:T(8,128)(2,1)}, bf16[176,2048]{1,0:T(8,128)(2,1)}, bf16[176,2048]{1,0:T(8,128)(2,1)}) custom-call(s32[3]{0:T(128)} %pad_add_fusion.at_ref, bf16[16,144,128]{2,1,0:T(8,128)(2,1)} %bitcast.65, bf16[16,144,128]{2,1,0:T(8,128)(2,1)} %copy-done.8, bf16[16,144,128]{2,1,0:T(8,128)(2,1)} %copy-done.7, bf16[16,144,128]{2,1,0:T(8,128)(2,1)} %copy-done.6, ...), custom_call_target="tpu_custom_call" | custom-call | flops 100000000 | bytes 6881280 | tf_op jit(solution)/shard_map/serve/pallas_call | solution.py:157
  239.2 8.2 %all-to-all-done.5 = bf16[4,4,2,64,256]{4,3,2,1,0:T(8,128)(2,1)S(1)} async-done(((bf16[4,4,2,64,256]{4,3,2,1,0:T(8,128)(2,1)}), bf16[4,4,2,64,256]{4,3,2,1,0:T(8,128)(2,1)S(1)}, u32[]{:S(2)}, u32[]{:S(2)}) %all-to-all-start.5) | async-done | bytes 1048608 | tf_op jit(solution)/shard_map/all_to_all | solution.py:28
  247.6 2.7 %collective-permute-start.23 = (bf16[2,2,64,256]{3,2,1,0:T(8,128)(2,1)S(1)}, bf16[2,2,64,256]{3,2,1,0:T(8,128)(2,1)S(1)}, u32[]{:S(2)}, u32[]{:S(2)}) collective-permute-start(bf16[2,2,64,256]{3,2,1,0:T(8,128)(2,1)S(1)} %slice_reduce_fusion.1), channel_id=1, source_target_pairs={{0,64},{64,0},{128,192},{192,128},{1,65},{65,1},{129,193},{193,129... | collective-permute-start | bytes 393224 | tf_op jit(solution)/shard_map/ppermute | solution.py:36
  250.4 5.3 %collective-permute-done.23 = bf16[2,2,64,256]{3,2,1,0:T(8,128)(2,1)S(1)} collective-permute-done((bf16[2,2,64,256]{3,2,1,0:T(8,128)(2,1)S(1)}, bf16[2,2,64,256]{3,2,1,0:T(8,128)(2,1)S(1)}, u32[]{:S(2)}, u32[]{:S(2)}) %collective-permute-start.23) | collective-permute-done | bytes 131104 | tf_op jit(solution)/shard_map/ppermute | solution.py:36
  255.7 5.8 %collective-permute-start.24 = (bf16[2,64,256]{2,1,0:T(8,128)(2,1)S(1)}, bf16[2,64,256]{2,1,0:T(8,128)(2,1)S(1)}, u32[]{:S(2)}, u32[]{:S(2)}) collective-permute-start(bf16[2,64,256]{2,1,0:T(8,128)(2,1)S(1)} %fusion.6), channel_id=1, source_target_pairs={{0,128},{64,192},{128,0},{192,64},{1,129},{65,193},{129,1},{193,65... | collective-permute-start | bytes 196616 | tf_op jit(solution)/shard_map/ppermute | solution.py:36
  261.5 5.1 %collective-permute-done.24 = bf16[2,64,256]{2,1,0:T(8,128)(2,1)S(1)} collective-permute-done((bf16[2,64,256]{2,1,0:T(8,128)(2,1)S(1)}, bf16[2,64,256]{2,1,0:T(8,128)(2,1)S(1)}, u32[]{:S(2)}, u32[]{:S(2)}) %collective-permute-start.24) | collective-permute-done | bytes 65568 | tf_op jit(solution)/shard_map/ppermute | solution.py:36
  266.7 1.9 collective-permute-start.25
  268.6 3.9 %collective-permute-done.25 = bf16[64,256]{1,0:T(8,128)(2,1)S(1)} collective-permute-done((bf16[64,256]{1,0:T(8,128)(2,1)S(1)}, bf16[64,256]{1,0:T(8,128)(2,1)S(1)}, u32[]{:S(2)}, u32[]{:S(2)}) %collective-permute-start.25) | collective-permute-done | bytes 32800 | tf_op jit(solution)/shard_map/ppermute | solution.py:36
  (111 shorter events, 25.4 us)
Async XLA Ops:
  1.4 21.9 %collective-permute-start = (bf16[64,256]{1,0:T(8,128)(2,1)S(1)}, bf16[64,256]{1,0:T(8,128)(2,1)S(1)}, u32[]{:S(2)}, u32[]{:S(2)}) collective-permute-start(bf16[64,256]{1,0:T(8,128)(2,1)S(1)} %broadcast_select_fusion.1), channel_id=1, source_target_pairs={{0,32},{32,0},{1,33},{33,1},{2,34},{34,2},{3,35},{35,3},{4,36},{36... | collective-permute-start | bytes 98312 | tf_op jit(solution)/shard_map/ppermute | solution.py:36
  14.5 8.8 %copy-start.18 = (bf16[512,64]{0,1:T(8,128)(2,1)S(1)}, bf16[512,64]{0,1:T(8,128)(2,1)}, u32[]{:S(2)}) copy-start(bf16[512,64]{0,1:T(8,128)(2,1)} %param.9) | copy-start | bytes 196612
  15.9 22.4 %all-to-all-start = ((bf16[16,32,264]{2,1,0:T(8,128)(2,1)}), bf16[16,32,264]{2,1,0:T(8,128)(2,1)S(1)}, u32[]{:S(2)}, u32[]{:S(2)}) async-start(bf16[16,32,264]{2,1,0:T(8,128)(2,1)} %reshape.59), calls=%async_computation | async-start | bytes 786432 | tf_op jit(solution)/shard_map/all_to_all | solution.py:28
  23.3 14.9 %copy-start.12 = (bf16[1,64,256]{2,1,0:T(8,128)(2,1)}, bf16[1,64,256]{2,1,0:T(8,128)(2,1)S(1)}, u32[]{:S(2)}) copy-start(bf16[1,64,256]{2,1,0:T(8,128)(2,1)S(1)} %get-tuple-element.118) | copy-start | bytes 98308
  23.3 14.9 %copy-start.15 = (bf16[1,64,256]{2,1,0:T(8,128)(2,1)}, bf16[1,64,256]{2,1,0:T(8,128)(2,1)S(1)}, u32[]{:S(2)}) copy-start(bf16[1,64,256]{2,1,0:T(8,128)(2,1)S(1)} %get-tuple-element.119) | copy-start | bytes 98308
  23.4 14.8 %collective-permute-start.1 = (bf16[2,64,256]{2,1,0:T(8,128)(2,1)S(1)}, bf16[2,64,256]{2,1,0:T(8,128)(2,1)S(1)}, u32[]{:S(2)}, u32[]{:S(2)}) collective-permute-start(bf16[2,64,256]{2,1,0:T(8,128)(2,1)S(1)} %get-tuple-element.121), channel_id=1, source_target_pairs={{0,128},{64,192},{128,0},{192,64},{1,129},{65,193},{129,1},{193,65... | collective-permute-start | bytes 196616 | tf_op jit(solution)/shard_map/ppermute | solution.py:36
  85.0 10.5 %collective-permute-start.2 = (bf16[8,144,128]{2,1,0:T(8,128)(2,1)S(1)}, bf16[8,144,128]{2,1,0:T(8,128)(2,1)S(1)}, u32[]{:S(2)}, u32[]{:S(2)}) collective-permute-start(bf16[8,144,128]{2,1,0:T(8,128)(2,1)S(1)} %slice.60), channel_id=1, source_target_pairs={{0,32},{32,0},{1,33},{33,1},{2,34},{34,2},{3,35},{35,3},{4,36},{36... | collective-permute-start | bytes 884744 | tf_op jit(solution)/shard_map/ppermute | solution.py:36
  95.7 26.1 %copy-start.1 = (bf16[8,2,144,128]{3,2,1,0:T(8,128)(2,1)}, bf16[8,2,144,128]{3,2,1,0:T(8,128)(2,1)S(1)}, u32[]{:S(2)}) copy-start(bf16[8,2,144,128]{3,2,1,0:T(8,128)(2,1)S(1)} %copy.26) | copy-start | bytes 1769476
  95.7 29.8 %collective-permute-start.7 = (bf16[16,144,128]{2,1,0:T(8,128)(2,1)S(1)}, bf16[16,144,128]{2,1,0:T(8,128)(2,1)S(1)}, u32[]{:S(2)}, u32[]{:S(2)}) collective-permute-start(bf16[16,144,128]{2,1,0:T(8,128)(2,1)S(1)} %bitcast.66), channel_id=1, source_target_pairs={{0,6},{2,4},{4,2},{6,0},{1,7},{3,5},{5,3},{7,1},{8,14},{10,12},{12... | collective-permute-start | bytes 1769480 | tf_op jit(solution)/shard_map/ppermute | solution.py:36
  97.6 29.8 %collective-permute-start.6 = (bf16[16,144,128]{2,1,0:T(8,128)(2,1)S(1)}, bf16[16,144,128]{2,1,0:T(8,128)(2,1)S(1)}, u32[]{:S(2)}, u32[]{:S(2)}) collective-permute-start(bf16[16,144,128]{2,1,0:T(8,128)(2,1)S(1)} %bitcast.67), channel_id=1, source_target_pairs={{0,4},{2,6},{4,0},{6,2},{1,5},{3,7},{5,1},{7,3},{8,12},{10,14},{12... | collective-permute-start | bytes 1769480 | tf_op jit(solution)/shard_map/ppermute | solution.py:36
  102.4 27.4 %collective-permute-start.5 = (bf16[16,144,128]{2,1,0:T(8,128)(2,1)S(1)}, bf16[16,144,128]{2,1,0:T(8,128)(2,1)}, u32[]{:S(2)}, u32[]{:S(2)}) collective-permute-start(bf16[16,144,128]{2,1,0:T(8,128)(2,1)S(1)} %bitcast.68), channel_id=1, source_target_pairs={{0,2},{2,0},{4,6},{6,4},{1,3},{3,1},{5,7},{7,5},{8,10},{10,8},{12,... | collective-permute-start | bytes 1769480 | tf_op jit(solution)/shard_map/ppermute | solution.py:36
  105.5 8.9 %collective-permute-start.3 = (bf16[2,2,64,256]{3,2,1,0:T(8,128)(2,1)S(1)}, bf16[2,2,64,256]{3,2,1,0:T(8,128)(2,1)S(1)}, u32[]{:S(2)}, u32[]{:S(2)}) collective-permute-start(bf16[2,2,64,256]{3,2,1,0:T(8,128)(2,1)S(1)} %pad_maximum_fusion.4), channel_id=1, source_target_pairs={{0,64},{64,0},{128,192},{192,128},{1,65},{65,1},{129,193},{193,129... | collective-permute-start | bytes 393224 | tf_op jit(solution)/shard_map/ppermute | solution.py:36
  115.6 16.5 %all-to-all-start.2 = ((bf16[4,4,2,64,256]{4,3,2,1,0:T(8,128)(2,1)}), bf16[4,4,2,64,256]{4,3,2,1,0:T(8,128)(2,1)S(1)}, u32[]{:S(2)}, u32[]{:S(2)}) async-start(bf16[4,4,2,64,256]{4,3,2,1,0:T(8,128)(2,1)} %broadcast_in_dim.7), calls=%async_computation.2 | async-start | bytes 2097152 | tf_op jit(solution)/shard_map/all_to_all | solution.py:28
  119.8 12.0 %collective-permute-start.4 = (bf16[8,144,128]{2,1,0:T(8,128)(2,1)S(1)}, bf16[8,144,128]{2,1,0:T(8,128)(2,1)S(1)}, u32[]{:S(2)}, u32[]{:S(2)}) collective-permute-start(bf16[8,144,128]{2,1,0:T(8,128)(2,1)S(1)} %get-tuple-element.62), channel_id=1, source_target_pairs={{0,32},{32,0},{1,33},{33,1},{2,34},{34,2},{3,35},{35,3},{4,36},{36... | collective-permute-start | bytes 884744 | tf_op jit(solution)/shard_map/ppermute | solution.py:36
  121.7 10.2 %collective-permute-start.8 = (bf16[16,144,128]{2,1,0:T(8,128)(2,1)S(1)}, bf16[16,144,128]{2,1,0:T(8,128)(2,1)}, u32[]{:S(2)}, u32[]{:S(2)}) collective-permute-start(bf16[16,144,128]{2,1,0:T(8,128)(2,1)S(1)} %bitcast.69), channel_id=1, source_target_pairs={{0,1},{1,0},{2,3},{3,2},{4,5},{5,4},{6,7},{7,6},{8,9},{9,8},{10,11... | collective-permute-start | bytes 1769480 | tf_op jit(solution)/shard_map/ppermute | solution.py:36
  125.5 6.4 %copy-start.4 = (bf16[16,144,128]{2,1,0:T(8,128)(2,1)}, bf16[16,144,128]{2,1,0:T(8,128)(2,1)S(1)}, u32[]{:S(2)}) copy-start(bf16[16,144,128]{2,1,0:T(8,128)(2,1)S(1)} %collective-permute-done.7.refs_3_) | copy-start | bytes 1769476
  125.5 6.5 %collective-permute-start.11 = (bf16[16,144,128]{2,1,0:T(8,128)(2,1)S(1)}, bf16[16,144,128]{2,1,0:T(8,128)(2,1)}, u32[]{:S(2)}, u32[]{:S(2)}) collective-permute-start(bf16[16,144,128]{2,1,0:T(8,128)(2,1)S(1)} %collective-permute-done.7.refs_3_), channel_id=1, source_target_pairs={{0,1},{1,0},{2,3},{3,2},{4,5},{5,4},{6,7},{7,6},{8,9},{9,8},{10,11... | collective-permute-start | bytes 1769480 | tf_op jit(solution)/shard_map/ppermute | solution.py:36
  127.4 4.5 %copy-start.5 = (bf16[16,144,128]{2,1,0:T(8,128)(2,1)}, bf16[16,144,128]{2,1,0:T(8,128)(2,1)S(1)}, u32[]{:S(2)}) copy-start(bf16[16,144,128]{2,1,0:T(8,128)(2,1)S(1)} %collective-permute-done.6.refs_2_) | copy-start | bytes 1769476
  127.5 4.6 %collective-permute-start.10 = (bf16[16,144,128]{2,1,0:T(8,128)(2,1)S(1)}, bf16[16,144,128]{2,1,0:T(8,128)(2,1)}, u32[]{:S(2)}, u32[]{:S(2)}) collective-permute-start(bf16[16,144,128]{2,1,0:T(8,128)(2,1)S(1)} %collective-permute-done.6.refs_2_), channel_id=1, source_target_pairs={{0,1},{1,0},{2,3},{3,2},{4,5},{5,4},{6,7},{7,6},{8,9},{9,8},{10,11... | collective-permute-start | bytes 1769480 | tf_op jit(solution)/shard_map/ppermute | solution.py:36
  129.9 4.2 %collective-permute-start.9 = (bf16[16,144,128]{2,1,0:T(8,128)(2,1)}, bf16[16,144,128]{2,1,0:T(8,128)(2,1)}, u32[]{:S(2)}, u32[]{:S(2)}) collective-permute-start(bf16[16,144,128]{2,1,0:T(8,128)(2,1)} %collective-permute-done.5.refs_1_), channel_id=1, source_target_pairs={{0,1},{1,0},{2,3},{3,2},{4,5},{5,4},{6,7},{7,6},{8,9},{9,8},{10,11... | collective-permute-start | bytes 1769480 | tf_op jit(solution)/shard_map/ppermute | solution.py:36
  132.0 75.0 %copy-start = (bf16[8,2,144,128]{3,2,1,0:T(8,128)(2,1)}, bf16[8,2,144,128]{3,2,1,0:T(8,128)(2,1)S(1)}, u32[]{:S(2)}) copy-start(bf16[8,2,144,128]{3,2,1,0:T(8,128)(2,1)S(1)} %pad_maximum_fusion.1) | copy-start | bytes 1769476
  132.0 2.1 copy-start.2
  142.3 19.6 %all-to-all-start.3 = ((bf16[4,4,2,64,256]{4,3,2,1,0:T(8,128)(2,1)}), bf16[4,4,2,64,256]{4,3,2,1,0:T(8,128)(2,1)S(1)}, u32[]{:S(2)}, u32[]{:S(2)}) async-start(bf16[4,4,2,64,256]{4,3,2,1,0:T(8,128)(2,1)} %half_step.2), calls=%async_computation.3 | async-start | bytes 2097152 | tf_op jit(solution)/shard_map/all_to_all | solution.py:28
  146.5 37.4 %collective-permute-start.16 = (bf16[16,144,128]{2,1,0:T(8,128)(2,1)S(1)}, bf16[16,144,128]{2,1,0:T(8,128)(2,1)S(1)}, u32[]{:S(2)}, u32[]{:S(2)}) collective-permute-start(bf16[16,144,128]{2,1,0:T(8,128)(2,1)S(1)} %bitcast.60), channel_id=1, source_target_pairs={{0,6},{2,4},{4,2},{6,0},{1,7},{3,5},{5,3},{7,1},{8,14},{10,12},{12... | collective-permute-start | bytes 1769480 | tf_op jit(solution)/shard_map/ppermute | solution.py:36
  149.0 34.9 %collective-permute-start.15 = (bf16[16,144,128]{2,1,0:T(8,128)(2,1)S(1)}, bf16[16,144,128]{2,1,0:T(8,128)(2,1)S(1)}, u32[]{:S(2)}, u32[]{:S(2)}) collective-permute-start(bf16[16,144,128]{2,1,0:T(8,128)(2,1)S(1)} %bitcast.61), channel_id=1, source_target_pairs={{0,4},{2,6},{4,0},{6,2},{1,5},{3,7},{5,1},{7,3},{8,12},{10,14},{12... | collective-permute-start | bytes 1769480 | tf_op jit(solution)/shard_map/ppermute | solution.py:36
  152.1 31.8 %collective-permute-start.14 = (bf16[16,144,128]{2,1,0:T(8,128)(2,1)S(1)}, bf16[16,144,128]{2,1,0:T(8,128)(2,1)S(1)}, u32[]{:S(2)}, u32[]{:S(2)}) collective-permute-start(bf16[16,144,128]{2,1,0:T(8,128)(2,1)S(1)} %bitcast.62), channel_id=1, source_target_pairs={{0,2},{2,0},{4,6},{6,4},{1,3},{3,1},{5,7},{7,5},{8,10},{10,8},{12,... | collective-permute-start | bytes 1769480 | tf_op jit(solution)/shard_map/ppermute | solution.py:36
  162.0 10.0 %collective-permute-start.12 = (bf16[2,2,64,256]{3,2,1,0:T(8,128)(2,1)S(1)}, bf16[2,2,64,256]{3,2,1,0:T(8,128)(2,1)S(1)}, u32[]{:S(2)}, u32[]{:S(2)}) collective-permute-start(bf16[2,2,64,256]{3,2,1,0:T(8,128)(2,1)S(1)} %slice_reduce_fusion), channel_id=1, source_target_pairs={{0,64},{64,0},{128,192},{192,128},{1,65},{65,1},{129,193},{193,129... | collective-permute-start | bytes 393224 | tf_op jit(solution)/shard_map/ppermute | solution.py:36
  172.0 11.8 %collective-permute-start.13 = (bf16[2,64,256]{2,1,0:T(8,128)(2,1)S(1)}, bf16[2,64,256]{2,1,0:T(8,128)(2,1)S(1)}, u32[]{:S(2)}, u32[]{:S(2)}) collective-permute-start(bf16[2,64,256]{2,1,0:T(8,128)(2,1)S(1)} %fusion.5), channel_id=1, source_target_pairs={{0,128},{64,192},{128,0},{192,64},{1,129},{65,193},{129,1},{193,65... | collective-permute-start | bytes 196616 | tf_op jit(solution)/shard_map/ppermute | solution.py:36
  175.8 8.1 %copy-start.13 = (bf16[1,64,256]{2,1,0:T(8,128)(2,1)S(1)}, bf16[1,64,256]{2,1,0:T(8,128)(2,1)}, u32[]{:S(2)}) copy-start(bf16[1,64,256]{2,1,0:T(8,128)(2,1)} %copy-done.12) | copy-start | bytes 98308
  175.8 8.1 %copy-start.16 = (bf16[1,64,256]{2,1,0:T(8,128)(2,1)S(1)}, bf16[1,64,256]{2,1,0:T(8,128)(2,1)}, u32[]{:S(2)}) copy-start(bf16[1,64,256]{2,1,0:T(8,128)(2,1)} %copy-done.15) | copy-start | bytes 98308
  183.9 29.3 %copy-start.6 = (bf16[16,144,128]{2,1,0:T(8,128)(2,1)}, bf16[16,144,128]{2,1,0:T(8,128)(2,1)S(1)}, u32[]{:S(2)}) copy-start(bf16[16,144,128]{2,1,0:T(8,128)(2,1)S(1)} %collective-permute-done.16.refs_3_) | copy-start | bytes 1769476
  183.9 27.4 %copy-start.7 = (bf16[16,144,128]{2,1,0:T(8,128)(2,1)}, bf16[16,144,128]{2,1,0:T(8,128)(2,1)S(1)}, u32[]{:S(2)}) copy-start(bf16[16,144,128]{2,1,0:T(8,128)(2,1)S(1)} %collective-permute-done.15.refs_2_) | copy-start | bytes 1769476
  183.9 24.9 %copy-start.8 = (bf16[16,144,128]{2,1,0:T(8,128)(2,1)}, bf16[16,144,128]{2,1,0:T(8,128)(2,1)S(1)}, u32[]{:S(2)}) copy-start(bf16[16,144,128]{2,1,0:T(8,128)(2,1)S(1)} %collective-permute-done.14.refs_1_) | copy-start | bytes 1769476
  184.0 10.4 %collective-permute-start.17 = (bf16[2,64,256]{2,1,0:T(8,128)(2,1)S(1)}, bf16[2,64,256]{2,1,0:T(8,128)(2,1)S(1)}, u32[]{:S(2)}, u32[]{:S(2)}) collective-permute-start(bf16[2,64,256]{2,1,0:T(8,128)(2,1)S(1)} %add_convert_fusion), channel_id=1, source_target_pairs={{0,128},{64,192},{128,0},{192,64},{1,129},{65,193},{129,1},{193,65... | collective-permute-start | bytes 196616 | tf_op jit(solution)/shard_map/ppermute | solution.py:36
  194.4 7.8 %collective-permute-start.18 = (bf16[2,2,64,256]{3,2,1,0:T(8,128)(2,1)S(1)}, bf16[2,2,64,256]{3,2,1,0:T(8,128)(2,1)S(1)}, u32[]{:S(2)}, u32[]{:S(2)}) collective-permute-start(bf16[2,2,64,256]{3,2,1,0:T(8,128)(2,1)S(1)} %pad_maximum_fusion.5), channel_id=1, source_target_pairs={{0,64},{64,0},{128,192},{192,128},{1,65},{65,1},{129,193},{193,129... | collective-permute-start | bytes 393224 | tf_op jit(solution)/shard_map/ppermute | solution.py:36
  203.3 18.0 %all-to-all-start.4 = ((bf16[4,4,2,64,256]{4,3,2,1,0:T(8,128)(2,1)}), bf16[4,4,2,64,256]{4,3,2,1,0:T(8,128)(2,1)S(1)}, u32[]{:S(2)}, u32[]{:S(2)}) async-start(bf16[4,4,2,64,256]{4,3,2,1,0:T(8,128)(2,1)} %broadcast_in_dim.8), calls=%async_computation.4 | async-start | bytes 2097152 | tf_op jit(solution)/shard_map/all_to_all | solution.py:28
  206.9 8.7 %collective-permute-start.19 = (bf16[16,144,128]{2,1,0:T(8,128)(2,1)S(1)}, bf16[16,144,128]{2,1,0:T(8,128)(2,1)S(1)}, u32[]{:S(2)}, u32[]{:S(2)}) collective-permute-start(bf16[16,144,128]{2,1,0:T(8,128)(2,1)S(1)} %bitcast.63), channel_id=1, source_target_pairs={{0,1},{1,0},{2,3},{3,2},{4,5},{5,4},{6,7},{7,6},{8,9},{9,8},{10,11... | collective-permute-start | bytes 1769480 | tf_op jit(solution)/shard_map/ppermute | solution.py:36
  208.8 6.8 %collective-permute-start.20 = (bf16[16,144,128]{2,1,0:T(8,128)(2,1)S(1)}, bf16[16,144,128]{2,1,0:T(8,128)(2,1)S(1)}, u32[]{:S(2)}, u32[]{:S(2)}) collective-permute-start(bf16[16,144,128]{2,1,0:T(8,128)(2,1)S(1)} %collective-permute-done.14.refs_1_), channel_id=1, source_target_pairs={{0,1},{1,0},{2,3},{3,2},{4,5},{5,4},{6,7},{7,6},{8,9},{9,8},{10,11... | collective-permute-start | bytes 1769480 | tf_op jit(solution)/shard_map/ppermute | solution.py:36
  211.3 4.4 %collective-permute-start.21 = (bf16[16,144,128]{2,1,0:T(8,128)(2,1)S(1)}, bf16[16,144,128]{2,1,0:T(8,128)(2,1)S(1)}, u32[]{:S(2)}, u32[]{:S(2)}) collective-permute-start(bf16[16,144,128]{2,1,0:T(8,128)(2,1)S(1)} %collective-permute-done.15.refs_2_), channel_id=1, source_target_pairs={{0,1},{1,0},{2,3},{3,2},{4,5},{5,4},{6,7},{7,6},{8,9},{9,8},{10,11... | collective-permute-start | bytes 1769480 | tf_op jit(solution)/shard_map/ppermute | solution.py:36
  213.2 4.3 %collective-permute-start.22 = (bf16[16,144,128]{2,1,0:T(8,128)(2,1)S(1)}, bf16[16,144,128]{2,1,0:T(8,128)(2,1)}, u32[]{:S(2)}, u32[]{:S(2)}) collective-permute-start(bf16[16,144,128]{2,1,0:T(8,128)(2,1)S(1)} %collective-permute-done.16.refs_3_), channel_id=1, source_target_pairs={{0,1},{1,0},{2,3},{3,2},{4,5},{5,4},{6,7},{7,6},{8,9},{9,8},{10,11... | collective-permute-start | bytes 1769480 | tf_op jit(solution)/shard_map/ppermute | solution.py:36
  215.7 1.0 copy-start.10
  221.3 1.0 copy-start.3
  230.4 17.0 %all-to-all-start.5 = ((bf16[4,4,2,64,256]{4,3,2,1,0:T(8,128)(2,1)}), bf16[4,4,2,64,256]{4,3,2,1,0:T(8,128)(2,1)S(1)}, u32[]{:S(2)}, u32[]{:S(2)}) async-start(bf16[4,4,2,64,256]{4,3,2,1,0:T(8,128)(2,1)} %half_step.3), calls=%async_computation.5 | async-start | bytes 2097152 | tf_op jit(solution)/shard_map/all_to_all | solution.py:28
  247.5 19.1 %copy-start.14 = (bf16[1,64,256]{2,1,0:T(8,128)(2,1)S(1)}, bf16[1,64,256]{2,1,0:T(8,128)(2,1)}, u32[]{:S(2)}) copy-start(bf16[1,64,256]{2,1,0:T(8,128)(2,1)} %copy-done.12) | copy-start | bytes 98308
  247.5 19.1 %copy-start.17 = (bf16[1,64,256]{2,1,0:T(8,128)(2,1)S(1)}, bf16[1,64,256]{2,1,0:T(8,128)(2,1)}, u32[]{:S(2)}) copy-start(bf16[1,64,256]{2,1,0:T(8,128)(2,1)} %copy-done.15) | copy-start | bytes 98308
  247.6 8.1 %collective-permute-start.23 = (bf16[2,2,64,256]{3,2,1,0:T(8,128)(2,1)S(1)}, bf16[2,2,64,256]{3,2,1,0:T(8,128)(2,1)S(1)}, u32[]{:S(2)}, u32[]{:S(2)}) collective-permute-start(bf16[2,2,64,256]{3,2,1,0:T(8,128)(2,1)S(1)} %slice_reduce_fusion.1), channel_id=1, source_target_pairs={{0,64},{64,0},{128,192},{192,128},{1,65},{65,1},{129,193},{193,129... | collective-permute-start | bytes 393224 | tf_op jit(solution)/shard_map/ppermute | solution.py:36
  255.7 10.9 %collective-permute-start.24 = (bf16[2,64,256]{2,1,0:T(8,128)(2,1)S(1)}, bf16[2,64,256]{2,1,0:T(8,128)(2,1)S(1)}, u32[]{:S(2)}, u32[]{:S(2)}) collective-permute-start(bf16[2,64,256]{2,1,0:T(8,128)(2,1)S(1)} %fusion.6), channel_id=1, source_target_pairs={{0,128},{64,192},{128,0},{192,64},{1,129},{65,193},{129,1},{193,65... | collective-permute-start | bytes 196616 | tf_op jit(solution)/shard_map/ppermute | solution.py:36
  266.7 5.8 %collective-permute-start.25 = (bf16[64,256]{1,0:T(8,128)(2,1)S(1)}, bf16[64,256]{1,0:T(8,128)(2,1)S(1)}, u32[]{:S(2)}, u32[]{:S(2)}) collective-permute-start(bf16[64,256]{1,0:T(8,128)(2,1)S(1)} %select_bitcast_fusion.4), channel_id=1, source_target_pairs={{0,32},{32,0},{1,33},{33,1},{2,34},{34,2},{3,35},{35,3},{4,36},{36... | collective-permute-start | bytes 98312 | tf_op jit(solution)/shard_map/ppermute | solution.py:36
  (2 other events, 1.7 us)

commit v2 on v1

--- a/solution.py
+++ b/solution.py
@@ -40,13 +40,37 @@
     return lax.optimization_barrier((value, *others))[0]
 
 
-def by_block(layers):
-    cols = jnp.stack([matrix for matrices in layers for matrix in matrices])
-    n = cols.shape[0]
-    to_yx = cols.reshape(n, ROWS, Y * X, PART).transpose(2, 1, 0, 3).reshape(Y * X, ROWS, n * PART)
-    here = swap(to_yx, ("y", "x")).reshape(Y, X, ROWS, n * PART)
-    turned = here.transpose(1, 3, 0, 2).reshape(X, n, PART, LANES)
-    return jnp.pad(turned, ((0, 0), (0, 0), (0, PADDED - PART), (0, 0))).reshape(X, n * PADDED, LANES)
+def pack_kernel(gain_ref, gate_ref, up_ref, down_ref, gain2_ref, gate2_ref, up2_ref, down2_ref, out_ref, row_ref):
+    sources = (
+        (gain_ref, gate_ref), (gain_ref, up_ref), (None, down_ref),
+        (gain2_ref, gate2_ref), (gain2_ref, up2_ref), (None, down2_ref),
+    )
+    for peer in range(Y * X):
+        for n, (gain, ref) in enumerate(sources):
+            cols = ref[:, peer * PART : (peer + 1) * PART]
+            row_ref[:, n * PART : (n + 1) * PART] = cols if gain is None else gain[...] * cols
+        out_ref[peer] = row_ref[...].astype(BF16)
+
+
+def packed(layers):
+    arrays = [a for gain, *matrices in layers for a in (gain[:, None], *matrices)]
+    vmem = pl.BlockSpec(memory_space=pltpu.VMEM)
+    width = 3 * len(layers) * PART
+    return pl.pallas_call(
+        pack_kernel,
+        out_shape=jax.ShapeDtypeStruct((Y * X, ROWS, width), BF16),
+        in_specs=[vmem] * len(arrays),
+        out_specs=vmem,
+        scratch_shapes=[pltpu.VMEM((ROWS, width), F32)],
+        cost_estimate=pl.CostEstimate(flops=10**6, bytes_accessed=10**6, transcendentals=0),
+        name="pack",
+    )(*arrays)
+
+
+def by_block(to_yx):
+    here = swap(to_yx, ("y", "x")).reshape(Y, X, ROWS, -1)
+    turned = here.transpose(1, 3, 0, 2).reshape(X, -1, PART, LANES)
+    return jnp.pad(turned, ((0, 0), (0, 0), (0, PADDED - PART), (0, 0))).reshape(X, -1, LANES)
 
 
 def by_span(parts):
@@ -90,15 +114,16 @@
     acc_ref[...] = jnp.zeros_like(acc_ref)
     sq_ref[...] = jnp.zeros_like(sq_ref)
 
-    def inward(zl, _):
-        k, b = slot(zl, zq)
-        tokens = x_ref[:, k, b].reshape(Y * FEATS, width)
+    def inward(z, _):
+        k, _ = slot(z * B, zq)
+        tokens = jnp.concatenate([x_ref[:, k, b].reshape(Y * FEATS, width) for b in range(B)], axis=0)
         wide = tokens.astype(F32)
-        sq_ref[...] += jnp.sum((wide * wide).reshape(Y * FEATS // 8, 8, width), axis=0)
-        acc_ref[...] += jnp.dot(both(zl, 0, 2 * PADDED), tokens, preferred_element_type=F32)
+        sq_ref[...] += jnp.sum((wide * wide).reshape(B * Y * FEATS // 8, 8, width), axis=0)
+        weights = jnp.concatenate([both(z * B + b, 0, 2 * PADDED) for b in range(B)], axis=1)
+        acc_ref[...] += jnp.dot(weights, tokens, preferred_element_type=F32)
         return 0
 
-    lax.fori_loop(0, ZL, inward, 0)
+    lax.fori_loop(0, ZQ, inward, 0)
     squares = jnp.sum(sq_ref[...], axis=0, keepdims=True)
     scale = lax.rsqrt(squares / D + NORM_EPS) * D ** (-0.5)
     sums = acc_ref[...].reshape(pieces, 2 * PADDED, width)
@@ -205,17 +230,15 @@
     half = prompt.shape[0] // B
     turned = prompt.T
     parts = by_block(
-        [
-            ((gain_pre[:, None] * gate_pre).astype(BF16), (gain_pre[:, None] * up_pre).astype(BF16), down_pre.astype(BF16)),
-            ((gain_post[:, None] * gate_post).astype(BF16), (gain_post[:, None] * up_post).astype(BF16), down_post.astype(BF16)),
-        ]
+        packed([(gain_pre, gate_pre, up_pre, down_pre), (gain_post, gate_post, up_post, down_post)])
     )
     tokens = jnp.stack(traded(turned[:, :half], turned[:, half:]))
     parts, wide = lax.optimization_barrier((parts, far_zq(tokens)))
     one, two = by_span(parts)
+    wide = after(wide, one)
     one = paired(one)
+    wide = near_zq(wide)
     pieces = over_x(one)
-    wide = near_zq(after(wide, one))
     wide = share(wide, "y", Y)
     two = paired(after(two, one))
     pieces += over_core(pieces)

time: 276 us -> 273 us (0.989)
  Pallas kernels: 26.9 us -> 31.7 us
  local copies, waits for them, and re-layouts: 13.5 us -> 9.53 us
  other arithmetic: 6.74 us -> 2.82 us
    pallas_call x0 -> x1, Pallas kernels: none -> 6.04 us  [packed(): pl.pallas_call(pack_kernel, out_shape=jax.ShapeDtypeStruct((Y * X, ROWS,...]
    another operation x13 -> x0, local copies, waits for them, and re-layouts: 5.27 us -> none  [by_block(): cols = jnp.stack([matrix for matrices in layers for matrix in matrices])]
    convert_element_type x4 -> x0, other arithmetic: 3.88 us -> none  [the longest x1 1.04 us: local(): (gain_pre[:, None] * up_pre).astype(BF16)]
  transfers between devices with their start and end apart: 31 -> 31, of which waited for: 15 -> 15; matrix products, arithmetic and copies ran while one was open for 5% -> 2% of each run, Pallas kernels for 4% -> 6%
where the time goes in v2:
time: 273 us; the launch traced here: 270 us
  starting transfers between devices  102 us (37%)
  waiting for transfers between devices  77.2 us (28%)
  blocking collectives  45 us (16%)
  Pallas kernels  31.7 us (12%)
  local copies, waits for them, and re-layouts  9.53 us (3%)
  other arithmetic  2.82 us (1%)
    ppermute x26, starting transfers between devices, from_peer(): return lax.ppermute(block, axis, [(i, i ^ flip) for i in range(size)])  79.4 us
    ppermute x26, waiting for transfers between devices, from_peer(): return lax.ppermute(block, axis, [(i, i ^ flip) for i in range(size)])  59.5 us
    all_to_all x1, blocking collectives, swap(): return lax.all_to_all(blocks, axis, split_axis=0, concat_axis=0, tiled=True)  45 us
    all_to_all x5, starting transfers between devices, swap(): return lax.all_to_all(blocks, axis, split_axis=0, concat_axis=0, tiled=True)  23 us
    all_to_all x5, waiting for transfers between devices, swap(): return lax.all_to_all(blocks, axis, split_axis=0, concat_axis=0, tiled=True)  17.7 us
    pallas_call x2, Pallas kernels, half_partial(): pl.pallas_call(half_kernel, out_shape=jax.ShapeDtypeStruct(tokens.shape,...  14.9 us
    pallas_call x2, Pallas kernels, served(): pl.pallas_call(serve_kernel, out_shape=[jax.ShapeDtypeStruct((BLOCK, D),...  10.7 us
    pallas_call x1, Pallas kernels, packed(): pl.pallas_call(pack_kernel, out_shape=jax.ShapeDtypeStruct((Y * X, ROWS,...  6.04 us
  transfers between devices with their start and end apart: 31, of which 15 were waited for; matrix products, arithmetic and copies ran while one was open for 2% of the time, Pallas kernels for 6%

profile of v2, /device:TPU:6, one launch (start us, length us, event | category | flops | bytes accessed | tf_op | source)
XLA Modules:
  0.0 270.0 jit_solution(3458908630652582671)
XLA Ops:
  1.5 3.8 %collective-permute-start = (bf16[64,256]{1,0:T(8,128)(2,1)S(1)}, bf16[64,256]{1,0:T(8,128)(2,1)S(1)}, u32[]{:S(2)}, u32[]{:S(2)}) collective-permute-start(bf16[64,256]{1,0:T(8,128)(2,1)S(1)} %broadcast_select_fusion.1), channel_id=1, source_target_pairs={{0,32},{32,0},{1,33},{33,1},{2,34},{34,2},{3,35},{35,3},{4,36},{36... | collective-permute-start | bytes 98312 | tf_op jit(solution)/shard_map/ppermute | solution.py:36
  8.0 6.0 %pack.1 = bf16[16,32,264]{2,1,0:T(8,128)(2,1)} custom-call(f32[32,1]{1,0:T(8,128)} %copy.20.gain_ref, f32[32,704]{1,0:T(8,128)} %gate_ref.1, f32[32,704]{1,0:T(8,128)} %up_ref.1, f32[32,704]{1,0:T(8,128)} %down_ref.1, f32[32,1]{1,0:T(8,128)} %copy.21.gain2_ref, f32[32,704]{1,0:T(8,128)} %gate2_ref.1, f32[32,704]{1,0:T(8,128)} %up2_ref.1, f32[32,704]{1,0:T(8,128)} %down2_ref.1), custom_call_target="tpu_custom_call" | custom-call | flops 1000000 | bytes 1000000 | tf_op jit(solution)/shard_map/pack/pallas_call | solution.py:59
  14.0 7.4 %all-to-all-start = ((bf16[16,32,264]{2,1,0:T(8,128)(2,1)}), bf16[16,32,264]{2,1,0:T(8,128)(2,1)S(1)}, u32[]{:S(2)}, u32[]{:S(2)}) async-start(bf16[16,32,264]{2,1,0:T(8,128)(2,1)} %pack.1), calls=%async_computation | async-start | bytes 786432 | tf_op jit(solution)/shard_map/all_to_all | solution.py:28
  21.5 9.1 %collective-permute-start.1 = (bf16[2,64,256]{2,1,0:T(8,128)(2,1)S(1)}, bf16[2,64,256]{2,1,0:T(8,128)(2,1)S(1)}, u32[]{:S(2)}, u32[]{:S(2)}) collective-permute-start(bf16[2,64,256]{2,1,0:T(8,128)(2,1)S(1)} %get-tuple-element.121), channel_id=1, source_target_pairs={{0,128},{64,192},{128,0},{192,64},{1,129},{65,193},{129,1},{193,65... | collective-permute-start | bytes 196616 | tf_op jit(solution)/shard_map/ppermute | solution.py:36
  30.6 5.7 %collective-permute-done.1 = bf16[2,64,256]{2,1,0:T(8,128)(2,1)S(1)} collective-permute-done((bf16[2,64,256]{2,1,0:T(8,128)(2,1)S(1)}, bf16[2,64,256]{2,1,0:T(8,128)(2,1)S(1)}, u32[]{:S(2)}, u32[]{:S(2)}) %collective-permute-start.1) | collective-permute-done | bytes 65568 | tf_op jit(solution)/shard_map/ppermute | solution.py:36
  38.1 45.0 %all_to_all.30 = bf16[8,288,128]{2,1,0:T(8,128)(2,1)S(1)} all-to-all(bf16[8,288,128]{2,1,0:T(8,128)(2,1)S(1)} %bitcast.73), channel_id=1, replica_groups=mesh['gr'=2,'zq'=4,'b'=2,'y'=4,'x'=4,'core'=2] {'gr','zq'}, dimensions={0} | all-to-all | bytes 1179648 | tf_op jit(solution)/shard_map/all_to_all | solution.py:28
  83.1 2.4 collective-permute-start.3
  85.5 8.1 %collective-permute-done.3 = bf16[8,144,128]{2,1,0:T(8,128)(2,1)S(1)} collective-permute-done((bf16[8,144,128]{2,1,0:T(8,128)(2,1)S(1)}, bf16[8,144,128]{2,1,0:T(8,128)(2,1)S(1)}, u32[]{:S(2)}, u32[]{:S(2)}) %collective-permute-start.3) | collective-permute-done | bytes 294944 | tf_op jit(solution)/shard_map/ppermute | solution.py:36
  93.8 1.9 collective-permute-start.7
  95.8 4.8 %collective-permute-start.6 = (bf16[16,144,128]{2,1,0:T(8,128)(2,1)S(1)}, bf16[16,144,128]{2,1,0:T(8,128)(2,1)S(1)}, u32[]{:S(2)}, u32[]{:S(2)}) collective-permute-start(bf16[16,144,128]{2,1,0:T(8,128)(2,1)S(1)} %bitcast.67), channel_id=1, source_target_pairs={{0,4},{2,6},{4,0},{6,2},{1,5},{3,7},{5,1},{7,3},{8,12},{10,14},{12... | collective-permute-start | bytes 1769480 | tf_op jit(solution)/shard_map/ppermute | solution.py:36
  100.6 3.1 %collective-permute-start.5 = (bf16[16,144,128]{2,1,0:T(8,128)(2,1)S(1)}, bf16[16,144,128]{2,1,0:T(8,128)(2,1)}, u32[]{:S(2)}, u32[]{:S(2)}) collective-permute-start(bf16[16,144,128]{2,1,0:T(8,128)(2,1)S(1)} %bitcast.68), channel_id=1, source_target_pairs={{0,2},{2,0},{4,6},{6,4},{1,3},{3,1},{5,7},{7,5},{8,10},{10,8},{12,... | collective-permute-start | bytes 1769480 | tf_op jit(solution)/shard_map/ppermute | solution.py:36
  103.7 3.9 %collective-permute-start.2 = (bf16[2,2,64,256]{3,2,1,0:T(8,128)(2,1)S(1)}, bf16[2,2,64,256]{3,2,1,0:T(8,128)(2,1)S(1)}, u32[]{:S(2)}, u32[]{:S(2)}) collective-permute-start(bf16[2,2,64,256]{3,2,1,0:T(8,128)(2,1)S(1)} %pad_maximum_fusion.4), channel_id=1, source_target_pairs={{0,64},{64,0},{128,192},{192,128},{1,65},{65,1},{129,193},{193,129... | collective-permute-start | bytes 393224 | tf_op jit(solution)/shard_map/ppermute | solution.py:36
  107.6 5.0 %collective-permute-done.2 = bf16[2,2,64,256]{3,2,1,0:T(8,128)(2,1)S(1)} collective-permute-done((bf16[2,2,64,256]{3,2,1,0:T(8,128)(2,1)S(1)}, bf16[2,2,64,256]{3,2,1,0:T(8,128)(2,1)S(1)}, u32[]{:S(2)}, u32[]{:S(2)}) %collective-permute-start.2) | collective-permute-done | bytes 131104 | tf_op jit(solution)/shard_map/ppermute | solution.py:36
  113.7 4.2 %all-to-all-start.2 = ((bf16[4,4,2,64,256]{4,3,2,1,0:T(8,128)(2,1)}), bf16[4,4,2,64,256]{4,3,2,1,0:T(8,128)(2,1)S(1)}, u32[]{:S(2)}, u32[]{:S(2)}) async-start(bf16[4,4,2,64,256]{4,3,2,1,0:T(8,128)(2,1)} %broadcast_in_dim.13), calls=%async_computation.2 | async-start | bytes 2097152 | tf_op jit(solution)/shard_map/all_to_all | solution.py:28
  119.9 1.9 collective-permute-start.8
  125.6 2.4 collective-permute-start.10
  128.0 1.9 collective-permute-start.9
  130.2 2.1 collective-permute-done.9.refs_5_
  132.3 7.5 %half_step.2 = bf16[4,4,2,64,256]{4,3,2,1,0:T(8,128)(2,1)} custom-call(s32[1]{0:T(128)} %bitcast.3.at_ref, bf16[4,4,2,64,256]{4,3,2,1,0:T(8,128)(2,1)} %copy-done.2, bf16[16,144,128]{2,1,0:T(8,128)(2,1)} %bitcast.70, bf16[16,144,128]{2,1,0:T(8,128)(2,1)} %collective-permute-done.5.refs_1_, bf16[16,144,128]{2,1,0:T(8,128)(2,1)} %copy-done.5, ...), custom_call_target="tpu_custom_call" | custom-call | flops 1207959552 | bytes 6815744 | tf_op jit(solution)/shard_map/half_step/pallas_call | solution.py:149
  139.7 4.3 %all-to-all-start.3 = ((bf16[4,4,2,64,256]{4,3,2,1,0:T(8,128)(2,1)}), bf16[4,4,2,64,256]{4,3,2,1,0:T(8,128)(2,1)S(1)}, u32[]{:S(2)}, u32[]{:S(2)}) async-start(bf16[4,4,2,64,256]{4,3,2,1,0:T(8,128)(2,1)} %half_step.2), calls=%async_computation.3 | async-start | bytes 2097152 | tf_op jit(solution)/shard_map/all_to_all | solution.py:28
  144.0 2.5 collective-permute-start.16
  146.5 3.1 %collective-permute-start.15 = (bf16[16,144,128]{2,1,0:T(8,128)(2,1)S(1)}, bf16[16,144,128]{2,1,0:T(8,128)(2,1)S(1)}, u32[]{:S(2)}, u32[]{:S(2)}) collective-permute-start(bf16[16,144,128]{2,1,0:T(8,128)(2,1)S(1)} %bitcast.61), channel_id=1, source_target_pairs={{0,4},{2,6},{4,0},{6,2},{1,5},{3,7},{5,1},{7,3},{8,12},{10,14},{12... | collective-permute-start | bytes 1769480 | tf_op jit(solution)/shard_map/ppermute | solution.py:36
  149.6 4.2 %collective-permute-start.14 = (bf16[16,144,128]{2,1,0:T(8,128)(2,1)S(1)}, bf16[16,144,128]{2,1,0:T(8,128)(2,1)S(1)}, u32[]{:S(2)}, u32[]{:S(2)}) collective-permute-start(bf16[16,144,128]{2,1,0:T(8,128)(2,1)S(1)} %bitcast.62), channel_id=1, source_target_pairs={{0,2},{2,0},{4,6},{6,4},{1,3},{3,1},{5,7},{7,5},{8,10},{10,8},{12,... | collective-permute-start | bytes 1769480 | tf_op jit(solution)/shard_map/ppermute | solution.py:36
  153.8 5.6 %all-to-all-done.3 = bf16[4,4,2,64,256]{4,3,2,1,0:T(8,128)(2,1)S(1)} async-done(((bf16[4,4,2,64,256]{4,3,2,1,0:T(8,128)(2,1)}), bf16[4,4,2,64,256]{4,3,2,1,0:T(8,128)(2,1)S(1)}, u32[]{:S(2)}, u32[]{:S(2)}) %all-to-all-start.3) | async-done | bytes 1048608 | tf_op jit(solution)/shard_map/all_to_all | solution.py:28
  159.5 3.7 %collective-permute-start.12 = (bf16[2,2,64,256]{3,2,1,0:T(8,128)(2,1)S(1)}, bf16[2,2,64,256]{3,2,1,0:T(8,128)(2,1)S(1)}, u32[]{:S(2)}, u32[]{:S(2)}) collective-permute-start(bf16[2,2,64,256]{3,2,1,0:T(8,128)(2,1)S(1)} %slice_reduce_fusion), channel_id=1, source_target_pairs={{0,64},{64,0},{128,192},{192,128},{1,65},{65,1},{129,193},{193,129... | collective-permute-start | bytes 393224 | tf_op jit(solution)/shard_map/ppermute | solution.py:36
  163.2 6.2 %collective-permute-done.12 = bf16[2,2,64,256]{3,2,1,0:T(8,128)(2,1)S(1)} collective-permute-done((bf16[2,2,64,256]{3,2,1,0:T(8,128)(2,1)S(1)}, bf16[2,2,64,256]{3,2,1,0:T(8,128)(2,1)S(1)}, u32[]{:S(2)}, u32[]{:S(2)}) %collective-permute-start.12) | collective-permute-done | bytes 131104 | tf_op jit(solution)/shard_map/ppermute | solution.py:36
  169.5 3.1 %collective-permute-start.13 = (bf16[2,64,256]{2,1,0:T(8,128)(2,1)S(1)}, bf16[2,64,256]{2,1,0:T(8,128)(2,1)S(1)}, u32[]{:S(2)}, u32[]{:S(2)}) collective-permute-start(bf16[2,64,256]{2,1,0:T(8,128)(2,1)S(1)} %fusion.5), channel_id=1, source_target_pairs={{0,128},{64,192},{128,0},{192,64},{1,129},{65,193},{129,1},{193,65... | collective-permute-start | bytes 196616 | tf_op jit(solution)/shard_map/ppermute | solution.py:36
  173.2 5.4 %serve.2 = (bf16[176,2048]{1,0:T(8,128)(2,1)}, bf16[176,2048]{1,0:T(8,128)(2,1)}, bf16[176,2048]{1,0:T(8,128)(2,1)}) custom-call(s32[3]{0:T(128)} %pad_add_fusion.at_ref, bf16[16,144,128]{2,1,0:T(8,128)(2,1)} %bitcast.71, bf16[16,144,128]{2,1,0:T(8,128)(2,1)} %collective-permute-done.5.refs_1_, bf16[16,144,128]{2,1,0:T(8,128)(2,1)} %copy-done.5, ...), custom_call_target="tpu_custom_call" | custom-call | flops 100000000 | bytes 6881280 | tf_op jit(solution)/shard_map/serve/pallas_call | solution.py:182
  178.6 2.7 %collective-permute-done.13 = bf16[2,64,256]{2,1,0:T(8,128)(2,1)S(1)} collective-permute-done((bf16[2,64,256]{2,1,0:T(8,128)(2,1)S(1)}, bf16[2,64,256]{2,1,0:T(8,128)(2,1)S(1)}, u32[]{:S(2)}, u32[]{:S(2)}) %collective-permute-start.13) | collective-permute-done | bytes 65568 | tf_op jit(solution)/shard_map/ppermute | solution.py:36
  181.5 3.9 %collective-permute-start.17 = (bf16[2,64,256]{2,1,0:T(8,128)(2,1)S(1)}, bf16[2,64,256]{2,1,0:T(8,128)(2,1)S(1)}, u32[]{:S(2)}, u32[]{:S(2)}) collective-permute-start(bf16[2,64,256]{2,1,0:T(8,128)(2,1)S(1)} %add_convert_fusion), channel_id=1, source_target_pairs={{0,128},{64,192},{128,0},{192,64},{1,129},{65,193},{129,1},{193,65... | collective-permute-start | bytes 196616 | tf_op jit(solution)/shard_map/ppermute | solution.py:36
  185.4 6.5 %collective-permute-done.17 = bf16[2,64,256]{2,1,0:T(8,128)(2,1)S(1)} collective-permute-done((bf16[2,64,256]{2,1,0:T(8,128)(2,1)S(1)}, bf16[2,64,256]{2,1,0:T(8,128)(2,1)S(1)}, u32[]{:S(2)}, u32[]{:S(2)}) %collective-permute-start.17) | collective-permute-done | bytes 65568 | tf_op jit(solution)/shard_map/ppermute | solution.py:36
  191.9 1.9 collective-permute-start.18
  193.8 5.8 %collective-permute-done.18 = bf16[2,2,64,256]{3,2,1,0:T(8,128)(2,1)S(1)} collective-permute-done((bf16[2,2,64,256]{3,2,1,0:T(8,128)(2,1)S(1)}, bf16[2,2,64,256]{3,2,1,0:T(8,128)(2,1)S(1)}, u32[]{:S(2)}, u32[]{:S(2)}) %collective-permute-start.18) | collective-permute-done | bytes 131104 | tf_op jit(solution)/shard_map/ppermute | solution.py:36
  200.8 3.6 %all-to-all-start.4 = ((bf16[4,4,2,64,256]{4,3,2,1,0:T(8,128)(2,1)}), bf16[4,4,2,64,256]{4,3,2,1,0:T(8,128)(2,1)S(1)}, u32[]{:S(2)}, u32[]{:S(2)}) async-start(bf16[4,4,2,64,256]{4,3,2,1,0:T(8,128)(2,1)} %broadcast_in_dim.28), calls=%async_computation.4 | async-start | bytes 2097152 | tf_op jit(solution)/shard_map/all_to_all | solution.py:28
  206.3 2.4 collective-permute-start.20
  208.7 1.9 collective-permute-start.21
  210.7 2.4 collective-permute-start.22
  215.0 3.8 %all-to-all-done.4.x_ref = bf16[4,4,2,64,256]{4,3,2,1,0:T(8,128)(2,1)S(1)} async-done(((bf16[4,4,2,64,256]{4,3,2,1,0:T(8,128)(2,1)}), bf16[4,4,2,64,256]{4,3,2,1,0:T(8,128)(2,1)S(1)}, u32[]{:S(2)}, u32[]{:S(2)}) %all-to-all-start.4) | async-done | bytes 1048608 | tf_op jit(solution)/shard_map/all_to_all | solution.py:28
  219.8 7.5 %half_step.3 = bf16[4,4,2,64,256]{4,3,2,1,0:T(8,128)(2,1)} custom-call(s32[1]{0:T(128)} %bitcast.3.at_ref, bf16[4,4,2,64,256]{4,3,2,1,0:T(8,128)(2,1)} %copy-done.3, bf16[16,144,128]{2,1,0:T(8,128)(2,1)} %bitcast.64, bf16[16,144,128]{2,1,0:T(8,128)(2,1)} %copy-done.8, bf16[16,144,128]{2,1,0:T(8,128)(2,1)} %copy-done.7, bf16[16,144,128]{2,1,0:T(8,128)(2,1)} %copy-done.6, ...), custom_call_target="tpu_custom_call" | custom-call | flops 1207959552 | bytes 6815744 | tf_op jit(solution)/shard_map/half_step/pallas_call | solution.py:149
  227.3 3.5 %all-to-all-start.5 = ((bf16[4,4,2,64,256]{4,3,2,1,0:T(8,128)(2,1)}), bf16[4,4,2,64,256]{4,3,2,1,0:T(8,128)(2,1)S(1)}, u32[]{:S(2)}, u32[]{:S(2)}) async-start(bf16[4,4,2,64,256]{4,3,2,1,0:T(8,128)(2,1)} %half_step.3), calls=%async_computation.5 | async-start | bytes 2097152 | tf_op jit(solution)/shard_map/all_to_all | solution.py:28
  230.8 5.3 %serve.3 = (bf16[176,2048]{1,0:T(8,128)(2,1)}, bf16[176,2048]{1,0:T(8,128)(2,1)}, bf16[176,2048]{1,0:T(8,128)(2,1)}) custom-call(s32[3]{0:T(128)} %pad_add_fusion.at_ref, bf16[16,144,128]{2,1,0:T(8,128)(2,1)} %bitcast.65, bf16[16,144,128]{2,1,0:T(8,128)(2,1)} %copy-done.8, bf16[16,144,128]{2,1,0:T(8,128)(2,1)} %copy-done.7, bf16[16,144,128]{2,1,0:T(8,128)(2,1)} %copy-done.6, ...), custom_call_target="tpu_custom_call" | custom-call | flops 100000000 | bytes 6881280 | tf_op jit(solution)/shard_map/serve/pallas_call | solution.py:182
  236.1 8.3 %all-to-all-done.5 = bf16[4,4,2,64,256]{4,3,2,1,0:T(8,128)(2,1)S(1)} async-done(((bf16[4,4,2,64,256]{4,3,2,1,0:T(8,128)(2,1)}), bf16[4,4,2,64,256]{4,3,2,1,0:T(8,128)(2,1)S(1)}, u32[]{:S(2)}, u32[]{:S(2)}) %all-to-all-start.5) | async-done | bytes 1048608 | tf_op jit(solution)/shard_map/all_to_all | solution.py:28
  244.4 2.7 %collective-permute-start.23 = (bf16[2,2,64,256]{3,2,1,0:T(8,128)(2,1)S(1)}, bf16[2,2,64,256]{3,2,1,0:T(8,128)(2,1)S(1)}, u32[]{:S(2)}, u32[]{:S(2)}) collective-permute-start(bf16[2,2,64,256]{3,2,1,0:T(8,128)(2,1)S(1)} %slice_reduce_fusion.1), channel_id=1, source_target_pairs={{0,64},{64,0},{128,192},{192,128},{1,65},{65,1},{129,193},{193,129... | collective-permute-start | bytes 393224 | tf_op jit(solution)/shard_map/ppermute | solution.py:36
  247.2 5.3 %collective-permute-done.23 = bf16[2,2,64,256]{3,2,1,0:T(8,128)(2,1)S(1)} collective-permute-done((bf16[2,2,64,256]{3,2,1,0:T(8,128)(2,1)S(1)}, bf16[2,2,64,256]{3,2,1,0:T(8,128)(2,1)S(1)}, u32[]{:S(2)}, u32[]{:S(2)}) %collective-permute-start.23) | collective-permute-done | bytes 131104 | tf_op jit(solution)/shard_map/ppermute | solution.py:36
  252.6 4.5 %collective-permute-start.24 = (bf16[2,64,256]{2,1,0:T(8,128)(2,1)S(1)}, bf16[2,64,256]{2,1,0:T(8,128)(2,1)S(1)}, u32[]{:S(2)}, u32[]{:S(2)}) collective-permute-start(bf16[2,64,256]{2,1,0:T(8,128)(2,1)S(1)} %fusion.6), channel_id=1, source_target_pairs={{0,128},{64,192},{128,0},{192,64},{1,129},{65,193},{129,1},{193,65... | collective-permute-start | bytes 196616 | tf_op jit(solution)/shard_map/ppermute | solution.py:36
  257.1 6.4 %collective-permute-done.24 = bf16[2,64,256]{2,1,0:T(8,128)(2,1)S(1)} collective-permute-done((bf16[2,64,256]{2,1,0:T(8,128)(2,1)S(1)}, bf16[2,64,256]{2,1,0:T(8,128)(2,1)S(1)}, u32[]{:S(2)}, u32[]{:S(2)}) %collective-permute-start.24) | collective-permute-done | bytes 65568 | tf_op jit(solution)/shard_map/ppermute | solution.py:36
  263.5 1.9 collective-permute-start.25
  265.4 3.9 %collective-permute-done.25 = bf16[64,256]{1,0:T(8,128)(2,1)S(1)} collective-permute-done((bf16[64,256]{1,0:T(8,128)(2,1)S(1)}, bf16[64,256]{1,0:T(8,128)(2,1)S(1)}, u32[]{:S(2)}, u32[]{:S(2)}) %collective-permute-start.25) | collective-permute-done | bytes 32800 | tf_op jit(solution)/shard_map/ppermute | solution.py:36
  (96 shorter events, 20.0 us)
Async XLA Ops:
  0.6 20.8 %copy-start.18 = (bf16[512,64]{0,1:T(8,128)(2,1)S(1)}, bf16[512,64]{0,1:T(8,128)(2,1)}, u32[]{:S(2)}) copy-start(bf16[512,64]{0,1:T(8,128)(2,1)} %param.9) | copy-start | bytes 196612
  1.5 20.0 %collective-permute-start = (bf16[64,256]{1,0:T(8,128)(2,1)S(1)}, bf16[64,256]{1,0:T(8,128)(2,1)S(1)}, u32[]{:S(2)}, u32[]{:S(2)}) collective-permute-start(bf16[64,256]{1,0:T(8,128)(2,1)S(1)} %broadcast_select_fusion.1), channel_id=1, source_target_pairs={{0,32},{32,0},{1,33},{33,1},{2,34},{34,2},{3,35},{35,3},{4,36},{36... | collective-permute-start | bytes 98312 | tf_op jit(solution)/shard_map/ppermute | solution.py:36
  14.0 22.4 %all-to-all-start = ((bf16[16,32,264]{2,1,0:T(8,128)(2,1)}), bf16[16,32,264]{2,1,0:T(8,128)(2,1)S(1)}, u32[]{:S(2)}, u32[]{:S(2)}) async-start(bf16[16,32,264]{2,1,0:T(8,128)(2,1)} %pack.1), calls=%async_computation | async-start | bytes 786432 | tf_op jit(solution)/shard_map/all_to_all | solution.py:28
  21.5 14.9 %copy-start.12 = (bf16[1,64,256]{2,1,0:T(8,128)(2,1)}, bf16[1,64,256]{2,1,0:T(8,128)(2,1)S(1)}, u32[]{:S(2)}) copy-start(bf16[1,64,256]{2,1,0:T(8,128)(2,1)S(1)} %get-tuple-element.118) | copy-start | bytes 98308
  21.5 14.9 %copy-start.15 = (bf16[1,64,256]{2,1,0:T(8,128)(2,1)}, bf16[1,64,256]{2,1,0:T(8,128)(2,1)S(1)}, u32[]{:S(2)}) copy-start(bf16[1,64,256]{2,1,0:T(8,128)(2,1)S(1)} %get-tuple-element.119) | copy-start | bytes 98308
  21.5 14.8 %collective-permute-start.1 = (bf16[2,64,256]{2,1,0:T(8,128)(2,1)S(1)}, bf16[2,64,256]{2,1,0:T(8,128)(2,1)S(1)}, u32[]{:S(2)}, u32[]{:S(2)}) collective-permute-start(bf16[2,64,256]{2,1,0:T(8,128)(2,1)S(1)} %get-tuple-element.121), channel_id=1, source_target_pairs={{0,128},{64,192},{128,0},{192,64},{1,129},{65,193},{129,1},{193,65... | collective-permute-start | bytes 196616 | tf_op jit(solution)/shard_map/ppermute | solution.py:36
  83.1 10.5 %collective-permute-start.3 = (bf16[8,144,128]{2,1,0:T(8,128)(2,1)S(1)}, bf16[8,144,128]{2,1,0:T(8,128)(2,1)S(1)}, u32[]{:S(2)}, u32[]{:S(2)}) collective-permute-start(bf16[8,144,128]{2,1,0:T(8,128)(2,1)S(1)} %slice.60), channel_id=1, source_target_pairs={{0,32},{32,0},{1,33},{33,1},{2,34},{34,2},{3,35},{35,3},{4,36},{36... | collective-permute-start | bytes 884744 | tf_op jit(solution)/shard_map/ppermute | solution.py:36
  93.8 26.1 %copy-start.1 = (bf16[8,2,144,128]{3,2,1,0:T(8,128)(2,1)}, bf16[8,2,144,128]{3,2,1,0:T(8,128)(2,1)S(1)}, u32[]{:S(2)}) copy-start(bf16[8,2,144,128]{3,2,1,0:T(8,128)(2,1)S(1)} %copy.24) | copy-start | bytes 1769476
  93.8 29.8 %collective-permute-start.7 = (bf16[16,144,128]{2,1,0:T(8,128)(2,1)S(1)}, bf16[16,144,128]{2,1,0:T(8,128)(2,1)S(1)}, u32[]{:S(2)}, u32[]{:S(2)}) collective-permute-start(bf16[16,144,128]{2,1,0:T(8,128)(2,1)S(1)} %bitcast.66), channel_id=1, source_target_pairs={{0,6},{2,4},{4,2},{6,0},{1,7},{3,5},{5,3},{7,1},{8,14},{10,12},{12... | collective-permute-start | bytes 1769480 | tf_op jit(solution)/shard_map/ppermute | solution.py:36
  95.8 29.8 %collective-permute-start.6 = (bf16[16,144,128]{2,1,0:T(8,128)(2,1)S(1)}, bf16[16,144,128]{2,1,0:T(8,128)(2,1)S(1)}, u32[]{:S(2)}, u32[]{:S(2)}) collective-permute-start(bf16[16,144,128]{2,1,0:T(8,128)(2,1)S(1)} %bitcast.67), channel_id=1, source_target_pairs={{0,4},{2,6},{4,0},{6,2},{1,5},{3,7},{5,1},{7,3},{8,12},{10,14},{12... | collective-permute-start | bytes 1769480 | tf_op jit(solution)/shard_map/ppermute | solution.py:36
  100.6 27.4 %collective-permute-start.5 = (bf16[16,144,128]{2,1,0:T(8,128)(2,1)S(1)}, bf16[16,144,128]{2,1,0:T(8,128)(2,1)}, u32[]{:S(2)}, u32[]{:S(2)}) collective-permute-start(bf16[16,144,128]{2,1,0:T(8,128)(2,1)S(1)} %bitcast.68), channel_id=1, source_target_pairs={{0,2},{2,0},{4,6},{6,4},{1,3},{3,1},{5,7},{7,5},{8,10},{10,8},{12,... | collective-permute-start | bytes 1769480 | tf_op jit(solution)/shard_map/ppermute | solution.py:36
  103.7 8.9 %collective-permute-start.2 = (bf16[2,2,64,256]{3,2,1,0:T(8,128)(2,1)S(1)}, bf16[2,2,64,256]{3,2,1,0:T(8,128)(2,1)S(1)}, u32[]{:S(2)}, u32[]{:S(2)}) collective-permute-start(bf16[2,2,64,256]{3,2,1,0:T(8,128)(2,1)S(1)} %pad_maximum_fusion.4), channel_id=1, source_target_pairs={{0,64},{64,0},{128,192},{192,128},{1,65},{65,1},{129,193},{193,129... | collective-permute-start | bytes 393224 | tf_op jit(solution)/shard_map/ppermute | solution.py:36
  113.7 16.5 %all-to-all-start.2 = ((bf16[4,4,2,64,256]{4,3,2,1,0:T(8,128)(2,1)}), bf16[4,4,2,64,256]{4,3,2,1,0:T(8,128)(2,1)S(1)}, u32[]{:S(2)}, u32[]{:S(2)}) async-start(bf16[4,4,2,64,256]{4,3,2,1,0:T(8,128)(2,1)} %broadcast_in_dim.13), calls=%async_computation.2 | async-start | bytes 2097152 | tf_op jit(solution)/shard_map/all_to_all | solution.py:28
  117.9 12.0 %collective-permute-start.4 = (bf16[8,144,128]{2,1,0:T(8,128)(2,1)S(1)}, bf16[8,144,128]{2,1,0:T(8,128)(2,1)S(1)}, u32[]{:S(2)}, u32[]{:S(2)}) collective-permute-start(bf16[8,144,128]{2,1,0:T(8,128)(2,1)S(1)} %get-tuple-element.62), channel_id=1, source_target_pairs={{0,32},{32,0},{1,33},{33,1},{2,34},{34,2},{3,35},{35,3},{4,36},{36... | collective-permute-start | bytes 884744 | tf_op jit(solution)/shard_map/ppermute | solution.py:36
  119.9 10.3 %collective-permute-start.8 = (bf16[16,144,128]{2,1,0:T(8,128)(2,1)S(1)}, bf16[16,144,128]{2,1,0:T(8,128)(2,1)}, u32[]{:S(2)}, u32[]{:S(2)}) collective-permute-start(bf16[16,144,128]{2,1,0:T(8,128)(2,1)S(1)} %bitcast.69), channel_id=1, source_target_pairs={{0,1},{1,0},{2,3},{3,2},{4,5},{5,4},{6,7},{7,6},{8,9},{9,8},{10,11... | collective-permute-start | bytes 1769480 | tf_op jit(solution)/shard_map/ppermute | solution.py:36
  123.7 6.4 %copy-start.4 = (bf16[16,144,128]{2,1,0:T(8,128)(2,1)}, bf16[16,144,128]{2,1,0:T(8,128)(2,1)S(1)}, u32[]{:S(2)}) copy-start(bf16[16,144,128]{2,1,0:T(8,128)(2,1)S(1)} %collective-permute-done.7.refs_3_) | copy-start | bytes 1769476
  123.7 6.5 %collective-permute-start.11 = (bf16[16,144,128]{2,1,0:T(8,128)(2,1)S(1)}, bf16[16,144,128]{2,1,0:T(8,128)(2,1)}, u32[]{:S(2)}, u32[]{:S(2)}) collective-permute-start(bf16[16,144,128]{2,1,0:T(8,128)(2,1)S(1)} %collective-permute-done.7.refs_3_), channel_id=1, source_target_pairs={{0,1},{1,0},{2,3},{3,2},{4,5},{5,4},{6,7},{7,6},{8,9},{9,8},{10,11... | collective-permute-start | bytes 1769480 | tf_op jit(solution)/shard_map/ppermute | solution.py:36
  125.6 4.5 %copy-start.5 = (bf16[16,144,128]{2,1,0:T(8,128)(2,1)}, bf16[16,144,128]{2,1,0:T(8,128)(2,1)S(1)}, u32[]{:S(2)}) copy-start(bf16[16,144,128]{2,1,0:T(8,128)(2,1)S(1)} %collective-permute-done.6.refs_2_) | copy-start | bytes 1769476
  125.6 4.6 %collective-permute-start.10 = (bf16[16,144,128]{2,1,0:T(8,128)(2,1)S(1)}, bf16[16,144,128]{2,1,0:T(8,128)(2,1)}, u32[]{:S(2)}, u32[]{:S(2)}) collective-permute-start(bf16[16,144,128]{2,1,0:T(8,128)(2,1)S(1)} %collective-permute-done.6.refs_2_), channel_id=1, source_target_pairs={{0,1},{1,0},{2,3},{3,2},{4,5},{5,4},{6,7},{7,6},{8,9},{9,8},{10,11... | collective-permute-start | bytes 1769480 | tf_op jit(solution)/shard_map/ppermute | solution.py:36
  128.0 4.2 %collective-permute-start.9 = (bf16[16,144,128]{2,1,0:T(8,128)(2,1)}, bf16[16,144,128]{2,1,0:T(8,128)(2,1)}, u32[]{:S(2)}, u32[]{:S(2)}) collective-permute-start(bf16[16,144,128]{2,1,0:T(8,128)(2,1)} %collective-permute-done.5.refs_1_), channel_id=1, source_target_pairs={{0,1},{1,0},{2,3},{3,2},{4,5},{5,4},{6,7},{7,6},{8,9},{9,8},{10,11... | collective-permute-start | bytes 1769480 | tf_op jit(solution)/shard_map/ppermute | solution.py:36
  130.1 74.3 %copy-start = (bf16[8,2,144,128]{3,2,1,0:T(8,128)(2,1)}, bf16[8,2,144,128]{3,2,1,0:T(8,128)(2,1)S(1)}, u32[]{:S(2)}) copy-start(bf16[8,2,144,128]{3,2,1,0:T(8,128)(2,1)S(1)} %pad_maximum_fusion.1) | copy-start | bytes 1769476
  130.2 2.1 copy-start.2
  139.7 19.6 %all-to-all-start.3 = ((bf16[4,4,2,64,256]{4,3,2,1,0:T(8,128)(2,1)}), bf16[4,4,2,64,256]{4,3,2,1,0:T(8,128)(2,1)S(1)}, u32[]{:S(2)}, u32[]{:S(2)}) async-start(bf16[4,4,2,64,256]{4,3,2,1,0:T(8,128)(2,1)} %half_step.2), calls=%async_computation.3 | async-start | bytes 2097152 | tf_op jit(solution)/shard_map/all_to_all | solution.py:28
  144.0 37.4 %collective-permute-start.16 = (bf16[16,144,128]{2,1,0:T(8,128)(2,1)S(1)}, bf16[16,144,128]{2,1,0:T(8,128)(2,1)S(1)}, u32[]{:S(2)}, u32[]{:S(2)}) collective-permute-start(bf16[16,144,128]{2,1,0:T(8,128)(2,1)S(1)} %bitcast.60), channel_id=1, source_target_pairs={{0,6},{2,4},{4,2},{6,0},{1,7},{3,5},{5,3},{7,1},{8,14},{10,12},{12... | collective-permute-start | bytes 1769480 | tf_op jit(solution)/shard_map/ppermute | solution.py:36
  146.5 34.9 %collective-permute-start.15 = (bf16[16,144,128]{2,1,0:T(8,128)(2,1)S(1)}, bf16[16,144,128]{2,1,0:T(8,128)(2,1)S(1)}, u32[]{:S(2)}, u32[]{:S(2)}) collective-permute-start(bf16[16,144,128]{2,1,0:T(8,128)(2,1)S(1)} %bitcast.61), channel_id=1, source_target_pairs={{0,4},{2,6},{4,0},{6,2},{1,5},{3,7},{5,1},{7,3},{8,12},{10,14},{12... | collective-permute-start | bytes 1769480 | tf_op jit(solution)/shard_map/ppermute | solution.py:36
  149.6 31.8 %collective-permute-start.14 = (bf16[16,144,128]{2,1,0:T(8,128)(2,1)S(1)}, bf16[16,144,128]{2,1,0:T(8,128)(2,1)S(1)}, u32[]{:S(2)}, u32[]{:S(2)}) collective-permute-start(bf16[16,144,128]{2,1,0:T(8,128)(2,1)S(1)} %bitcast.62), channel_id=1, source_target_pairs={{0,2},{2,0},{4,6},{6,4},{1,3},{3,1},{5,7},{7,5},{8,10},{10,8},{12,... | collective-permute-start | bytes 1769480 | tf_op jit(solution)/shard_map/ppermute | solution.py:36
  159.5 10.0 %collective-permute-start.12 = (bf16[2,2,64,256]{3,2,1,0:T(8,128)(2,1)S(1)}, bf16[2,2,64,256]{3,2,1,0:T(8,128)(2,1)S(1)}, u32[]{:S(2)}, u32[]{:S(2)}) collective-permute-start(bf16[2,2,64,256]{3,2,1,0:T(8,128)(2,1)S(1)} %slice_reduce_fusion), channel_id=1, source_target_pairs={{0,64},{64,0},{128,192},{192,128},{1,65},{65,1},{129,193},{193,129... | collective-permute-start | bytes 393224 | tf_op jit(solution)/shard_map/ppermute | solution.py:36
  169.5 11.9 %collective-permute-start.13 = (bf16[2,64,256]{2,1,0:T(8,128)(2,1)S(1)}, bf16[2,64,256]{2,1,0:T(8,128)(2,1)S(1)}, u32[]{:S(2)}, u32[]{:S(2)}) collective-permute-start(bf16[2,64,256]{2,1,0:T(8,128)(2,1)S(1)} %fusion.5), channel_id=1, source_target_pairs={{0,128},{64,192},{128,0},{192,64},{1,129},{65,193},{129,1},{193,65... | collective-permute-start | bytes 196616 | tf_op jit(solution)/shard_map/ppermute | solution.py:36
  173.2 8.2 %copy-start.13 = (bf16[1,64,256]{2,1,0:T(8,128)(2,1)S(1)}, bf16[1,64,256]{2,1,0:T(8,128)(2,1)}, u32[]{:S(2)}) copy-start(bf16[1,64,256]{2,1,0:T(8,128)(2,1)} %copy-done.12) | copy-start | bytes 98308
  173.2 8.2 %copy-start.16 = (bf16[1,64,256]{2,1,0:T(8,128)(2,1)S(1)}, bf16[1,64,256]{2,1,0:T(8,128)(2,1)}, u32[]{:S(2)}) copy-start(bf16[1,64,256]{2,1,0:T(8,128)(2,1)} %copy-done.15) | copy-start | bytes 98308
  181.4 29.3 %copy-start.6 = (bf16[16,144,128]{2,1,0:T(8,128)(2,1)}, bf16[16,144,128]{2,1,0:T(8,128)(2,1)S(1)}, u32[]{:S(2)}) copy-start(bf16[16,144,128]{2,1,0:T(8,128)(2,1)S(1)} %collective-permute-done.16.refs_3_) | copy-start | bytes 1769476
  181.4 27.3 %copy-start.7 = (bf16[16,144,128]{2,1,0:T(8,128)(2,1)}, bf16[16,144,128]{2,1,0:T(8,128)(2,1)S(1)}, u32[]{:S(2)}) copy-start(bf16[16,144,128]{2,1,0:T(8,128)(2,1)S(1)} %collective-permute-done.15.refs_2_) | copy-start | bytes 1769476
  181.4 24.9 %copy-start.8 = (bf16[16,144,128]{2,1,0:T(8,128)(2,1)}, bf16[16,144,128]{2,1,0:T(8,128)(2,1)S(1)}, u32[]{:S(2)}) copy-start(bf16[16,144,128]{2,1,0:T(8,128)(2,1)S(1)} %collective-permute-done.14.refs_1_) | copy-start | bytes 1769476
  181.5 10.4 %collective-permute-start.17 = (bf16[2,64,256]{2,1,0:T(8,128)(2,1)S(1)}, bf16[2,64,256]{2,1,0:T(8,128)(2,1)S(1)}, u32[]{:S(2)}, u32[]{:S(2)}) collective-permute-start(bf16[2,64,256]{2,1,0:T(8,128)(2,1)S(1)} %add_convert_fusion), channel_id=1, source_target_pairs={{0,128},{64,192},{128,0},{192,64},{1,129},{65,193},{129,1},{193,65... | collective-permute-start | bytes 196616 | tf_op jit(solution)/shard_map/ppermute | solution.py:36
  191.9 7.8 %collective-permute-start.18 = (bf16[2,2,64,256]{3,2,1,0:T(8,128)(2,1)S(1)}, bf16[2,2,64,256]{3,2,1,0:T(8,128)(2,1)S(1)}, u32[]{:S(2)}, u32[]{:S(2)}) collective-permute-start(bf16[2,2,64,256]{3,2,1,0:T(8,128)(2,1)S(1)} %pad_maximum_fusion.5), channel_id=1, source_target_pairs={{0,64},{64,0},{128,192},{192,128},{1,65},{65,1},{129,193},{193,129... | collective-permute-start | bytes 393224 | tf_op jit(solution)/shard_map/ppermute | solution.py:36
  200.8 18.0 %all-to-all-start.4 = ((bf16[4,4,2,64,256]{4,3,2,1,0:T(8,128)(2,1)}), bf16[4,4,2,64,256]{4,3,2,1,0:T(8,128)(2,1)S(1)}, u32[]{:S(2)}, u32[]{:S(2)}) async-start(bf16[4,4,2,64,256]{4,3,2,1,0:T(8,128)(2,1)} %broadcast_in_dim.28), calls=%async_computation.4 | async-start | bytes 2097152 | tf_op jit(solution)/shard_map/all_to_all | solution.py:28
  204.4 8.7 %collective-permute-start.19 = (bf16[16,144,128]{2,1,0:T(8,128)(2,1)S(1)}, bf16[16,144,128]{2,1,0:T(8,128)(2,1)S(1)}, u32[]{:S(2)}, u32[]{:S(2)}) collective-permute-start(bf16[16,144,128]{2,1,0:T(8,128)(2,1)S(1)} %bitcast.63), channel_id=1, source_target_pairs={{0,1},{1,0},{2,3},{3,2},{4,5},{5,4},{6,7},{7,6},{8,9},{9,8},{10,11... | collective-permute-start | bytes 1769480 | tf_op jit(solution)/shard_map/ppermute | solution.py:36
  206.3 6.8 %collective-permute-start.20 = (bf16[16,144,128]{2,1,0:T(8,128)(2,1)S(1)}, bf16[16,144,128]{2,1,0:T(8,128)(2,1)S(1)}, u32[]{:S(2)}, u32[]{:S(2)}) collective-permute-start(bf16[16,144,128]{2,1,0:T(8,128)(2,1)S(1)} %collective-permute-done.14.refs_1_), channel_id=1, source_target_pairs={{0,1},{1,0},{2,3},{3,2},{4,5},{5,4},{6,7},{7,6},{8,9},{9,8},{10,11... | collective-permute-start | bytes 1769480 | tf_op jit(solution)/shard_map/ppermute | solution.py:36
  208.7 4.4 %collective-permute-start.21 = (bf16[16,144,128]{2,1,0:T(8,128)(2,1)S(1)}, bf16[16,144,128]{2,1,0:T(8,128)(2,1)S(1)}, u32[]{:S(2)}, u32[]{:S(2)}) collective-permute-start(bf16[16,144,128]{2,1,0:T(8,128)(2,1)S(1)} %collective-permute-done.15.refs_2_), channel_id=1, source_target_pairs={{0,1},{1,0},{2,3},{3,2},{4,5},{5,4},{6,7},{7,6},{8,9},{9,8},{10,11... | collective-permute-start | bytes 1769480 | tf_op jit(solution)/shard_map/ppermute | solution.py:36
  210.7 4.3 %collective-permute-start.22 = (bf16[16,144,128]{2,1,0:T(8,128)(2,1)S(1)}, bf16[16,144,128]{2,1,0:T(8,128)(2,1)}, u32[]{:S(2)}, u32[]{:S(2)}) collective-permute-start(bf16[16,144,128]{2,1,0:T(8,128)(2,1)S(1)} %collective-permute-done.16.refs_3_), channel_id=1, source_target_pairs={{0,1},{1,0},{2,3},{3,2},{4,5},{5,4},{6,7},{7,6},{8,9},{9,8},{10,11... | collective-permute-start | bytes 1769480 | tf_op jit(solution)/shard_map/ppermute | solution.py:36
  213.1 1.0 copy-start.10
  218.8 1.0 copy-start.3
  227.3 17.1 %all-to-all-start.5 = ((bf16[4,4,2,64,256]{4,3,2,1,0:T(8,128)(2,1)}), bf16[4,4,2,64,256]{4,3,2,1,0:T(8,128)(2,1)S(1)}, u32[]{:S(2)}, u32[]{:S(2)}) async-start(bf16[4,4,2,64,256]{4,3,2,1,0:T(8,128)(2,1)} %half_step.3), calls=%async_computation.5 | async-start | bytes 2097152 | tf_op jit(solution)/shard_map/all_to_all | solution.py:28
  244.3 19.1 %copy-start.14 = (bf16[1,64,256]{2,1,0:T(8,128)(2,1)S(1)}, bf16[1,64,256]{2,1,0:T(8,128)(2,1)}, u32[]{:S(2)}) copy-start(bf16[1,64,256]{2,1,0:T(8,128)(2,1)} %copy-done.12) | copy-start | bytes 98308
  244.3 19.1 %copy-start.17 = (bf16[1,64,256]{2,1,0:T(8,128)(2,1)S(1)}, bf16[1,64,256]{2,1,0:T(8,128)(2,1)}, u32[]{:S(2)}) copy-start(bf16[1,64,256]{2,1,0:T(8,128)(2,1)} %copy-done.15) | copy-start | bytes 98308
  244.4 8.1 %collective-permute-start.23 = (bf16[2,2,64,256]{3,2,1,0:T(8,128)(2,1)S(1)}, bf16[2,2,64,256]{3,2,1,0:T(8,128)(2,1)S(1)}, u32[]{:S(2)}, u32[]{:S(2)}) collective-permute-start(bf16[2,2,64,256]{3,2,1,0:T(8,128)(2,1)S(1)} %slice_reduce_fusion.1), channel_id=1, source_target_pairs={{0,64},{64,0},{128,192},{192,128},{1,65},{65,1},{129,193},{193,129... | collective-permute-start | bytes 393224 | tf_op jit(solution)/shard_map/ppermute | solution.py:36
  252.6 10.9 %collective-permute-start.24 = (bf16[2,64,256]{2,1,0:T(8,128)(2,1)S(1)}, bf16[2,64,256]{2,1,0:T(8,128)(2,1)S(1)}, u32[]{:S(2)}, u32[]{:S(2)}) collective-permute-start(bf16[2,64,256]{2,1,0:T(8,128)(2,1)S(1)} %fusion.6), channel_id=1, source_target_pairs={{0,128},{64,192},{128,0},{192,64},{1,129},{65,193},{129,1},{193,65... | collective-permute-start | bytes 196616 | tf_op jit(solution)/shard_map/ppermute | solution.py:36
  263.5 5.8 %collective-permute-start.25 = (bf16[64,256]{1,0:T(8,128)(2,1)S(1)}, bf16[64,256]{1,0:T(8,128)(2,1)S(1)}, u32[]{:S(2)}, u32[]{:S(2)}) collective-permute-start(bf16[64,256]{1,0:T(8,128)(2,1)S(1)} %select_bitcast_fusion.4), channel_id=1, source_target_pairs={{0,32},{32,0},{1,33},{33,1},{2,34},{34,2},{3,35},{35,3},{4,36},{36... | collective-permute-start | bytes 98312 | tf_op jit(solution)/shard_map/ppermute | solution.py:36
  (2 other events, 1.6 us)

commit v3 on v2

--- a/solution.py
+++ b/solution.py
@@ -22,6 +22,8 @@
 PIECE = 3 * PADDED
 FEATS = D // (ZL * Y)
 AT_ONCE = 4
+BUFFERS = 4
+MIB = 2**20
 
 
 def swap(blocks, axis):
@@ -45,15 +47,23 @@
         (gain_ref, gate_ref), (gain_ref, up_ref), (None, down_ref),
         (gain2_ref, gate2_ref), (gain2_ref, up2_ref), (None, down2_ref),
     )
+    shape = (ROWS, ROWS)
+    diagonal = lax.broadcasted_iota(jnp.int32, shape, 0) == lax.broadcasted_iota(jnp.int32, shape, 1)
+
+    def column(gain):
+        return jnp.sum(jnp.where(diagonal, jnp.broadcast_to(gain[...], shape), 0.0), axis=1, keepdims=True)
+
+    gains = {id(gain): column(gain) for gain in (gain_ref, gain2_ref)}
     for peer in range(Y * X):
+        row = row_ref.at[peer % BUFFERS]
         for n, (gain, ref) in enumerate(sources):
             cols = ref[:, peer * PART : (peer + 1) * PART]
-            row_ref[:, n * PART : (n + 1) * PART] = cols if gain is None else gain[...] * cols
-        out_ref[peer] = row_ref[...].astype(BF16)
+            row[:, n * PART : (n + 1) * PART] = cols if gain is None else gains[id(gain)] * cols
+        out_ref[peer] = row[...].astype(BF16)
 
 
 def packed(layers):
-    arrays = [a for gain, *matrices in layers for a in (gain[:, None], *matrices)]
+    arrays = [a for gain, *matrices in layers for a in (gain[None, :], *matrices)]
     vmem = pl.BlockSpec(memory_space=pltpu.VMEM)
     width = 3 * len(layers) * PART
     return pl.pallas_call(
@@ -61,8 +71,9 @@
         out_shape=jax.ShapeDtypeStruct((Y * X, ROWS, width), BF16),
         in_specs=[vmem] * len(arrays),
         out_specs=vmem,
-        scratch_shapes=[pltpu.VMEM((ROWS, width), F32)],
+        scratch_shapes=[pltpu.VMEM((BUFFERS, ROWS, width), F32)],
         cost_estimate=pl.CostEstimate(flops=10**6, bytes_accessed=10**6, transcendentals=0),
+        compiler_params=pltpu.CompilerParams(vmem_limit_bytes=8 * MIB),
         name="pack",
     )(*arrays)
 
@@ -87,11 +98,15 @@
 
 
 def over_x(pair):
-    return [pair] + [from_peer(pair, "x", X, k) for k in range(1, X)]
+    one, three = (from_peer(pair, "x", X, k) for k in (1, 3))
+    two = from_peer(pair, "x", X, 2)
+    return [pair, one, two, three]
 
 
 def over_core(pieces):
-    return [from_peer(piece, "core", CORE, 1) for piece in pieces]
+    own, one, three = (from_peer(pieces[k], "core", CORE, 1) for k in (0, 1, 3))
+    two = from_peer(pieces[2], "core", CORE, 1)
+    return [own, one, two, three]
 
 
 def slot(zl, zq):
@@ -155,6 +170,7 @@
         cost_estimate=pl.CostEstimate(
             flops=flops, bytes_accessed=2 * (2 * tokens.size + 2 * X * pieces[0].size), transcendentals=0
         ),
+        compiler_params=pltpu.CompilerParams(vmem_limit_bytes=20 * MIB),
         name="half_step",
     )(place("zq"), tokens, *pieces)
 
@@ -192,6 +208,7 @@
         cost_estimate=pl.CostEstimate(
             flops=10**8, bytes_accessed=2 * (2 * X * pieces[0].size + 3 * BLOCK * D), transcendentals=0
         ),
+        compiler_params=pltpu.CompilerParams(vmem_limit_bytes=16 * MIB),
         name="serve",
     )(place("x", "core", "b"), *pieces)
 

time: 273 us -> 277 us (1.015)
  Pallas kernels: 31.7 us -> 23.5 us
  local copies, waits for them, and re-layouts: 9.53 us -> 15.5 us
  waiting for transfers between devices: 77.2 us -> 81.4 us
  other arithmetic: 2.82 us -> 6.54 us
    unnamed x38 -> x42, local copies, waits for them, and re-layouts: 2.89 us -> 11.5 us
    pallas_call x1, Pallas kernels: 6.04 us -> 1.48 us  [packed(): pl.pallas_call(pack_kernel, out_shape=jax.ShapeDtypeStruct((Y * X, ROWS,...]
    ppermute x26, waiting for transfers between devices: 59.5 us -> 63.1 us  [from_peer(): return lax.ppermute(block, axis, [(i, i ^ flip) for i in range(size)])]
  transfers between devices with their start and end apart: 31 -> 31, of which waited for: 15 -> 17; matrix products, arithmetic and copies ran while one was open for 2% -> 2% of each run, Pallas kernels for 6% -> 4%
where the time goes in v3:
time: 277 us; the launch traced here: 275 us
  starting transfers between devices  101 us (36%)
  waiting for transfers between devices  81.4 us (29%)
  blocking collectives  45 us (16%)
  Pallas kernels  23.5 us (8%)
  local copies, waits for them, and re-layouts  15.5 us (6%)
  other arithmetic  6.54 us (2%)
    ppermute x26, starting transfers between devices, from_peer(): return lax.ppermute(block, axis, [(i, i ^ flip) for i in range(size)])  77.6 us
    ppermute x26, waiting for transfers between devices, from_peer(): return lax.ppermute(block, axis, [(i, i ^ flip) for i in range(size)])  63.1 us
    all_to_all x1, blocking collectives, swap(): return lax.all_to_all(blocks, axis, split_axis=0, concat_axis=0, tiled=True)  45 us
    all_to_all x5, starting transfers between devices, swap(): return lax.all_to_all(blocks, axis, split_axis=0, concat_axis=0, tiled=True)  23.8 us
    all_to_all x5, waiting for transfers between devices, swap(): return lax.all_to_all(blocks, axis, split_axis=0, concat_axis=0, tiled=True)  18.3 us
    pallas_call x2, Pallas kernels, half_partial(): pl.pallas_call(half_kernel, out_shape=jax.ShapeDtypeStruct(tokens.shape,...  12.7 us
    unnamed x42, local copies, waits for them, and re-layouts  11.5 us
    pallas_call x2, Pallas kernels, served(): pl.pallas_call(serve_kernel, out_shape=[jax.ShapeDtypeStruct((BLOCK, D),...  9.33 us
  transfers between devices with their start and end apart: 31, of which 17 were waited for; matrix products, arithmetic and copies ran while one was open for 2% of the time, Pallas kernels for 4%

profile of v3, /device:TPU:6, one launch (start us, length us, event | category | flops | bytes accessed | tf_op | source)
XLA Modules:
  0.0 274.6 jit_solution(16912275544109226148)
XLA Ops:
  1.5 3.8 %collective-permute-start = (bf16[64,256]{1,0:T(8,128)(2,1)S(1)}, bf16[64,256]{1,0:T(8,128)(2,1)S(1)}, u32[]{:S(2)}, u32[]{:S(2)}) collective-permute-start(bf16[64,256]{1,0:T(8,128)(2,1)S(1)} %broadcast_select_fusion.1), channel_id=1, source_target_pairs={{0,32},{32,0},{1,33},{33,1},{2,34},{34,2},{3,35},{35,3},{4,36},{36... | collective-permute-start | bytes 98312 | tf_op jit(solution)/shard_map/ppermute | solution.py:38
  13.4 7.4 %all-to-all-start = ((bf16[16,32,264]{2,1,0:T(8,128)(2,1)}), bf16[16,32,264]{2,1,0:T(8,128)(2,1)S(1)}, u32[]{:S(2)}, u32[]{:S(2)}) async-start(bf16[16,32,264]{2,1,0:T(8,128)(2,1)} %pack.1), calls=%async_computation | async-start | bytes 786432 | tf_op jit(solution)/shard_map/all_to_all | solution.py:30
  20.9 9.1 %collective-permute-start.1 = (bf16[2,64,256]{2,1,0:T(8,128)(2,1)S(1)}, bf16[2,64,256]{2,1,0:T(8,128)(2,1)S(1)}, u32[]{:S(2)}, u32[]{:S(2)}) collective-permute-start(bf16[2,64,256]{2,1,0:T(8,128)(2,1)S(1)} %get-tuple-element.121), channel_id=1, source_target_pairs={{0,128},{64,192},{128,0},{192,64},{1,129},{65,193},{129,1},{193,65... | collective-permute-start | bytes 196616 | tf_op jit(solution)/shard_map/ppermute | solution.py:38
  30.1 5.7 %collective-permute-done.1 = bf16[2,64,256]{2,1,0:T(8,128)(2,1)S(1)} collective-permute-done((bf16[2,64,256]{2,1,0:T(8,128)(2,1)S(1)}, bf16[2,64,256]{2,1,0:T(8,128)(2,1)S(1)}, u32[]{:S(2)}, u32[]{:S(2)}) %collective-permute-start.1) | collective-permute-done | bytes 65568 | tf_op jit(solution)/shard_map/ppermute | solution.py:38
  37.5 45.0 %all_to_all.30 = bf16[8,288,128]{2,1,0:T(8,128)(2,1)S(1)} all-to-all(bf16[8,288,128]{2,1,0:T(8,128)(2,1)S(1)} %bitcast.75), channel_id=1, replica_groups=mesh['gr'=2,'zq'=4,'b'=2,'y'=4,'x'=4,'core'=2] {'gr','zq'}, dimensions={0} | all-to-all | bytes 1179648 | tf_op jit(solution)/shard_map/all_to_all | solution.py:30
  82.5 2.4 collective-permute-start.3
  85.0 8.1 %collective-permute-done.3 = bf16[8,144,128]{2,1,0:T(8,128)(2,1)S(1)} collective-permute-done((bf16[8,144,128]{2,1,0:T(8,128)(2,1)S(1)}, bf16[8,144,128]{2,1,0:T(8,128)(2,1)S(1)}, u32[]{:S(2)}, u32[]{:S(2)}) %collective-permute-start.3) | collective-permute-done | bytes 294944 | tf_op jit(solution)/shard_map/ppermute | solution.py:38
  93.2 1.9 collective-permute-start.7
  95.2 4.8 %collective-permute-start.6 = (bf16[16,144,128]{2,1,0:T(8,128)(2,1)S(1)}, bf16[16,144,128]{2,1,0:T(8,128)(2,1)S(1)}, u32[]{:S(2)}, u32[]{:S(2)}) collective-permute-start(bf16[16,144,128]{2,1,0:T(8,128)(2,1)S(1)} %bitcast.67), channel_id=1, source_target_pairs={{0,4},{2,6},{4,0},{6,2},{1,5},{3,7},{5,1},{7,3},{8,12},{10,14},{12... | collective-permute-start | bytes 1769480 | tf_op jit(solution)/shard_map/ppermute | solution.py:38
  100.0 3.1 %collective-permute-start.5 = (bf16[16,144,128]{2,1,0:T(8,128)(2,1)S(1)}, bf16[16,144,128]{2,1,0:T(8,128)(2,1)}, u32[]{:S(2)}, u32[]{:S(2)}) collective-permute-start(bf16[16,144,128]{2,1,0:T(8,128)(2,1)S(1)} %bitcast.68), channel_id=1, source_target_pairs={{0,2},{2,0},{4,6},{6,4},{1,3},{3,1},{5,7},{7,5},{8,10},{10,8},{12,... | collective-permute-start | bytes 1769480 | tf_op jit(solution)/shard_map/ppermute | solution.py:38
  103.1 3.9 %collective-permute-start.2 = (bf16[2,2,64,256]{3,2,1,0:T(8,128)(2,1)S(1)}, bf16[2,2,64,256]{3,2,1,0:T(8,128)(2,1)S(1)}, u32[]{:S(2)}, u32[]{:S(2)}) collective-permute-start(bf16[2,2,64,256]{3,2,1,0:T(8,128)(2,1)S(1)} %pad_maximum_fusion.4), channel_id=1, source_target_pairs={{0,64},{64,0},{128,192},{192,128},{1,65},{65,1},{129,193},{193,129... | collective-permute-start | bytes 393224 | tf_op jit(solution)/shard_map/ppermute | solution.py:38
  107.0 5.0 %collective-permute-done.2 = bf16[2,2,64,256]{3,2,1,0:T(8,128)(2,1)S(1)} collective-permute-done((bf16[2,2,64,256]{3,2,1,0:T(8,128)(2,1)S(1)}, bf16[2,2,64,256]{3,2,1,0:T(8,128)(2,1)S(1)}, u32[]{:S(2)}, u32[]{:S(2)}) %collective-permute-start.2) | collective-permute-done | bytes 131104 | tf_op jit(solution)/shard_map/ppermute | solution.py:38
  113.1 4.2 %all-to-all-start.2 = ((bf16[4,4,2,64,256]{4,3,2,1,0:T(8,128)(2,1)}), bf16[4,4,2,64,256]{4,3,2,1,0:T(8,128)(2,1)S(1)}, u32[]{:S(2)}, u32[]{:S(2)}) async-start(bf16[4,4,2,64,256]{4,3,2,1,0:T(8,128)(2,1)} %broadcast_in_dim.13), calls=%async_computation.2 | async-start | bytes 2097152 | tf_op jit(solution)/shard_map/all_to_all | solution.py:30
  119.3 1.9 collective-permute-start.8
  125.0 2.4 collective-permute-start.10
  127.4 1.9 collective-permute-start.9
  129.6 2.1 collective-permute-done.9.refs_5_
  131.7 6.6 %half_step.2 = bf16[4,4,2,64,256]{4,3,2,1,0:T(8,128)(2,1)} custom-call(s32[1]{0:T(128)} %bitcast.3.at_ref, bf16[4,4,2,64,256]{4,3,2,1,0:T(8,128)(2,1)S(1)} %all-to-all-done.2.x_ref, bf16[16,144,128]{2,1,0:T(8,128)(2,1)S(1)} %bitcast.70, bf16[16,144,128]{2,1,0:T(8,128)(2,1)} %collective-permute-done.5.refs_1_, ...), custom_call_target="tpu_custom_call" | custom-call | flops 1207959552 | bytes 6815744 | tf_op jit(solution)/shard_map/half_step/pallas_call | solution.py:164
  138.3 4.2 %all-to-all-start.3 = ((bf16[4,4,2,64,256]{4,3,2,1,0:T(8,128)(2,1)}), bf16[4,4,2,64,256]{4,3,2,1,0:T(8,128)(2,1)}, u32[]{:S(2)}, u32[]{:S(2)}) async-start(bf16[4,4,2,64,256]{4,3,2,1,0:T(8,128)(2,1)} %half_step.2), calls=%async_computation.3 | async-start | bytes 2097152 | tf_op jit(solution)/shard_map/all_to_all | solution.py:30
  142.6 2.4 collective-permute-start.16
  145.0 3.1 %collective-permute-start.15 = (bf16[16,144,128]{2,1,0:T(8,128)(2,1)S(1)}, bf16[16,144,128]{2,1,0:T(8,128)(2,1)}, u32[]{:S(2)}, u32[]{:S(2)}) collective-permute-start(bf16[16,144,128]{2,1,0:T(8,128)(2,1)S(1)} %bitcast.61), channel_id=1, source_target_pairs={{0,4},{2,6},{4,0},{6,2},{1,5},{3,7},{5,1},{7,3},{8,12},{10,14},{12... | collective-permute-start | bytes 1769480 | tf_op jit(solution)/shard_map/ppermute | solution.py:38
  148.1 4.3 %collective-permute-start.14 = (bf16[16,144,128]{2,1,0:T(8,128)(2,1)S(1)}, bf16[16,144,128]{2,1,0:T(8,128)(2,1)}, u32[]{:S(2)}, u32[]{:S(2)}) collective-permute-start(bf16[16,144,128]{2,1,0:T(8,128)(2,1)S(1)} %bitcast.62), channel_id=1, source_target_pairs={{0,2},{2,0},{4,6},{6,4},{1,3},{3,1},{5,7},{7,5},{8,10},{10,8},{12,... | collective-permute-start | bytes 1769480 | tf_op jit(solution)/shard_map/ppermute | solution.py:38
  152.4 5.9 %all-to-all-done.3 = bf16[4,4,2,64,256]{4,3,2,1,0:T(8,128)(2,1)} async-done(((bf16[4,4,2,64,256]{4,3,2,1,0:T(8,128)(2,1)}), bf16[4,4,2,64,256]{4,3,2,1,0:T(8,128)(2,1)}, u32[]{:S(2)}, u32[]{:S(2)}) %all-to-all-start.3) | async-done | bytes 1048608 | tf_op jit(solution)/shard_map/all_to_all | solution.py:30
  159.4 3.7 %collective-permute-start.12 = (bf16[2,2,64,256]{3,2,1,0:T(8,128)(2,1)S(1)}, bf16[2,2,64,256]{3,2,1,0:T(8,128)(2,1)S(1)}, u32[]{:S(2)}, u32[]{:S(2)}) collective-permute-start(bf16[2,2,64,256]{3,2,1,0:T(8,128)(2,1)S(1)} %slice_reduce_fusion), channel_id=1, source_target_pairs={{0,64},{64,0},{128,192},{192,128},{1,65},{65,1},{129,193},{193,129... | collective-permute-start | bytes 393224 | tf_op jit(solution)/shard_map/ppermute | solution.py:38
  164.2 5.4 %collective-permute-done.12 = bf16[2,2,64,256]{3,2,1,0:T(8,128)(2,1)S(1)} collective-permute-done((bf16[2,2,64,256]{3,2,1,0:T(8,128)(2,1)S(1)}, bf16[2,2,64,256]{3,2,1,0:T(8,128)(2,1)S(1)}, u32[]{:S(2)}, u32[]{:S(2)}) %collective-permute-start.12) | collective-permute-done | bytes 131104 | tf_op jit(solution)/shard_map/ppermute | solution.py:38
  169.7 3.1 %collective-permute-start.13 = (bf16[2,64,256]{2,1,0:T(8,128)(2,1)S(1)}, bf16[2,64,256]{2,1,0:T(8,128)(2,1)S(1)}, u32[]{:S(2)}, u32[]{:S(2)}) collective-permute-start(bf16[2,64,256]{2,1,0:T(8,128)(2,1)S(1)} %fusion.5), channel_id=1, source_target_pairs={{0,128},{64,192},{128,0},{192,64},{1,129},{65,193},{129,1},{193,65... | collective-permute-start | bytes 196616 | tf_op jit(solution)/shard_map/ppermute | solution.py:38
  172.9 4.9 %serve.2 = (bf16[176,2048]{1,0:T(8,128)(2,1)}, bf16[176,2048]{1,0:T(8,128)(2,1)}, bf16[176,2048]{1,0:T(8,128)(2,1)}) custom-call(s32[3]{0:T(128)S(1)} %pad_add_fusion.at_ref, bf16[16,144,128]{2,1,0:T(8,128)(2,1)S(1)} %bitcast.71, bf16[16,144,128]{2,1,0:T(8,128)(2,1)} %collective-permute-done.5.refs_1_, ...), custom_call_target="tpu_custom_call" | custom-call | flops 100000000 | bytes 6881280 | tf_op jit(solution)/shard_map/serve/pallas_call | solution.py:198
  177.8 4.0 %collective-permute-done.13 = bf16[2,64,256]{2,1,0:T(8,128)(2,1)S(1)} collective-permute-done((bf16[2,64,256]{2,1,0:T(8,128)(2,1)S(1)}, bf16[2,64,256]{2,1,0:T(8,128)(2,1)S(1)}, u32[]{:S(2)}, u32[]{:S(2)}) %collective-permute-start.13) | collective-permute-done | bytes 65568 | tf_op jit(solution)/shard_map/ppermute | solution.py:38
  181.8 2.7 collective-permute-start.17
  184.5 8.2 %collective-permute-done.17 = bf16[2,64,256]{2,1,0:T(8,128)(2,1)S(1)} collective-permute-done((bf16[2,64,256]{2,1,0:T(8,128)(2,1)S(1)}, bf16[2,64,256]{2,1,0:T(8,128)(2,1)S(1)}, u32[]{:S(2)}, u32[]{:S(2)}) %collective-permute-start.17) | collective-permute-done | bytes 65568 | tf_op jit(solution)/shard_map/ppermute | solution.py:38
  192.7 1.9 collective-permute-start.18
  194.7 6.5 %collective-permute-done.18 = bf16[2,2,64,256]{3,2,1,0:T(8,128)(2,1)S(1)} collective-permute-done((bf16[2,2,64,256]{3,2,1,0:T(8,128)(2,1)S(1)}, bf16[2,2,64,256]{3,2,1,0:T(8,128)(2,1)S(1)}, u32[]{:S(2)}, u32[]{:S(2)}) %collective-permute-start.18) | collective-permute-done | bytes 131104 | tf_op jit(solution)/shard_map/ppermute | solution.py:38
  202.3 3.5 %all-to-all-start.4 = ((bf16[4,4,2,64,256]{4,3,2,1,0:T(8,128)(2,1)}), bf16[4,4,2,64,256]{4,3,2,1,0:T(8,128)(2,1)S(1)}, u32[]{:S(2)}, u32[]{:S(2)}) async-start(bf16[4,4,2,64,256]{4,3,2,1,0:T(8,128)(2,1)} %broadcast_in_dim.28), calls=%async_computation.4 | async-start | bytes 2097152 | tf_op jit(solution)/shard_map/all_to_all | solution.py:30
  205.8 1.9 collective-permute-start.19
  207.8 2.4 collective-permute-start.20
  210.2 1.9 collective-permute-start.21
  212.1 2.4 collective-permute-start.22
  216.9 3.7 %all-to-all-done.4.x_ref = bf16[4,4,2,64,256]{4,3,2,1,0:T(8,128)(2,1)S(1)} async-done(((bf16[4,4,2,64,256]{4,3,2,1,0:T(8,128)(2,1)}), bf16[4,4,2,64,256]{4,3,2,1,0:T(8,128)(2,1)S(1)}, u32[]{:S(2)}, u32[]{:S(2)}) %all-to-all-start.4) | async-done | bytes 1048608 | tf_op jit(solution)/shard_map/all_to_all | solution.py:30
  222.8 6.1 %half_step.3 = bf16[4,4,2,64,256]{4,3,2,1,0:T(8,128)(2,1)} custom-call(s32[1]{0:T(128)} %bitcast.3.at_ref, bf16[4,4,2,64,256]{4,3,2,1,0:T(8,128)(2,1)S(1)} %all-to-all-done.4.x_ref, bf16[16,144,128]{2,1,0:T(8,128)(2,1)S(1)} %bitcast.64, bf16[16,144,128]{2,1,0:T(8,128)(2,1)} %collective-permute-done.14.refs_1_, ...), custom_call_target="tpu_custom_call" | custom-call | flops 1207959552 | bytes 6815744 | tf_op jit(solution)/shard_map/half_step/pallas_call | solution.py:164
  228.9 4.4 %all-to-all-start.5 = ((bf16[4,4,2,64,256]{4,3,2,1,0:T(8,128)(2,1)}), bf16[4,4,2,64,256]{4,3,2,1,0:T(8,128)(2,1)}, u32[]{:S(2)}, u32[]{:S(2)}) async-start(bf16[4,4,2,64,256]{4,3,2,1,0:T(8,128)(2,1)} %half_step.3), calls=%async_computation.5 | async-start | bytes 2097152 | tf_op jit(solution)/shard_map/all_to_all | solution.py:30
  234.4 4.5 %serve.3 = (bf16[176,2048]{1,0:T(8,128)(2,1)}, bf16[176,2048]{1,0:T(8,128)(2,1)}, bf16[176,2048]{1,0:T(8,128)(2,1)}) custom-call(s32[3]{0:T(128)S(1)} %pad_add_fusion.at_ref, bf16[16,144,128]{2,1,0:T(8,128)(2,1)S(1)} %bitcast.65, bf16[16,144,128]{2,1,0:T(8,128)(2,1)} %collective-permute-done.14.refs_1_, ...), custom_call_target="tpu_custom_call" | custom-call | flops 100000000 | bytes 6881280 | tf_op jit(solution)/shard_map/serve/pallas_call | solution.py:198
  238.9 8.5 %all-to-all-done.5 = bf16[4,4,2,64,256]{4,3,2,1,0:T(8,128)(2,1)} async-done(((bf16[4,4,2,64,256]{4,3,2,1,0:T(8,128)(2,1)}), bf16[4,4,2,64,256]{4,3,2,1,0:T(8,128)(2,1)}, u32[]{:S(2)}, u32[]{:S(2)}) %all-to-all-start.5) | async-done | bytes 1048608 | tf_op jit(solution)/shard_map/all_to_all | solution.py:30
  248.5 1.9 collective-permute-start.23
  251.6 4.7 %collective-permute-done.23 = bf16[2,2,64,256]{3,2,1,0:T(8,128)(2,1)S(1)} collective-permute-done((bf16[2,2,64,256]{3,2,1,0:T(8,128)(2,1)S(1)}, bf16[2,2,64,256]{3,2,1,0:T(8,128)(2,1)S(1)}, u32[]{:S(2)}, u32[]{:S(2)}) %collective-permute-start.23) | collective-permute-done | bytes 131104 | tf_op jit(solution)/shard_map/ppermute | solution.py:38
  256.3 4.8 %collective-permute-start.24 = (bf16[2,64,256]{2,1,0:T(8,128)(2,1)S(1)}, bf16[2,64,256]{2,1,0:T(8,128)(2,1)S(1)}, u32[]{:S(2)}, u32[]{:S(2)}) collective-permute-start(bf16[2,64,256]{2,1,0:T(8,128)(2,1)S(1)} %fusion.6), channel_id=1, source_target_pairs={{0,128},{64,192},{128,0},{192,64},{1,129},{65,193},{129,1},{193,65... | collective-permute-start | bytes 196616 | tf_op jit(solution)/shard_map/ppermute | solution.py:38
  261.1 6.9 %collective-permute-done.24 = bf16[2,64,256]{2,1,0:T(8,128)(2,1)S(1)} collective-permute-done((bf16[2,64,256]{2,1,0:T(8,128)(2,1)S(1)}, bf16[2,64,256]{2,1,0:T(8,128)(2,1)S(1)}, u32[]{:S(2)}, u32[]{:S(2)}) %collective-permute-start.24) | collective-permute-done | bytes 65568 | tf_op jit(solution)/shard_map/ppermute | solution.py:38
  268.1 1.9 collective-permute-start.25
  270.1 3.9 %collective-permute-done.25 = bf16[64,256]{1,0:T(8,128)(2,1)S(1)} collective-permute-done((bf16[64,256]{1,0:T(8,128)(2,1)S(1)}, bf16[64,256]{1,0:T(8,128)(2,1)S(1)}, u32[]{:S(2)}, u32[]{:S(2)}) %collective-permute-start.25) | collective-permute-done | bytes 32800 | tf_op jit(solution)/shard_map/ppermute | solution.py:38
  (98 shorter events, 30.1 us)
Async XLA Ops:
  0.6 20.2 %copy-start.20 = (bf16[512,64]{0,1:T(8,128)(2,1)S(1)}, bf16[512,64]{0,1:T(8,128)(2,1)}, u32[]{:S(2)}) copy-start(bf16[512,64]{0,1:T(8,128)(2,1)} %param.9) | copy-start | bytes 196612
  1.5 19.4 %collective-permute-start = (bf16[64,256]{1,0:T(8,128)(2,1)S(1)}, bf16[64,256]{1,0:T(8,128)(2,1)S(1)}, u32[]{:S(2)}, u32[]{:S(2)}) collective-permute-start(bf16[64,256]{1,0:T(8,128)(2,1)S(1)} %broadcast_select_fusion.1), channel_id=1, source_target_pairs={{0,32},{32,0},{1,33},{33,1},{2,34},{34,2},{3,35},{35,3},{4,36},{36... | collective-permute-start | bytes 98312 | tf_op jit(solution)/shard_map/ppermute | solution.py:38
  5.3 0.9 copy-start.6
  6.2 0.9 copy-start.7
  7.1 0.9 copy-start.8
  8.0 0.9 copy-start.9
  8.9 0.9 copy-start.10
  9.8 0.9 copy-start.11
  13.4 22.4 %all-to-all-start = ((bf16[16,32,264]{2,1,0:T(8,128)(2,1)}), bf16[16,32,264]{2,1,0:T(8,128)(2,1)S(1)}, u32[]{:S(2)}, u32[]{:S(2)}) async-start(bf16[16,32,264]{2,1,0:T(8,128)(2,1)} %pack.1), calls=%async_computation | async-start | bytes 786432 | tf_op jit(solution)/shard_map/all_to_all | solution.py:30
  20.9 14.9 %copy-start.14 = (bf16[1,64,256]{2,1,0:T(8,128)(2,1)}, bf16[1,64,256]{2,1,0:T(8,128)(2,1)S(1)}, u32[]{:S(2)}) copy-start(bf16[1,64,256]{2,1,0:T(8,128)(2,1)S(1)} %get-tuple-element.118) | copy-start | bytes 98308
  20.9 14.9 %copy-start.17 = (bf16[1,64,256]{2,1,0:T(8,128)(2,1)}, bf16[1,64,256]{2,1,0:T(8,128)(2,1)S(1)}, u32[]{:S(2)}) copy-start(bf16[1,64,256]{2,1,0:T(8,128)(2,1)S(1)} %get-tuple-element.119) | copy-start | bytes 98308
  20.9 14.8 %collective-permute-start.1 = (bf16[2,64,256]{2,1,0:T(8,128)(2,1)S(1)}, bf16[2,64,256]{2,1,0:T(8,128)(2,1)S(1)}, u32[]{:S(2)}, u32[]{:S(2)}) collective-permute-start(bf16[2,64,256]{2,1,0:T(8,128)(2,1)S(1)} %get-tuple-element.121), channel_id=1, source_target_pairs={{0,128},{64,192},{128,0},{192,64},{1,129},{65,193},{129,1},{193,65... | collective-permute-start | bytes 196616 | tf_op jit(solution)/shard_map/ppermute | solution.py:38
  82.5 10.5 %collective-permute-start.3 = (bf16[8,144,128]{2,1,0:T(8,128)(2,1)S(1)}, bf16[8,144,128]{2,1,0:T(8,128)(2,1)S(1)}, u32[]{:S(2)}, u32[]{:S(2)}) collective-permute-start(bf16[8,144,128]{2,1,0:T(8,128)(2,1)S(1)} %slice.60), channel_id=1, source_target_pairs={{0,32},{32,0},{1,33},{33,1},{2,34},{34,2},{3,35},{35,3},{4,36},{36... | collective-permute-start | bytes 884744 | tf_op jit(solution)/shard_map/ppermute | solution.py:38
  93.2 29.8 %collective-permute-start.7 = (bf16[16,144,128]{2,1,0:T(8,128)(2,1)S(1)}, bf16[16,144,128]{2,1,0:T(8,128)(2,1)S(1)}, u32[]{:S(2)}, u32[]{:S(2)}) collective-permute-start(bf16[16,144,128]{2,1,0:T(8,128)(2,1)S(1)} %bitcast.66), channel_id=1, source_target_pairs={{0,6},{2,4},{4,2},{6,0},{1,7},{3,5},{5,3},{7,1},{8,14},{10,12},{12... | collective-permute-start | bytes 1769480 | tf_op jit(solution)/shard_map/ppermute | solution.py:38
  95.2 29.8 %collective-permute-start.6 = (bf16[16,144,128]{2,1,0:T(8,128)(2,1)S(1)}, bf16[16,144,128]{2,1,0:T(8,128)(2,1)S(1)}, u32[]{:S(2)}, u32[]{:S(2)}) collective-permute-start(bf16[16,144,128]{2,1,0:T(8,128)(2,1)S(1)} %bitcast.67), channel_id=1, source_target_pairs={{0,4},{2,6},{4,0},{6,2},{1,5},{3,7},{5,1},{7,3},{8,12},{10,14},{12... | collective-permute-start | bytes 1769480 | tf_op jit(solution)/shard_map/ppermute | solution.py:38
  100.0 27.4 %collective-permute-start.5 = (bf16[16,144,128]{2,1,0:T(8,128)(2,1)S(1)}, bf16[16,144,128]{2,1,0:T(8,128)(2,1)}, u32[]{:S(2)}, u32[]{:S(2)}) collective-permute-start(bf16[16,144,128]{2,1,0:T(8,128)(2,1)S(1)} %bitcast.68), channel_id=1, source_target_pairs={{0,2},{2,0},{4,6},{6,4},{1,3},{3,1},{5,7},{7,5},{8,10},{10,8},{12,... | collective-permute-start | bytes 1769480 | tf_op jit(solution)/shard_map/ppermute | solution.py:38
  103.1 8.9 %collective-permute-start.2 = (bf16[2,2,64,256]{3,2,1,0:T(8,128)(2,1)S(1)}, bf16[2,2,64,256]{3,2,1,0:T(8,128)(2,1)S(1)}, u32[]{:S(2)}, u32[]{:S(2)}) collective-permute-start(bf16[2,2,64,256]{3,2,1,0:T(8,128)(2,1)S(1)} %pad_maximum_fusion.4), channel_id=1, source_target_pairs={{0,64},{64,0},{128,192},{192,128},{1,65},{65,1},{129,193},{193,129... | collective-permute-start | bytes 393224 | tf_op jit(solution)/shard_map/ppermute | solution.py:38
  113.1 16.5 %all-to-all-start.2 = ((bf16[4,4,2,64,256]{4,3,2,1,0:T(8,128)(2,1)}), bf16[4,4,2,64,256]{4,3,2,1,0:T(8,128)(2,1)S(1)}, u32[]{:S(2)}, u32[]{:S(2)}) async-start(bf16[4,4,2,64,256]{4,3,2,1,0:T(8,128)(2,1)} %broadcast_in_dim.13), calls=%async_computation.2 | async-start | bytes 2097152 | tf_op jit(solution)/shard_map/all_to_all | solution.py:30
  117.4 12.0 %collective-permute-start.4 = (bf16[8,144,128]{2,1,0:T(8,128)(2,1)S(1)}, bf16[8,144,128]{2,1,0:T(8,128)(2,1)S(1)}, u32[]{:S(2)}, u32[]{:S(2)}) collective-permute-start(bf16[8,144,128]{2,1,0:T(8,128)(2,1)S(1)} %get-tuple-element.62), channel_id=1, source_target_pairs={{0,32},{32,0},{1,33},{33,1},{2,34},{34,2},{3,35},{35,3},{4,36},{36... | collective-permute-start | bytes 884744 | tf_op jit(solution)/shard_map/ppermute | solution.py:38
  119.3 10.2 %collective-permute-start.8 = (bf16[16,144,128]{2,1,0:T(8,128)(2,1)S(1)}, bf16[16,144,128]{2,1,0:T(8,128)(2,1)}, u32[]{:S(2)}, u32[]{:S(2)}) collective-permute-start(bf16[16,144,128]{2,1,0:T(8,128)(2,1)S(1)} %bitcast.69), channel_id=1, source_target_pairs={{0,1},{1,0},{2,3},{3,2},{4,5},{5,4},{6,7},{7,6},{8,9},{9,8},{10,11... | collective-permute-start | bytes 1769480 | tf_op jit(solution)/shard_map/ppermute | solution.py:38
  123.1 6.5 %collective-permute-start.11 = (bf16[16,144,128]{2,1,0:T(8,128)(2,1)S(1)}, bf16[16,144,128]{2,1,0:T(8,128)(2,1)}, u32[]{:S(2)}, u32[]{:S(2)}) collective-permute-start(bf16[16,144,128]{2,1,0:T(8,128)(2,1)S(1)} %collective-permute-done.7.refs_3_), channel_id=1, source_target_pairs={{0,1},{1,0},{2,3},{3,2},{4,5},{5,4},{6,7},{7,6},{8,9},{9,8},{10,11... | collective-permute-start | bytes 1769480 | tf_op jit(solution)/shard_map/ppermute | solution.py:38
  125.0 4.6 %collective-permute-start.10 = (bf16[16,144,128]{2,1,0:T(8,128)(2,1)S(1)}, bf16[16,144,128]{2,1,0:T(8,128)(2,1)}, u32[]{:S(2)}, u32[]{:S(2)}) collective-permute-start(bf16[16,144,128]{2,1,0:T(8,128)(2,1)S(1)} %collective-permute-done.6.refs_2_), channel_id=1, source_target_pairs={{0,1},{1,0},{2,3},{3,2},{4,5},{5,4},{6,7},{7,6},{8,9},{9,8},{10,11... | collective-permute-start | bytes 1769480 | tf_op jit(solution)/shard_map/ppermute | solution.py:38
  127.4 4.2 %collective-permute-start.9 = (bf16[16,144,128]{2,1,0:T(8,128)(2,1)}, bf16[16,144,128]{2,1,0:T(8,128)(2,1)}, u32[]{:S(2)}, u32[]{:S(2)}) collective-permute-start(bf16[16,144,128]{2,1,0:T(8,128)(2,1)} %collective-permute-done.5.refs_1_), channel_id=1, source_target_pairs={{0,1},{1,0},{2,3},{3,2},{4,5},{5,4},{6,7},{7,6},{8,9},{9,8},{10,11... | collective-permute-start | bytes 1769480 | tf_op jit(solution)/shard_map/ppermute | solution.py:38
  138.3 20.0 %all-to-all-start.3 = ((bf16[4,4,2,64,256]{4,3,2,1,0:T(8,128)(2,1)}), bf16[4,4,2,64,256]{4,3,2,1,0:T(8,128)(2,1)}, u32[]{:S(2)}, u32[]{:S(2)}) async-start(bf16[4,4,2,64,256]{4,3,2,1,0:T(8,128)(2,1)} %half_step.2), calls=%async_computation.3 | async-start | bytes 2097152 | tf_op jit(solution)/shard_map/all_to_all | solution.py:30
  142.6 39.2 %collective-permute-start.16 = (bf16[16,144,128]{2,1,0:T(8,128)(2,1)S(1)}, bf16[16,144,128]{2,1,0:T(8,128)(2,1)S(1)}, u32[]{:S(2)}, u32[]{:S(2)}) collective-permute-start(bf16[16,144,128]{2,1,0:T(8,128)(2,1)S(1)} %bitcast.60), channel_id=1, source_target_pairs={{0,6},{2,4},{4,2},{6,0},{1,7},{3,5},{5,3},{7,1},{8,14},{10,12},{12... | collective-permute-start | bytes 1769480 | tf_op jit(solution)/shard_map/ppermute | solution.py:38
  145.0 36.8 %collective-permute-start.15 = (bf16[16,144,128]{2,1,0:T(8,128)(2,1)S(1)}, bf16[16,144,128]{2,1,0:T(8,128)(2,1)}, u32[]{:S(2)}, u32[]{:S(2)}) collective-permute-start(bf16[16,144,128]{2,1,0:T(8,128)(2,1)S(1)} %bitcast.61), channel_id=1, source_target_pairs={{0,4},{2,6},{4,0},{6,2},{1,5},{3,7},{5,1},{7,3},{8,12},{10,14},{12... | collective-permute-start | bytes 1769480 | tf_op jit(solution)/shard_map/ppermute | solution.py:38
  148.1 33.7 %collective-permute-start.14 = (bf16[16,144,128]{2,1,0:T(8,128)(2,1)S(1)}, bf16[16,144,128]{2,1,0:T(8,128)(2,1)}, u32[]{:S(2)}, u32[]{:S(2)}) collective-permute-start(bf16[16,144,128]{2,1,0:T(8,128)(2,1)S(1)} %bitcast.62), channel_id=1, source_target_pairs={{0,2},{2,0},{4,6},{6,4},{1,3},{3,1},{5,7},{7,5},{8,10},{10,8},{12,... | collective-permute-start | bytes 1769480 | tf_op jit(solution)/shard_map/ppermute | solution.py:38
  159.4 10.3 %collective-permute-start.12 = (bf16[2,2,64,256]{3,2,1,0:T(8,128)(2,1)S(1)}, bf16[2,2,64,256]{3,2,1,0:T(8,128)(2,1)S(1)}, u32[]{:S(2)}, u32[]{:S(2)}) collective-permute-start(bf16[2,2,64,256]{3,2,1,0:T(8,128)(2,1)S(1)} %slice_reduce_fusion), channel_id=1, source_target_pairs={{0,64},{64,0},{128,192},{192,128},{1,65},{65,1},{129,193},{193,129... | collective-permute-start | bytes 393224 | tf_op jit(solution)/shard_map/ppermute | solution.py:38
  169.7 12.0 %collective-permute-start.13 = (bf16[2,64,256]{2,1,0:T(8,128)(2,1)S(1)}, bf16[2,64,256]{2,1,0:T(8,128)(2,1)S(1)}, u32[]{:S(2)}, u32[]{:S(2)}) collective-permute-start(bf16[2,64,256]{2,1,0:T(8,128)(2,1)S(1)} %fusion.5), channel_id=1, source_target_pairs={{0,128},{64,192},{128,0},{192,64},{1,129},{65,193},{129,1},{193,65... | collective-permute-start | bytes 196616 | tf_op jit(solution)/shard_map/ppermute | solution.py:38
  172.9 8.9 %copy-start.15 = (bf16[1,64,256]{2,1,0:T(8,128)(2,1)S(1)}, bf16[1,64,256]{2,1,0:T(8,128)(2,1)}, u32[]{:S(2)}) copy-start(bf16[1,64,256]{2,1,0:T(8,128)(2,1)} %copy-done.14) | copy-start | bytes 98308
  172.9 8.9 %copy-start.18 = (bf16[1,64,256]{2,1,0:T(8,128)(2,1)S(1)}, bf16[1,64,256]{2,1,0:T(8,128)(2,1)}, u32[]{:S(2)}) copy-start(bf16[1,64,256]{2,1,0:T(8,128)(2,1)} %copy-done.17) | copy-start | bytes 98308
  181.8 10.9 %collective-permute-start.17 = (bf16[2,64,256]{2,1,0:T(8,128)(2,1)S(1)}, bf16[2,64,256]{2,1,0:T(8,128)(2,1)S(1)}, u32[]{:S(2)}, u32[]{:S(2)}) collective-permute-start(bf16[2,64,256]{2,1,0:T(8,128)(2,1)S(1)} %add_convert_fusion), channel_id=1, source_target_pairs={{0,128},{64,192},{128,0},{192,64},{1,129},{65,193},{129,1},{193,65... | collective-permute-start | bytes 196616 | tf_op jit(solution)/shard_map/ppermute | solution.py:38
  192.7 8.4 %collective-permute-start.18 = (bf16[2,2,64,256]{3,2,1,0:T(8,128)(2,1)S(1)}, bf16[2,2,64,256]{3,2,1,0:T(8,128)(2,1)S(1)}, u32[]{:S(2)}, u32[]{:S(2)}) collective-permute-start(bf16[2,2,64,256]{3,2,1,0:T(8,128)(2,1)S(1)} %pad_maximum_fusion.5), channel_id=1, source_target_pairs={{0,64},{64,0},{128,192},{192,128},{1,65},{65,1},{129,193},{193,129... | collective-permute-start | bytes 393224 | tf_op jit(solution)/shard_map/ppermute | solution.py:38
  202.3 18.4 %all-to-all-start.4 = ((bf16[4,4,2,64,256]{4,3,2,1,0:T(8,128)(2,1)}), bf16[4,4,2,64,256]{4,3,2,1,0:T(8,128)(2,1)S(1)}, u32[]{:S(2)}, u32[]{:S(2)}) async-start(bf16[4,4,2,64,256]{4,3,2,1,0:T(8,128)(2,1)} %broadcast_in_dim.28), calls=%async_computation.4 | async-start | bytes 2097152 | tf_op jit(solution)/shard_map/all_to_all | solution.py:30
  205.8 8.7 %collective-permute-start.19 = (bf16[16,144,128]{2,1,0:T(8,128)(2,1)S(1)}, bf16[16,144,128]{2,1,0:T(8,128)(2,1)S(1)}, u32[]{:S(2)}, u32[]{:S(2)}) collective-permute-start(bf16[16,144,128]{2,1,0:T(8,128)(2,1)S(1)} %bitcast.63), channel_id=1, source_target_pairs={{0,1},{1,0},{2,3},{3,2},{4,5},{5,4},{6,7},{7,6},{8,9},{9,8},{10,11... | collective-permute-start | bytes 1769480 | tf_op jit(solution)/shard_map/ppermute | solution.py:38
  207.8 6.8 %collective-permute-start.20 = (bf16[16,144,128]{2,1,0:T(8,128)(2,1)}, bf16[16,144,128]{2,1,0:T(8,128)(2,1)S(1)}, u32[]{:S(2)}, u32[]{:S(2)}) collective-permute-start(bf16[16,144,128]{2,1,0:T(8,128)(2,1)} %collective-permute-done.14.refs_1_), channel_id=1, source_target_pairs={{0,1},{1,0},{2,3},{3,2},{4,5},{5,4},{6,7},{7,6},{8,9},{9,8},{10,11... | collective-permute-start | bytes 1769480 | tf_op jit(solution)/shard_map/ppermute | solution.py:38
  210.2 4.4 %collective-permute-start.21 = (bf16[16,144,128]{2,1,0:T(8,128)(2,1)}, bf16[16,144,128]{2,1,0:T(8,128)(2,1)S(1)}, u32[]{:S(2)}, u32[]{:S(2)}) collective-permute-start(bf16[16,144,128]{2,1,0:T(8,128)(2,1)} %collective-permute-done.15.refs_2_), channel_id=1, source_target_pairs={{0,1},{1,0},{2,3},{3,2},{4,5},{5,4},{6,7},{7,6},{8,9},{9,8},{10,11... | collective-permute-start | bytes 1769480 | tf_op jit(solution)/shard_map/ppermute | solution.py:38
  212.1 4.0 %collective-permute-start.22 = (bf16[16,144,128]{2,1,0:T(8,128)(2,1)S(1)}, bf16[16,144,128]{2,1,0:T(8,128)(2,1)S(1)}, u32[]{:S(2)}, u32[]{:S(2)}) collective-permute-start(bf16[16,144,128]{2,1,0:T(8,128)(2,1)S(1)} %collective-permute-done.16.refs_3_), channel_id=1, source_target_pairs={{0,1},{1,0},{2,3},{3,2},{4,5},{5,4},{6,7},{7,6},{8,9},{9,8},{10,11... | collective-permute-start | bytes 1769480 | tf_op jit(solution)/shard_map/ppermute | solution.py:38
  220.7 1.1 copy-start.1
  221.8 1.1 copy-start.4
  228.9 4.4 %copy-start.2 = (bf16[16,144,128]{2,1,0:T(8,128)(2,1)S(1)}, bf16[16,144,128]{2,1,0:T(8,128)(2,1)}, u32[]{:S(2)}) copy-start(bf16[16,144,128]{2,1,0:T(8,128)(2,1)} %copy-done) | copy-start | bytes 1769476
  228.9 18.5 %all-to-all-start.5 = ((bf16[4,4,2,64,256]{4,3,2,1,0:T(8,128)(2,1)}), bf16[4,4,2,64,256]{4,3,2,1,0:T(8,128)(2,1)}, u32[]{:S(2)}, u32[]{:S(2)}) async-start(bf16[4,4,2,64,256]{4,3,2,1,0:T(8,128)(2,1)} %half_step.3), calls=%async_computation.5 | async-start | bytes 2097152 | tf_op jit(solution)/shard_map/all_to_all | solution.py:30
  233.3 1.1 copy-start.5
  247.4 20.7 %copy-start.16 = (bf16[1,64,256]{2,1,0:T(8,128)(2,1)S(1)}, bf16[1,64,256]{2,1,0:T(8,128)(2,1)}, u32[]{:S(2)}) copy-start(bf16[1,64,256]{2,1,0:T(8,128)(2,1)} %copy-done.14) | copy-start | bytes 98308
  247.4 20.7 %copy-start.19 = (bf16[1,64,256]{2,1,0:T(8,128)(2,1)S(1)}, bf16[1,64,256]{2,1,0:T(8,128)(2,1)}, u32[]{:S(2)}) copy-start(bf16[1,64,256]{2,1,0:T(8,128)(2,1)} %copy-done.17) | copy-start | bytes 98308
  248.5 7.8 %collective-permute-start.23 = (bf16[2,2,64,256]{3,2,1,0:T(8,128)(2,1)S(1)}, bf16[2,2,64,256]{3,2,1,0:T(8,128)(2,1)S(1)}, u32[]{:S(2)}, u32[]{:S(2)}) collective-permute-start(bf16[2,2,64,256]{3,2,1,0:T(8,128)(2,1)S(1)} %slice_reduce_fusion.1), channel_id=1, source_target_pairs={{0,64},{64,0},{128,192},{192,128},{1,65},{65,1},{129,193},{193,129... | collective-permute-start | bytes 393224 | tf_op jit(solution)/shard_map/ppermute | solution.py:38
  256.3 11.7 %collective-permute-start.24 = (bf16[2,64,256]{2,1,0:T(8,128)(2,1)S(1)}, bf16[2,64,256]{2,1,0:T(8,128)(2,1)S(1)}, u32[]{:S(2)}, u32[]{:S(2)}) collective-permute-start(bf16[2,64,256]{2,1,0:T(8,128)(2,1)S(1)} %fusion.6), channel_id=1, source_target_pairs={{0,128},{64,192},{128,0},{192,64},{1,129},{65,193},{129,1},{193,65... | collective-permute-start | bytes 196616 | tf_op jit(solution)/shard_map/ppermute | solution.py:38
  268.1 5.8 %collective-permute-start.25 = (bf16[64,256]{1,0:T(8,128)(2,1)S(1)}, bf16[64,256]{1,0:T(8,128)(2,1)S(1)}, u32[]{:S(2)}, u32[]{:S(2)}) collective-permute-start(bf16[64,256]{1,0:T(8,128)(2,1)S(1)} %select_bitcast_fusion.4), channel_id=1, source_target_pairs={{0,32},{32,0},{1,33},{33,1},{2,34},{34,2},{3,35},{35,3},{4,36},{36... | collective-permute-start | bytes 98312 | tf_op jit(solution)/shard_map/ppermute | solution.py:38
  (4 other events, 2.9 us)

commit v4 on v3

--- a/solution.py
+++ b/solution.py
@@ -42,40 +42,47 @@
     return lax.optimization_barrier((value, *others))[0]
 
 
-def pack_kernel(gain_ref, gate_ref, up_ref, down_ref, gain2_ref, gate2_ref, up2_ref, down2_ref, out_ref, row_ref):
-    sources = (
-        (gain_ref, gate_ref), (gain_ref, up_ref), (None, down_ref),
-        (gain2_ref, gate2_ref), (gain2_ref, up2_ref), (None, down2_ref),
-    )
+def pack_kernel(gain_ref, gain2_ref, *refs):
+    inputs, (out_ref, held_ref, row_ref, sems) = refs[:-4], refs[-4:]
+    copies = [pltpu.make_async_copy(ref, held_ref.at[n], sems.at[n]) for n, ref in enumerate(inputs)]
+    for copy in copies:
+        copy.start()
     shape = (ROWS, ROWS)
     diagonal = lax.broadcasted_iota(jnp.int32, shape, 0) == lax.broadcasted_iota(jnp.int32, shape, 1)
 
     def column(gain):
         return jnp.sum(jnp.where(diagonal, jnp.broadcast_to(gain[...], shape), 0.0), axis=1, keepdims=True)
 
-    gains = {id(gain): column(gain) for gain in (gain_ref, gain2_ref)}
+    first, second = column(gain_ref), column(gain2_ref)
+    gains = (first, first, None, second, second, None)
+    for copy in copies:
+        copy.wait()
     for peer in range(Y * X):
         row = row_ref.at[peer % BUFFERS]
-        for n, (gain, ref) in enumerate(sources):
-            cols = ref[:, peer * PART : (peer + 1) * PART]
-            row[:, n * PART : (n + 1) * PART] = cols if gain is None else gains[id(gain)] * cols
+        for n, gain in enumerate(gains):
+            cols = held_ref[n, :, peer * PART : (peer + 1) * PART]
+            row[:, n * PART : (n + 1) * PART] = cols if gain is None else gain * cols
         out_ref[peer] = row[...].astype(BF16)
 
 
 def packed(layers):
-    arrays = [a for gain, *matrices in layers for a in (gain[None, :], *matrices)]
+    gains = [layer[0][None, :] for layer in layers]
+    matrices = [matrix for layer in layers for matrix in layer[1:]]
     vmem = pl.BlockSpec(memory_space=pltpu.VMEM)
-    width = 3 * len(layers) * PART
+    width = len(matrices) * PART
     return pl.pallas_call(
         pack_kernel,
         out_shape=jax.ShapeDtypeStruct((Y * X, ROWS, width), BF16),
-        in_specs=[vmem] * len(arrays),
+        in_specs=[vmem] * len(gains) + [pl.BlockSpec(memory_space=pl.ANY)] * len(matrices),
         out_specs=vmem,
-        scratch_shapes=[pltpu.VMEM((BUFFERS, ROWS, width), F32)],
+        scratch_shapes=[
+            pltpu.VMEM((len(matrices), *matrices[0].shape), F32),
+            pltpu.VMEM((BUFFERS, ROWS, width), F32),
+            pltpu.SemaphoreType.DMA((len(matrices),)),
+        ],
         cost_estimate=pl.CostEstimate(flops=10**6, bytes_accessed=10**6, transcendentals=0),
-        compiler_params=pltpu.CompilerParams(vmem_limit_bytes=8 * MIB),
         name="pack",
-    )(*arrays)
+    )(*gains, *matrices)
 
 
 def by_block(to_yx):

time: 277 us -> 272 us (0.982)
  local copies, waits for them, and re-layouts: 15.5 us -> 8.79 us
    unnamed x42 -> x26, local copies, waits for them, and re-layouts: 11.5 us -> 4.84 us
  transfers between devices with their start and end apart: 31 -> 31, of which waited for: 17 -> 17; matrix products, arithmetic and copies ran while one was open for 2% -> 2% of each run, Pallas kernels for 4% -> 5%
where the time goes in v4:
time: 272 us; the launch traced here: 270 us
  starting transfers between devices  101 us (37%)
  waiting for transfers between devices  81.4 us (30%)
  blocking collectives  45 us (17%)
  Pallas kernels  25.3 us (9%)
  local copies, waits for them, and re-layouts  8.79 us (3%)
  other arithmetic  6.54 us (2%)
    ppermute x26, starting transfers between devices, from_peer(): return lax.ppermute(block, axis, [(i, i ^ flip) for i in range(size)])  77.6 us
    ppermute x26, waiting for transfers between devices, from_peer(): return lax.ppermute(block, axis, [(i, i ^ flip) for i in range(size)])  63.2 us
    all_to_all x1, blocking collectives, swap(): return lax.all_to_all(blocks, axis, split_axis=0, concat_axis=0, tiled=True)  45 us
    all_to_all x5, starting transfers between devices, swap(): return lax.all_to_all(blocks, axis, split_axis=0, concat_axis=0, tiled=True)  23.8 us
    all_to_all x5, waiting for transfers between devices, swap(): return lax.all_to_all(blocks, axis, split_axis=0, concat_axis=0, tiled=True)  18.2 us
    pallas_call x2, Pallas kernels, half_partial(): pl.pallas_call(half_kernel, out_shape=jax.ShapeDtypeStruct(tokens.shape,...  12.7 us
    pallas_call x2, Pallas kernels, served(): pl.pallas_call(serve_kernel, out_shape=[jax.ShapeDtypeStruct((BLOCK, D),...  9.33 us
  transfers between devices with their start and end apart: 31, of which 17 were waited for; matrix products, arithmetic and copies ran while one was open for 2% of the time, Pallas kernels for 5%

profile of v4, /device:TPU:6, one launch (start us, length us, event | category | flops | bytes accessed | tf_op | source)
XLA Modules:
  0.0 269.6 jit_solution(4421883675805387348)
XLA Ops:
  1.5 3.8 %collective-permute-start = (bf16[64,256]{1,0:T(8,128)(2,1)S(1)}, bf16[64,256]{1,0:T(8,128)(2,1)S(1)}, u32[]{:S(2)}, u32[]{:S(2)}) collective-permute-start(bf16[64,256]{1,0:T(8,128)(2,1)S(1)} %broadcast_select_fusion.1), channel_id=1, source_target_pairs={{0,32},{32,0},{1,33},{33,1},{2,34},{34,2},{3,35},{35,3},{4,36},{36... | collective-permute-start | bytes 98312 | tf_op jit(solution)/shard_map/ppermute | solution.py:38
  5.3 3.2 %pack.1 = bf16[16,32,264]{2,1,0:T(8,128)(2,1)} custom-call(f32[1,32]{1,0:T(1,128)} %bitcast.81, f32[1,32]{1,0:T(1,128)} %bitcast.82, f32[32,704]{1,0:T(8,128)} %refs_0_.1, f32[32,704]{1,0:T(8,128)} %refs_1_.1, f32[32,704]{1,0:T(8,128)} %refs_2_.1, f32[32,704]{1,0:T(8,128)} %refs_3_.1, f32[32,704]{1,0:T(8,128)} %refs_4_.1, f32[32,704]{1,0:T(8,128)} %refs_5_.1), custom_call_target="tpu_custom_call" | custom-call | flops 1000000 | bytes 1000000 | tf_op jit(solution)/shard_map/pack/pallas_call | solution.py:73
  8.5 7.4 %all-to-all-start = ((bf16[16,32,264]{2,1,0:T(8,128)(2,1)}), bf16[16,32,264]{2,1,0:T(8,128)(2,1)S(1)}, u32[]{:S(2)}, u32[]{:S(2)}) async-start(bf16[16,32,264]{2,1,0:T(8,128)(2,1)} %pack.1), calls=%async_computation | async-start | bytes 786432 | tf_op jit(solution)/shard_map/all_to_all | solution.py:30
  16.1 9.1 %collective-permute-start.1 = (bf16[2,64,256]{2,1,0:T(8,128)(2,1)S(1)}, bf16[2,64,256]{2,1,0:T(8,128)(2,1)S(1)}, u32[]{:S(2)}, u32[]{:S(2)}) collective-permute-start(bf16[2,64,256]{2,1,0:T(8,128)(2,1)S(1)} %get-tuple-element.121), channel_id=1, source_target_pairs={{0,128},{64,192},{128,0},{192,64},{1,129},{65,193},{129,1},{193,65... | collective-permute-start | bytes 196616 | tf_op jit(solution)/shard_map/ppermute | solution.py:38
  25.2 5.7 %collective-permute-done.1 = bf16[2,64,256]{2,1,0:T(8,128)(2,1)S(1)} collective-permute-done((bf16[2,64,256]{2,1,0:T(8,128)(2,1)S(1)}, bf16[2,64,256]{2,1,0:T(8,128)(2,1)S(1)}, u32[]{:S(2)}, u32[]{:S(2)}) %collective-permute-start.1) | collective-permute-done | bytes 65568 | tf_op jit(solution)/shard_map/ppermute | solution.py:38
  32.6 45.0 %all_to_all.30 = bf16[8,288,128]{2,1,0:T(8,128)(2,1)S(1)} all-to-all(bf16[8,288,128]{2,1,0:T(8,128)(2,1)S(1)} %bitcast.73), channel_id=1, replica_groups=mesh['gr'=2,'zq'=4,'b'=2,'y'=4,'x'=4,'core'=2] {'gr','zq'}, dimensions={0} | all-to-all | bytes 1179648 | tf_op jit(solution)/shard_map/all_to_all | solution.py:30
  77.6 2.4 collective-permute-start.3
  80.1 8.1 %collective-permute-done.3 = bf16[8,144,128]{2,1,0:T(8,128)(2,1)S(1)} collective-permute-done((bf16[8,144,128]{2,1,0:T(8,128)(2,1)S(1)}, bf16[8,144,128]{2,1,0:T(8,128)(2,1)S(1)}, u32[]{:S(2)}, u32[]{:S(2)}) %collective-permute-start.3) | collective-permute-done | bytes 294944 | tf_op jit(solution)/shard_map/ppermute | solution.py:38
  88.3 1.9 collective-permute-start.7
  90.3 4.8 %collective-permute-start.6 = (bf16[16,144,128]{2,1,0:T(8,128)(2,1)S(1)}, bf16[16,144,128]{2,1,0:T(8,128)(2,1)S(1)}, u32[]{:S(2)}, u32[]{:S(2)}) collective-permute-start(bf16[16,144,128]{2,1,0:T(8,128)(2,1)S(1)} %bitcast.67), channel_id=1, source_target_pairs={{0,4},{2,6},{4,0},{6,2},{1,5},{3,7},{5,1},{7,3},{8,12},{10,14},{12... | collective-permute-start | bytes 1769480 | tf_op jit(solution)/shard_map/ppermute | solution.py:38
  95.1 3.1 %collective-permute-start.5 = (bf16[16,144,128]{2,1,0:T(8,128)(2,1)S(1)}, bf16[16,144,128]{2,1,0:T(8,128)(2,1)}, u32[]{:S(2)}, u32[]{:S(2)}) collective-permute-start(bf16[16,144,128]{2,1,0:T(8,128)(2,1)S(1)} %bitcast.68), channel_id=1, source_target_pairs={{0,2},{2,0},{4,6},{6,4},{1,3},{3,1},{5,7},{7,5},{8,10},{10,8},{12,... | collective-permute-start | bytes 1769480 | tf_op jit(solution)/shard_map/ppermute | solution.py:38
  98.2 3.9 %collective-permute-start.2 = (bf16[2,2,64,256]{3,2,1,0:T(8,128)(2,1)S(1)}, bf16[2,2,64,256]{3,2,1,0:T(8,128)(2,1)S(1)}, u32[]{:S(2)}, u32[]{:S(2)}) collective-permute-start(bf16[2,2,64,256]{3,2,1,0:T(8,128)(2,1)S(1)} %pad_maximum_fusion.4), channel_id=1, source_target_pairs={{0,64},{64,0},{128,192},{192,128},{1,65},{65,1},{129,193},{193,129... | collective-permute-start | bytes 393224 | tf_op jit(solution)/shard_map/ppermute | solution.py:38
  102.1 5.0 %collective-permute-done.2 = bf16[2,2,64,256]{3,2,1,0:T(8,128)(2,1)S(1)} collective-permute-done((bf16[2,2,64,256]{3,2,1,0:T(8,128)(2,1)S(1)}, bf16[2,2,64,256]{3,2,1,0:T(8,128)(2,1)S(1)}, u32[]{:S(2)}, u32[]{:S(2)}) %collective-permute-start.2) | collective-permute-done | bytes 131104 | tf_op jit(solution)/shard_map/ppermute | solution.py:38
  108.2 4.2 %all-to-all-start.2 = ((bf16[4,4,2,64,256]{4,3,2,1,0:T(8,128)(2,1)}), bf16[4,4,2,64,256]{4,3,2,1,0:T(8,128)(2,1)S(1)}, u32[]{:S(2)}, u32[]{:S(2)}) async-start(bf16[4,4,2,64,256]{4,3,2,1,0:T(8,128)(2,1)} %broadcast_in_dim.13), calls=%async_computation.2 | async-start | bytes 2097152 | tf_op jit(solution)/shard_map/all_to_all | solution.py:30
  114.4 1.9 collective-permute-start.8
  120.1 2.4 collective-permute-start.10
  122.5 1.9 collective-permute-start.9
  124.7 2.1 collective-permute-done.9.refs_5_
  126.8 6.6 %half_step.2 = bf16[4,4,2,64,256]{4,3,2,1,0:T(8,128)(2,1)} custom-call(s32[1]{0:T(128)} %bitcast.3.at_ref, bf16[4,4,2,64,256]{4,3,2,1,0:T(8,128)(2,1)S(1)} %all-to-all-done.2.x_ref, bf16[16,144,128]{2,1,0:T(8,128)(2,1)S(1)} %bitcast.70, bf16[16,144,128]{2,1,0:T(8,128)(2,1)} %collective-permute-done.5.refs_1_, ...), custom_call_target="tpu_custom_call" | custom-call | flops 1207959552 | bytes 6815744 | tf_op jit(solution)/shard_map/half_step/pallas_call | solution.py:171
  133.4 4.2 %all-to-all-start.3 = ((bf16[4,4,2,64,256]{4,3,2,1,0:T(8,128)(2,1)}), bf16[4,4,2,64,256]{4,3,2,1,0:T(8,128)(2,1)}, u32[]{:S(2)}, u32[]{:S(2)}) async-start(bf16[4,4,2,64,256]{4,3,2,1,0:T(8,128)(2,1)} %half_step.2), calls=%async_computation.3 | async-start | bytes 2097152 | tf_op jit(solution)/shard_map/all_to_all | solution.py:30
  137.7 2.4 collective-permute-start.16
  140.1 3.1 %collective-permute-start.15 = (bf16[16,144,128]{2,1,0:T(8,128)(2,1)S(1)}, bf16[16,144,128]{2,1,0:T(8,128)(2,1)}, u32[]{:S(2)}, u32[]{:S(2)}) collective-permute-start(bf16[16,144,128]{2,1,0:T(8,128)(2,1)S(1)} %bitcast.61), channel_id=1, source_target_pairs={{0,4},{2,6},{4,0},{6,2},{1,5},{3,7},{5,1},{7,3},{8,12},{10,14},{12... | collective-permute-start | bytes 1769480 | tf_op jit(solution)/shard_map/ppermute | solution.py:38
  143.2 4.3 %collective-permute-start.14 = (bf16[16,144,128]{2,1,0:T(8,128)(2,1)S(1)}, bf16[16,144,128]{2,1,0:T(8,128)(2,1)}, u32[]{:S(2)}, u32[]{:S(2)}) collective-permute-start(bf16[16,144,128]{2,1,0:T(8,128)(2,1)S(1)} %bitcast.62), channel_id=1, source_target_pairs={{0,2},{2,0},{4,6},{6,4},{1,3},{3,1},{5,7},{7,5},{8,10},{10,8},{12,... | collective-permute-start | bytes 1769480 | tf_op jit(solution)/shard_map/ppermute | solution.py:38
  147.5 5.9 %all-to-all-done.3 = bf16[4,4,2,64,256]{4,3,2,1,0:T(8,128)(2,1)} async-done(((bf16[4,4,2,64,256]{4,3,2,1,0:T(8,128)(2,1)}), bf16[4,4,2,64,256]{4,3,2,1,0:T(8,128)(2,1)}, u32[]{:S(2)}, u32[]{:S(2)}) %all-to-all-start.3) | async-done | bytes 1048608 | tf_op jit(solution)/shard_map/all_to_all | solution.py:30
  154.5 3.7 %collective-permute-start.12 = (bf16[2,2,64,256]{3,2,1,0:T(8,128)(2,1)S(1)}, bf16[2,2,64,256]{3,2,1,0:T(8,128)(2,1)S(1)}, u32[]{:S(2)}, u32[]{:S(2)}) collective-permute-start(bf16[2,2,64,256]{3,2,1,0:T(8,128)(2,1)S(1)} %slice_reduce_fusion), channel_id=1, source_target_pairs={{0,64},{64,0},{128,192},{192,128},{1,65},{65,1},{129,193},{193,129... | collective-permute-start | bytes 393224 | tf_op jit(solution)/shard_map/ppermute | solution.py:38
  159.3 5.4 %collective-permute-done.12 = bf16[2,2,64,256]{3,2,1,0:T(8,128)(2,1)S(1)} collective-permute-done((bf16[2,2,64,256]{3,2,1,0:T(8,128)(2,1)S(1)}, bf16[2,2,64,256]{3,2,1,0:T(8,128)(2,1)S(1)}, u32[]{:S(2)}, u32[]{:S(2)}) %collective-permute-start.12) | collective-permute-done | bytes 131104 | tf_op jit(solution)/shard_map/ppermute | solution.py:38
  164.8 3.1 %collective-permute-start.13 = (bf16[2,64,256]{2,1,0:T(8,128)(2,1)S(1)}, bf16[2,64,256]{2,1,0:T(8,128)(2,1)S(1)}, u32[]{:S(2)}, u32[]{:S(2)}) collective-permute-start(bf16[2,64,256]{2,1,0:T(8,128)(2,1)S(1)} %fusion.5), channel_id=1, source_target_pairs={{0,128},{64,192},{128,0},{192,64},{1,129},{65,193},{129,1},{193,65... | collective-permute-start | bytes 196616 | tf_op jit(solution)/shard_map/ppermute | solution.py:38
  168.0 4.9 %serve.2 = (bf16[176,2048]{1,0:T(8,128)(2,1)}, bf16[176,2048]{1,0:T(8,128)(2,1)}, bf16[176,2048]{1,0:T(8,128)(2,1)}) custom-call(s32[3]{0:T(128)S(1)} %pad_add_fusion.at_ref, bf16[16,144,128]{2,1,0:T(8,128)(2,1)S(1)} %bitcast.71, bf16[16,144,128]{2,1,0:T(8,128)(2,1)} %collective-permute-done.5.refs_1_, ...), custom_call_target="tpu_custom_call" | custom-call | flops 100000000 | bytes 6881280 | tf_op jit(solution)/shard_map/serve/pallas_call | solution.py:205
  172.9 3.9 %collective-permute-done.13 = bf16[2,64,256]{2,1,0:T(8,128)(2,1)S(1)} collective-permute-done((bf16[2,64,256]{2,1,0:T(8,128)(2,1)S(1)}, bf16[2,64,256]{2,1,0:T(8,128)(2,1)S(1)}, u32[]{:S(2)}, u32[]{:S(2)}) %collective-permute-start.13) | collective-permute-done | bytes 65568 | tf_op jit(solution)/shard_map/ppermute | solution.py:38
  176.9 2.7 collective-permute-start.17
  179.6 8.2 %collective-permute-done.17 = bf16[2,64,256]{2,1,0:T(8,128)(2,1)S(1)} collective-permute-done((bf16[2,64,256]{2,1,0:T(8,128)(2,1)S(1)}, bf16[2,64,256]{2,1,0:T(8,128)(2,1)S(1)}, u32[]{:S(2)}, u32[]{:S(2)}) %collective-permute-start.17) | collective-permute-done | bytes 65568 | tf_op jit(solution)/shard_map/ppermute | solution.py:38
  187.8 1.9 collective-permute-start.18
  189.7 6.5 %collective-permute-done.18 = bf16[2,2,64,256]{3,2,1,0:T(8,128)(2,1)S(1)} collective-permute-done((bf16[2,2,64,256]{3,2,1,0:T(8,128)(2,1)S(1)}, bf16[2,2,64,256]{3,2,1,0:T(8,128)(2,1)S(1)}, u32[]{:S(2)}, u32[]{:S(2)}) %collective-permute-start.18) | collective-permute-done | bytes 131104 | tf_op jit(solution)/shard_map/ppermute | solution.py:38
  197.4 3.5 %all-to-all-start.4 = ((bf16[4,4,2,64,256]{4,3,2,1,0:T(8,128)(2,1)}), bf16[4,4,2,64,256]{4,3,2,1,0:T(8,128)(2,1)S(1)}, u32[]{:S(2)}, u32[]{:S(2)}) async-start(bf16[4,4,2,64,256]{4,3,2,1,0:T(8,128)(2,1)} %broadcast_in_dim.28), calls=%async_computation.4 | async-start | bytes 2097152 | tf_op jit(solution)/shard_map/all_to_all | solution.py:30
  200.9 1.9 collective-permute-start.19
  202.8 2.4 collective-permute-start.20
  207.1 2.4 collective-permute-start.22
  212.0 3.7 %all-to-all-done.4.x_ref = bf16[4,4,2,64,256]{4,3,2,1,0:T(8,128)(2,1)S(1)} async-done(((bf16[4,4,2,64,256]{4,3,2,1,0:T(8,128)(2,1)}), bf16[4,4,2,64,256]{4,3,2,1,0:T(8,128)(2,1)S(1)}, u32[]{:S(2)}, u32[]{:S(2)}) %all-to-all-start.4) | async-done | bytes 1048608 | tf_op jit(solution)/shard_map/all_to_all | solution.py:30
  217.9 6.1 %half_step.3 = bf16[4,4,2,64,256]{4,3,2,1,0:T(8,128)(2,1)} custom-call(s32[1]{0:T(128)} %bitcast.3.at_ref, bf16[4,4,2,64,256]{4,3,2,1,0:T(8,128)(2,1)S(1)} %all-to-all-done.4.x_ref, bf16[16,144,128]{2,1,0:T(8,128)(2,1)S(1)} %bitcast.64, bf16[16,144,128]{2,1,0:T(8,128)(2,1)} %collective-permute-done.14.refs_1_, ...), custom_call_target="tpu_custom_call" | custom-call | flops 1207959552 | bytes 6815744 | tf_op jit(solution)/shard_map/half_step/pallas_call | solution.py:171
  224.0 4.4 %all-to-all-start.5 = ((bf16[4,4,2,64,256]{4,3,2,1,0:T(8,128)(2,1)}), bf16[4,4,2,64,256]{4,3,2,1,0:T(8,128)(2,1)}, u32[]{:S(2)}, u32[]{:S(2)}) async-start(bf16[4,4,2,64,256]{4,3,2,1,0:T(8,128)(2,1)} %half_step.3), calls=%async_computation.5 | async-start | bytes 2097152 | tf_op jit(solution)/shard_map/all_to_all | solution.py:30
  229.4 4.5 %serve.3 = (bf16[176,2048]{1,0:T(8,128)(2,1)}, bf16[176,2048]{1,0:T(8,128)(2,1)}, bf16[176,2048]{1,0:T(8,128)(2,1)}) custom-call(s32[3]{0:T(128)S(1)} %pad_add_fusion.at_ref, bf16[16,144,128]{2,1,0:T(8,128)(2,1)S(1)} %bitcast.65, bf16[16,144,128]{2,1,0:T(8,128)(2,1)} %collective-permute-done.14.refs_1_, ...), custom_call_target="tpu_custom_call" | custom-call | flops 100000000 | bytes 6881280 | tf_op jit(solution)/shard_map/serve/pallas_call | solution.py:205
  233.9 8.5 %all-to-all-done.5 = bf16[4,4,2,64,256]{4,3,2,1,0:T(8,128)(2,1)} async-done(((bf16[4,4,2,64,256]{4,3,2,1,0:T(8,128)(2,1)}), bf16[4,4,2,64,256]{4,3,2,1,0:T(8,128)(2,1)}, u32[]{:S(2)}, u32[]{:S(2)}) %all-to-all-start.5) | async-done | bytes 1048608 | tf_op jit(solution)/shard_map/all_to_all | solution.py:30
  243.6 1.9 collective-permute-start.23
  246.6 4.7 %collective-permute-done.23 = bf16[2,2,64,256]{3,2,1,0:T(8,128)(2,1)S(1)} collective-permute-done((bf16[2,2,64,256]{3,2,1,0:T(8,128)(2,1)S(1)}, bf16[2,2,64,256]{3,2,1,0:T(8,128)(2,1)S(1)}, u32[]{:S(2)}, u32[]{:S(2)}) %collective-permute-start.23) | collective-permute-done | bytes 131104 | tf_op jit(solution)/shard_map/ppermute | solution.py:38
  251.4 4.7 %collective-permute-start.24 = (bf16[2,64,256]{2,1,0:T(8,128)(2,1)S(1)}, bf16[2,64,256]{2,1,0:T(8,128)(2,1)S(1)}, u32[]{:S(2)}, u32[]{:S(2)}) collective-permute-start(bf16[2,64,256]{2,1,0:T(8,128)(2,1)S(1)} %fusion.6), channel_id=1, source_target_pairs={{0,128},{64,192},{128,0},{192,64},{1,129},{65,193},{129,1},{193,65... | collective-permute-start | bytes 196616 | tf_op jit(solution)/shard_map/ppermute | solution.py:38
  256.1 7.0 %collective-permute-done.24 = bf16[2,64,256]{2,1,0:T(8,128)(2,1)S(1)} collective-permute-done((bf16[2,64,256]{2,1,0:T(8,128)(2,1)S(1)}, bf16[2,64,256]{2,1,0:T(8,128)(2,1)S(1)}, u32[]{:S(2)}, u32[]{:S(2)}) %collective-permute-start.24) | collective-permute-done | bytes 65568 | tf_op jit(solution)/shard_map/ppermute | solution.py:38
  263.2 1.9 collective-permute-start.25
  265.1 3.9 %collective-permute-done.25 = bf16[64,256]{1,0:T(8,128)(2,1)S(1)} collective-permute-done((bf16[64,256]{1,0:T(8,128)(2,1)S(1)}, bf16[64,256]{1,0:T(8,128)(2,1)S(1)}, u32[]{:S(2)}, u32[]{:S(2)}) %collective-permute-start.25) | collective-permute-done | bytes 32800 | tf_op jit(solution)/shard_map/ppermute | solution.py:38
  (82 shorter events, 23.8 us)
Async XLA Ops:
  0.6 15.4 %copy-start.12 = (bf16[512,64]{0,1:T(8,128)(2,1)S(1)}, bf16[512,64]{0,1:T(8,128)(2,1)}, u32[]{:S(2)}) copy-start(bf16[512,64]{0,1:T(8,128)(2,1)} %param.9) | copy-start | bytes 196612
  1.5 14.5 %collective-permute-start = (bf16[64,256]{1,0:T(8,128)(2,1)S(1)}, bf16[64,256]{1,0:T(8,128)(2,1)S(1)}, u32[]{:S(2)}, u32[]{:S(2)}) collective-permute-start(bf16[64,256]{1,0:T(8,128)(2,1)S(1)} %broadcast_select_fusion.1), channel_id=1, source_target_pairs={{0,32},{32,0},{1,33},{33,1},{2,34},{34,2},{3,35},{35,3},{4,36},{36... | collective-permute-start | bytes 98312 | tf_op jit(solution)/shard_map/ppermute | solution.py:38
  8.5 22.4 %all-to-all-start = ((bf16[16,32,264]{2,1,0:T(8,128)(2,1)}), bf16[16,32,264]{2,1,0:T(8,128)(2,1)S(1)}, u32[]{:S(2)}, u32[]{:S(2)}) async-start(bf16[16,32,264]{2,1,0:T(8,128)(2,1)} %pack.1), calls=%async_computation | async-start | bytes 786432 | tf_op jit(solution)/shard_map/all_to_all | solution.py:30
  16.0 14.9 %copy-start.6 = (bf16[1,64,256]{2,1,0:T(8,128)(2,1)}, bf16[1,64,256]{2,1,0:T(8,128)(2,1)S(1)}, u32[]{:S(2)}) copy-start(bf16[1,64,256]{2,1,0:T(8,128)(2,1)S(1)} %get-tuple-element.118) | copy-start | bytes 98308
  16.0 14.9 %copy-start.9 = (bf16[1,64,256]{2,1,0:T(8,128)(2,1)}, bf16[1,64,256]{2,1,0:T(8,128)(2,1)S(1)}, u32[]{:S(2)}) copy-start(bf16[1,64,256]{2,1,0:T(8,128)(2,1)S(1)} %get-tuple-element.119) | copy-start | bytes 98308
  16.1 14.8 %collective-permute-start.1 = (bf16[2,64,256]{2,1,0:T(8,128)(2,1)S(1)}, bf16[2,64,256]{2,1,0:T(8,128)(2,1)S(1)}, u32[]{:S(2)}, u32[]{:S(2)}) collective-permute-start(bf16[2,64,256]{2,1,0:T(8,128)(2,1)S(1)} %get-tuple-element.121), channel_id=1, source_target_pairs={{0,128},{64,192},{128,0},{192,64},{1,129},{65,193},{129,1},{193,65... | collective-permute-start | bytes 196616 | tf_op jit(solution)/shard_map/ppermute | solution.py:38
  77.6 10.5 %collective-permute-start.3 = (bf16[8,144,128]{2,1,0:T(8,128)(2,1)S(1)}, bf16[8,144,128]{2,1,0:T(8,128)(2,1)S(1)}, u32[]{:S(2)}, u32[]{:S(2)}) collective-permute-start(bf16[8,144,128]{2,1,0:T(8,128)(2,1)S(1)} %slice.60), channel_id=1, source_target_pairs={{0,32},{32,0},{1,33},{33,1},{2,34},{34,2},{3,35},{35,3},{4,36},{36... | collective-permute-start | bytes 884744 | tf_op jit(solution)/shard_map/ppermute | solution.py:38
  88.3 29.8 %collective-permute-start.7 = (bf16[16,144,128]{2,1,0:T(8,128)(2,1)S(1)}, bf16[16,144,128]{2,1,0:T(8,128)(2,1)S(1)}, u32[]{:S(2)}, u32[]{:S(2)}) collective-permute-start(bf16[16,144,128]{2,1,0:T(8,128)(2,1)S(1)} %bitcast.66), channel_id=1, source_target_pairs={{0,6},{2,4},{4,2},{6,0},{1,7},{3,5},{5,3},{7,1},{8,14},{10,12},{12... | collective-permute-start | bytes 1769480 | tf_op jit(solution)/shard_map/ppermute | solution.py:38
  90.3 29.8 %collective-permute-start.6 = (bf16[16,144,128]{2,1,0:T(8,128)(2,1)S(1)}, bf16[16,144,128]{2,1,0:T(8,128)(2,1)S(1)}, u32[]{:S(2)}, u32[]{:S(2)}) collective-permute-start(bf16[16,144,128]{2,1,0:T(8,128)(2,1)S(1)} %bitcast.67), channel_id=1, source_target_pairs={{0,4},{2,6},{4,0},{6,2},{1,5},{3,7},{5,1},{7,3},{8,12},{10,14},{12... | collective-permute-start | bytes 1769480 | tf_op jit(solution)/shard_map/ppermute | solution.py:38
  95.1 27.4 %collective-permute-start.5 = (bf16[16,144,128]{2,1,0:T(8,128)(2,1)S(1)}, bf16[16,144,128]{2,1,0:T(8,128)(2,1)}, u32[]{:S(2)}, u32[]{:S(2)}) collective-permute-start(bf16[16,144,128]{2,1,0:T(8,128)(2,1)S(1)} %bitcast.68), channel_id=1, source_target_pairs={{0,2},{2,0},{4,6},{6,4},{1,3},{3,1},{5,7},{7,5},{8,10},{10,8},{12,... | collective-permute-start | bytes 1769480 | tf_op jit(solution)/shard_map/ppermute | solution.py:38
  98.2 8.9 %collective-permute-start.2 = (bf16[2,2,64,256]{3,2,1,0:T(8,128)(2,1)S(1)}, bf16[2,2,64,256]{3,2,1,0:T(8,128)(2,1)S(1)}, u32[]{:S(2)}, u32[]{:S(2)}) collective-permute-start(bf16[2,2,64,256]{3,2,1,0:T(8,128)(2,1)S(1)} %pad_maximum_fusion.4), channel_id=1, source_target_pairs={{0,64},{64,0},{128,192},{192,128},{1,65},{65,1},{129,193},{193,129... | collective-permute-start | bytes 393224 | tf_op jit(solution)/shard_map/ppermute | solution.py:38
  108.2 16.5 %all-to-all-start.2 = ((bf16[4,4,2,64,256]{4,3,2,1,0:T(8,128)(2,1)}), bf16[4,4,2,64,256]{4,3,2,1,0:T(8,128)(2,1)S(1)}, u32[]{:S(2)}, u32[]{:S(2)}) async-start(bf16[4,4,2,64,256]{4,3,2,1,0:T(8,128)(2,1)} %broadcast_in_dim.13), calls=%async_computation.2 | async-start | bytes 2097152 | tf_op jit(solution)/shard_map/all_to_all | solution.py:30
  112.5 12.0 %collective-permute-start.4 = (bf16[8,144,128]{2,1,0:T(8,128)(2,1)S(1)}, bf16[8,144,128]{2,1,0:T(8,128)(2,1)S(1)}, u32[]{:S(2)}, u32[]{:S(2)}) collective-permute-start(bf16[8,144,128]{2,1,0:T(8,128)(2,1)S(1)} %get-tuple-element.62), channel_id=1, source_target_pairs={{0,32},{32,0},{1,33},{33,1},{2,34},{34,2},{3,35},{35,3},{4,36},{36... | collective-permute-start | bytes 884744 | tf_op jit(solution)/shard_map/ppermute | solution.py:38
  114.4 10.2 %collective-permute-start.8 = (bf16[16,144,128]{2,1,0:T(8,128)(2,1)S(1)}, bf16[16,144,128]{2,1,0:T(8,128)(2,1)}, u32[]{:S(2)}, u32[]{:S(2)}) collective-permute-start(bf16[16,144,128]{2,1,0:T(8,128)(2,1)S(1)} %bitcast.69), channel_id=1, source_target_pairs={{0,1},{1,0},{2,3},{3,2},{4,5},{5,4},{6,7},{7,6},{8,9},{9,8},{10,11... | collective-permute-start | bytes 1769480 | tf_op jit(solution)/shard_map/ppermute | solution.py:38
  118.2 6.5 %collective-permute-start.11 = (bf16[16,144,128]{2,1,0:T(8,128)(2,1)S(1)}, bf16[16,144,128]{2,1,0:T(8,128)(2,1)}, u32[]{:S(2)}, u32[]{:S(2)}) collective-permute-start(bf16[16,144,128]{2,1,0:T(8,128)(2,1)S(1)} %collective-permute-done.7.refs_3_), channel_id=1, source_target_pairs={{0,1},{1,0},{2,3},{3,2},{4,5},{5,4},{6,7},{7,6},{8,9},{9,8},{10,11... | collective-permute-start | bytes 1769480 | tf_op jit(solution)/shard_map/ppermute | solution.py:38
  120.1 4.6 %collective-permute-start.10 = (bf16[16,144,128]{2,1,0:T(8,128)(2,1)S(1)}, bf16[16,144,128]{2,1,0:T(8,128)(2,1)}, u32[]{:S(2)}, u32[]{:S(2)}) collective-permute-start(bf16[16,144,128]{2,1,0:T(8,128)(2,1)S(1)} %collective-permute-done.6.refs_2_), channel_id=1, source_target_pairs={{0,1},{1,0},{2,3},{3,2},{4,5},{5,4},{6,7},{7,6},{8,9},{9,8},{10,11... | collective-permute-start | bytes 1769480 | tf_op jit(solution)/shard_map/ppermute | solution.py:38
  122.5 4.2 %collective-permute-start.9 = (bf16[16,144,128]{2,1,0:T(8,128)(2,1)}, bf16[16,144,128]{2,1,0:T(8,128)(2,1)}, u32[]{:S(2)}, u32[]{:S(2)}) collective-permute-start(bf16[16,144,128]{2,1,0:T(8,128)(2,1)} %collective-permute-done.5.refs_1_), channel_id=1, source_target_pairs={{0,1},{1,0},{2,3},{3,2},{4,5},{5,4},{6,7},{7,6},{8,9},{9,8},{10,11... | collective-permute-start | bytes 1769480 | tf_op jit(solution)/shard_map/ppermute | solution.py:38
  133.4 20.0 %all-to-all-start.3 = ((bf16[4,4,2,64,256]{4,3,2,1,0:T(8,128)(2,1)}), bf16[4,4,2,64,256]{4,3,2,1,0:T(8,128)(2,1)}, u32[]{:S(2)}, u32[]{:S(2)}) async-start(bf16[4,4,2,64,256]{4,3,2,1,0:T(8,128)(2,1)} %half_step.2), calls=%async_computation.3 | async-start | bytes 2097152 | tf_op jit(solution)/shard_map/all_to_all | solution.py:30
  137.7 39.2 %collective-permute-start.16 = (bf16[16,144,128]{2,1,0:T(8,128)(2,1)S(1)}, bf16[16,144,128]{2,1,0:T(8,128)(2,1)S(1)}, u32[]{:S(2)}, u32[]{:S(2)}) collective-permute-start(bf16[16,144,128]{2,1,0:T(8,128)(2,1)S(1)} %bitcast.60), channel_id=1, source_target_pairs={{0,6},{2,4},{4,2},{6,0},{1,7},{3,5},{5,3},{7,1},{8,14},{10,12},{12... | collective-permute-start | bytes 1769480 | tf_op jit(solution)/shard_map/ppermute | solution.py:38
  140.1 36.7 %collective-permute-start.15 = (bf16[16,144,128]{2,1,0:T(8,128)(2,1)S(1)}, bf16[16,144,128]{2,1,0:T(8,128)(2,1)}, u32[]{:S(2)}, u32[]{:S(2)}) collective-permute-start(bf16[16,144,128]{2,1,0:T(8,128)(2,1)S(1)} %bitcast.61), channel_id=1, source_target_pairs={{0,4},{2,6},{4,0},{6,2},{1,5},{3,7},{5,1},{7,3},{8,12},{10,14},{12... | collective-permute-start | bytes 1769480 | tf_op jit(solution)/shard_map/ppermute | solution.py:38
  143.2 33.6 %collective-permute-start.14 = (bf16[16,144,128]{2,1,0:T(8,128)(2,1)S(1)}, bf16[16,144,128]{2,1,0:T(8,128)(2,1)}, u32[]{:S(2)}, u32[]{:S(2)}) collective-permute-start(bf16[16,144,128]{2,1,0:T(8,128)(2,1)S(1)} %bitcast.62), channel_id=1, source_target_pairs={{0,2},{2,0},{4,6},{6,4},{1,3},{3,1},{5,7},{7,5},{8,10},{10,8},{12,... | collective-permute-start | bytes 1769480 | tf_op jit(solution)/shard_map/ppermute | solution.py:38
  154.5 10.2 %collective-permute-start.12 = (bf16[2,2,64,256]{3,2,1,0:T(8,128)(2,1)S(1)}, bf16[2,2,64,256]{3,2,1,0:T(8,128)(2,1)S(1)}, u32[]{:S(2)}, u32[]{:S(2)}) collective-permute-start(bf16[2,2,64,256]{3,2,1,0:T(8,128)(2,1)S(1)} %slice_reduce_fusion), channel_id=1, source_target_pairs={{0,64},{64,0},{128,192},{192,128},{1,65},{65,1},{129,193},{193,129... | collective-permute-start | bytes 393224 | tf_op jit(solution)/shard_map/ppermute | solution.py:38
  164.8 12.0 %collective-permute-start.13 = (bf16[2,64,256]{2,1,0:T(8,128)(2,1)S(1)}, bf16[2,64,256]{2,1,0:T(8,128)(2,1)S(1)}, u32[]{:S(2)}, u32[]{:S(2)}) collective-permute-start(bf16[2,64,256]{2,1,0:T(8,128)(2,1)S(1)} %fusion.5), channel_id=1, source_target_pairs={{0,128},{64,192},{128,0},{192,64},{1,129},{65,193},{129,1},{193,65... | collective-permute-start | bytes 196616 | tf_op jit(solution)/shard_map/ppermute | solution.py:38
  168.0 8.8 %copy-start.7 = (bf16[1,64,256]{2,1,0:T(8,128)(2,1)S(1)}, bf16[1,64,256]{2,1,0:T(8,128)(2,1)}, u32[]{:S(2)}) copy-start(bf16[1,64,256]{2,1,0:T(8,128)(2,1)} %copy-done.6) | copy-start | bytes 98308
  168.0 8.8 %copy-start.10 = (bf16[1,64,256]{2,1,0:T(8,128)(2,1)S(1)}, bf16[1,64,256]{2,1,0:T(8,128)(2,1)}, u32[]{:S(2)}) copy-start(bf16[1,64,256]{2,1,0:T(8,128)(2,1)} %copy-done.9) | copy-start | bytes 98308
  176.9 10.9 %collective-permute-start.17 = (bf16[2,64,256]{2,1,0:T(8,128)(2,1)S(1)}, bf16[2,64,256]{2,1,0:T(8,128)(2,1)S(1)}, u32[]{:S(2)}, u32[]{:S(2)}) collective-permute-start(bf16[2,64,256]{2,1,0:T(8,128)(2,1)S(1)} %add_convert_fusion), channel_id=1, source_target_pairs={{0,128},{64,192},{128,0},{192,64},{1,129},{65,193},{129,1},{193,65... | collective-permute-start | bytes 196616 | tf_op jit(solution)/shard_map/ppermute | solution.py:38
  187.8 8.4 %collective-permute-start.18 = (bf16[2,2,64,256]{3,2,1,0:T(8,128)(2,1)S(1)}, bf16[2,2,64,256]{3,2,1,0:T(8,128)(2,1)S(1)}, u32[]{:S(2)}, u32[]{:S(2)}) collective-permute-start(bf16[2,2,64,256]{3,2,1,0:T(8,128)(2,1)S(1)} %pad_maximum_fusion.5), channel_id=1, source_target_pairs={{0,64},{64,0},{128,192},{192,128},{1,65},{65,1},{129,193},{193,129... | collective-permute-start | bytes 393224 | tf_op jit(solution)/shard_map/ppermute | solution.py:38
  197.4 18.4 %all-to-all-start.4 = ((bf16[4,4,2,64,256]{4,3,2,1,0:T(8,128)(2,1)}), bf16[4,4,2,64,256]{4,3,2,1,0:T(8,128)(2,1)S(1)}, u32[]{:S(2)}, u32[]{:S(2)}) async-start(bf16[4,4,2,64,256]{4,3,2,1,0:T(8,128)(2,1)} %broadcast_in_dim.28), calls=%async_computation.4 | async-start | bytes 2097152 | tf_op jit(solution)/shard_map/all_to_all | solution.py:30
  200.9 8.7 %collective-permute-start.19 = (bf16[16,144,128]{2,1,0:T(8,128)(2,1)S(1)}, bf16[16,144,128]{2,1,0:T(8,128)(2,1)S(1)}, u32[]{:S(2)}, u32[]{:S(2)}) collective-permute-start(bf16[16,144,128]{2,1,0:T(8,128)(2,1)S(1)} %bitcast.63), channel_id=1, source_target_pairs={{0,1},{1,0},{2,3},{3,2},{4,5},{5,4},{6,7},{7,6},{8,9},{9,8},{10,11... | collective-permute-start | bytes 1769480 | tf_op jit(solution)/shard_map/ppermute | solution.py:38
  202.8 6.8 %collective-permute-start.20 = (bf16[16,144,128]{2,1,0:T(8,128)(2,1)}, bf16[16,144,128]{2,1,0:T(8,128)(2,1)S(1)}, u32[]{:S(2)}, u32[]{:S(2)}) collective-permute-start(bf16[16,144,128]{2,1,0:T(8,128)(2,1)} %collective-permute-done.14.refs_1_), channel_id=1, source_target_pairs={{0,1},{1,0},{2,3},{3,2},{4,5},{5,4},{6,7},{7,6},{8,9},{9,8},{10,11... | collective-permute-start | bytes 1769480 | tf_op jit(solution)/shard_map/ppermute | solution.py:38
  205.2 4.4 %collective-permute-start.21 = (bf16[16,144,128]{2,1,0:T(8,128)(2,1)}, bf16[16,144,128]{2,1,0:T(8,128)(2,1)S(1)}, u32[]{:S(2)}, u32[]{:S(2)}) collective-permute-start(bf16[16,144,128]{2,1,0:T(8,128)(2,1)} %collective-permute-done.15.refs_2_), channel_id=1, source_target_pairs={{0,1},{1,0},{2,3},{3,2},{4,5},{5,4},{6,7},{7,6},{8,9},{9,8},{10,11... | collective-permute-start | bytes 1769480 | tf_op jit(solution)/shard_map/ppermute | solution.py:38
  207.1 4.0 %collective-permute-start.22 = (bf16[16,144,128]{2,1,0:T(8,128)(2,1)S(1)}, bf16[16,144,128]{2,1,0:T(8,128)(2,1)S(1)}, u32[]{:S(2)}, u32[]{:S(2)}) collective-permute-start(bf16[16,144,128]{2,1,0:T(8,128)(2,1)S(1)} %collective-permute-done.16.refs_3_), channel_id=1, source_target_pairs={{0,1},{1,0},{2,3},{3,2},{4,5},{5,4},{6,7},{7,6},{8,9},{9,8},{10,11... | collective-permute-start | bytes 1769480 | tf_op jit(solution)/shard_map/ppermute | solution.py:38
  209.6 0.8 copy-start
  211.2 0.8 copy-start.3
  215.7 1.1 copy-start.1
  216.8 1.1 copy-start.4
  224.0 4.4 %copy-start.2 = (bf16[16,144,128]{2,1,0:T(8,128)(2,1)S(1)}, bf16[16,144,128]{2,1,0:T(8,128)(2,1)}, u32[]{:S(2)}) copy-start(bf16[16,144,128]{2,1,0:T(8,128)(2,1)} %copy-done) | copy-start | bytes 1769476
  224.0 18.5 %all-to-all-start.5 = ((bf16[4,4,2,64,256]{4,3,2,1,0:T(8,128)(2,1)}), bf16[4,4,2,64,256]{4,3,2,1,0:T(8,128)(2,1)}, u32[]{:S(2)}, u32[]{:S(2)}) async-start(bf16[4,4,2,64,256]{4,3,2,1,0:T(8,128)(2,1)} %half_step.3), calls=%async_computation.5 | async-start | bytes 2097152 | tf_op jit(solution)/shard_map/all_to_all | solution.py:30
  228.4 1.1 copy-start.5
  242.4 20.7 %copy-start.8 = (bf16[1,64,256]{2,1,0:T(8,128)(2,1)S(1)}, bf16[1,64,256]{2,1,0:T(8,128)(2,1)}, u32[]{:S(2)}) copy-start(bf16[1,64,256]{2,1,0:T(8,128)(2,1)} %copy-done.6) | copy-start | bytes 98308
  242.4 20.7 %copy-start.11 = (bf16[1,64,256]{2,1,0:T(8,128)(2,1)S(1)}, bf16[1,64,256]{2,1,0:T(8,128)(2,1)}, u32[]{:S(2)}) copy-start(bf16[1,64,256]{2,1,0:T(8,128)(2,1)} %copy-done.9) | copy-start | bytes 98308
  243.6 7.8 %collective-permute-start.23 = (bf16[2,2,64,256]{3,2,1,0:T(8,128)(2,1)S(1)}, bf16[2,2,64,256]{3,2,1,0:T(8,128)(2,1)S(1)}, u32[]{:S(2)}, u32[]{:S(2)}) collective-permute-start(bf16[2,2,64,256]{3,2,1,0:T(8,128)(2,1)S(1)} %slice_reduce_fusion.1), channel_id=1, source_target_pairs={{0,64},{64,0},{128,192},{192,128},{1,65},{65,1},{129,193},{193,129... | collective-permute-start | bytes 393224 | tf_op jit(solution)/shard_map/ppermute | solution.py:38
  251.4 11.7 %collective-permute-start.24 = (bf16[2,64,256]{2,1,0:T(8,128)(2,1)S(1)}, bf16[2,64,256]{2,1,0:T(8,128)(2,1)S(1)}, u32[]{:S(2)}, u32[]{:S(2)}) collective-permute-start(bf16[2,64,256]{2,1,0:T(8,128)(2,1)S(1)} %fusion.6), channel_id=1, source_target_pairs={{0,128},{64,192},{128,0},{192,64},{1,129},{65,193},{129,1},{193,65... | collective-permute-start | bytes 196616 | tf_op jit(solution)/shard_map/ppermute | solution.py:38
  263.2 5.8 %collective-permute-start.25 = (bf16[64,256]{1,0:T(8,128)(2,1)S(1)}, bf16[64,256]{1,0:T(8,128)(2,1)S(1)}, u32[]{:S(2)}, u32[]{:S(2)}) collective-permute-start(bf16[64,256]{1,0:T(8,128)(2,1)S(1)} %select_bitcast_fusion.4), channel_id=1, source_target_pairs={{0,32},{32,0},{1,33},{33,1},{2,34},{34,2},{3,35},{35,3},{4,36},{36... | collective-permute-start | bytes 98312 | tf_op jit(solution)/shard_map/ppermute | solution.py:38

commit v5 on v4

--- a/solution.py
+++ b/solution.py
@@ -239,11 +239,21 @@
     return jnp.concatenate([two, from_peer(two, "zq", ZQ, 1)])
 
 
-def summed(by_y):
+def kept_half(by_y):
     send = jnp.sum(by_y[:, ZQ // 2 :].astype(F32), axis=0).astype(BF16)
     got = from_peer(send, "zq", ZQ, 1)
-    kept = jnp.sum(by_y[:, : ZQ // 2].astype(F32), axis=0) + got.astype(F32)
+    return jnp.sum(by_y[:, : ZQ // 2].astype(F32), axis=0) + got.astype(F32)
+
+
+def summed(by_y):
+    kept = kept_half(by_y)
     return kept[0] + from_peer(kept[1].astype(BF16), "zq", ZQ, 2).astype(F32)
+
+
+def summed_twice(by_y):
+    kept = kept_half(by_y).astype(BF16)
+    got = from_peer(kept, "zq", ZQ, 2)
+    return kept.astype(F32) + got[::-1].astype(F32)
 
 
 def stepped(tokens, total):
@@ -257,9 +267,9 @@
         packed([(gain_pre, gate_pre, up_pre, down_pre), (gain_post, gate_post, up_post, down_post)])
     )
     tokens = jnp.stack(traded(turned[:, :half], turned[:, half:]))
-    parts, wide = lax.optimization_barrier((parts, far_zq(tokens)))
+    parts, two_away = lax.optimization_barrier((parts, far_zq(tokens)))
     one, two = by_span(parts)
-    wide = after(wide, one)
+    wide = after(two_away, one)
     one = paired(one)
     wide = near_zq(wide)
     pieces = over_x(one)
@@ -272,16 +282,16 @@
     first = served(pieces)
     pieces = over_x(two)
     by_y = swap(partial, "y")
-    total, *first = lax.optimization_barrier((summed(by_y), *first))
+    total, *first = lax.optimization_barrier((summed_twice(by_y), *first))
     total, *pieces = lax.optimization_barrier((total, *pieces))
-    middle = stepped(tokens, total)
+    middle = stepped(two_away, total)
     pieces += over_core(pieces)
 
-    partial = half_partial(share(near_zq(far_zq(middle)), "y", Y), pieces)
+    partial = half_partial(share(near_zq(middle), "y", Y), pieces)
     partial, *pieces = lax.optimization_barrier((partial, *pieces))
     second = served(pieces)
     by_y, *second = lax.optimization_barrier((swap(partial, "y"), *second))
-    result = stepped(middle, summed(by_y))
+    result = stepped(middle[0], summed(by_y))
     back = jnp.concatenate(traded(result[0], result[1]), axis=1)
     return (back.T, *first, *second)
 

time: 272 us -> 264 us (0.971)
  waiting for transfers between devices: 81.4 us -> 75.2 us
    ppermute x26 -> x25, waiting for transfers between devices: 63.2 us -> 57.4 us  [from_peer(): return lax.ppermute(block, axis, [(i, i ^ flip) for i in range(size)])]
    ppermute x26 -> x25, starting transfers between devices: 77.6 us -> 76.3 us  [from_peer(): return lax.ppermute(block, axis, [(i, i ^ flip) for i in range(size)])]
  transfers between devices with their start and end apart: 31 -> 30, of which waited for: 17 -> 16; matrix products, arithmetic and copies ran while one was open for 2% -> 2% of each run, Pallas kernels for 5% -> 5%
where the time goes in v5:
time: 264 us; the launch traced here: 262 us
  starting transfers between devices  100 us (38%)
  waiting for transfers between devices  75.2 us (28%)
  blocking collectives  45 us (17%)
  Pallas kernels  25.3 us (10%)
  local copies, waits for them, and re-layouts  8.76 us (3%)
  other arithmetic  6.56 us (2%)
    ppermute x25, starting transfers between devices, from_peer(): return lax.ppermute(block, axis, [(i, i ^ flip) for i in range(size)])  76.3 us
    ppermute x25, waiting for transfers between devices, from_peer(): return lax.ppermute(block, axis, [(i, i ^ flip) for i in range(size)])  57.4 us
    all_to_all x1, blocking collectives, swap(): return lax.all_to_all(blocks, axis, split_axis=0, concat_axis=0, tiled=True)  45 us
    all_to_all x5, starting transfers between devices, swap(): return lax.all_to_all(blocks, axis, split_axis=0, concat_axis=0, tiled=True)  23.8 us
    all_to_all x5, waiting for transfers between devices, swap(): return lax.all_to_all(blocks, axis, split_axis=0, concat_axis=0, tiled=True)  17.8 us
    pallas_call x2, Pallas kernels, half_partial(): pl.pallas_call(half_kernel, out_shape=jax.ShapeDtypeStruct(tokens.shape,...  12.7 us
    pallas_call x2, Pallas kernels, served(): pl.pallas_call(serve_kernel, out_shape=[jax.ShapeDtypeStruct((BLOCK, D),...  9.33 us
  transfers between devices with their start and end apart: 30, of which 16 were waited for; matrix products, arithmetic and copies ran while one was open for 2% of the time, Pallas kernels for 5%

profile of v5, /device:TPU:6, one launch (start us, length us, event | category | flops | bytes accessed | tf_op | source)
XLA Modules:
  0.0 262.1 jit_solution(3936727877578499332)
XLA Ops:
  1.5 3.8 %collective-permute-start = (bf16[64,256]{1,0:T(8,128)(2,1)S(1)}, bf16[64,256]{1,0:T(8,128)(2,1)S(1)}, u32[]{:S(2)}, u32[]{:S(2)}) collective-permute-start(bf16[64,256]{1,0:T(8,128)(2,1)S(1)} %broadcast_select_fusion.1), channel_id=1, source_target_pairs={{0,32},{32,0},{1,33},{33,1},{2,34},{34,2},{3,35},{35,3},{4,36},{36... | collective-permute-start | bytes 98312 | tf_op jit(solution)/shard_map/ppermute | solution.py:38
  5.3 3.2 %pack.1 = bf16[16,32,264]{2,1,0:T(8,128)(2,1)} custom-call(f32[1,32]{1,0:T(1,128)} %bitcast.75, f32[1,32]{1,0:T(1,128)} %bitcast.76, f32[32,704]{1,0:T(8,128)} %refs_0_.1, f32[32,704]{1,0:T(8,128)} %refs_1_.1, f32[32,704]{1,0:T(8,128)} %refs_2_.1, f32[32,704]{1,0:T(8,128)} %refs_3_.1, f32[32,704]{1,0:T(8,128)} %refs_4_.1, f32[32,704]{1,0:T(8,128)} %refs_5_.1), custom_call_target="tpu_custom_call" | custom-call | flops 1000000 | bytes 1000000 | tf_op jit(solution)/shard_map/pack/pallas_call | solution.py:73
  8.5 7.4 %all-to-all-start = ((bf16[16,32,264]{2,1,0:T(8,128)(2,1)}), bf16[16,32,264]{2,1,0:T(8,128)(2,1)S(1)}, u32[]{:S(2)}, u32[]{:S(2)}) async-start(bf16[16,32,264]{2,1,0:T(8,128)(2,1)} %pack.1), calls=%async_computation | async-start | bytes 786432 | tf_op jit(solution)/shard_map/all_to_all | solution.py:30
  16.0 9.1 %collective-permute-start.1 = (bf16[2,64,256]{2,1,0:T(8,128)(2,1)S(1)}, bf16[2,64,256]{2,1,0:T(8,128)(2,1)S(1)}, u32[]{:S(2)}, u32[]{:S(2)}) collective-permute-start(bf16[2,64,256]{2,1,0:T(8,128)(2,1)S(1)} %get-tuple-element.121), channel_id=1, source_target_pairs={{0,128},{64,192},{128,0},{192,64},{1,129},{65,193},{129,1},{193,65... | collective-permute-start | bytes 196616 | tf_op jit(solution)/shard_map/ppermute | solution.py:38
  25.1 5.7 %collective-permute-done.1 = bf16[2,64,256]{2,1,0:T(8,128)(2,1)S(1)} collective-permute-done((bf16[2,64,256]{2,1,0:T(8,128)(2,1)S(1)}, bf16[2,64,256]{2,1,0:T(8,128)(2,1)S(1)}, u32[]{:S(2)}, u32[]{:S(2)}) %collective-permute-start.1) | collective-permute-done | bytes 65568 | tf_op jit(solution)/shard_map/ppermute | solution.py:38
  32.6 45.0 %all_to_all.30 = bf16[8,288,128]{2,1,0:T(8,128)(2,1)S(1)} all-to-all(bf16[8,288,128]{2,1,0:T(8,128)(2,1)S(1)} %bitcast.69), channel_id=1, replica_groups=mesh['gr'=2,'zq'=4,'b'=2,'y'=4,'x'=4,'core'=2] {'gr','zq'}, dimensions={0} | all-to-all | bytes 1179648 | tf_op jit(solution)/shard_map/all_to_all | solution.py:30
  77.6 2.4 collective-permute-start.3
  80.0 8.1 %collective-permute-done.3 = bf16[8,144,128]{2,1,0:T(8,128)(2,1)S(1)} collective-permute-done((bf16[8,144,128]{2,1,0:T(8,128)(2,1)S(1)}, bf16[8,144,128]{2,1,0:T(8,128)(2,1)S(1)}, u32[]{:S(2)}, u32[]{:S(2)}) %collective-permute-start.3) | collective-permute-done | bytes 294944 | tf_op jit(solution)/shard_map/ppermute | solution.py:38
  88.3 1.9 collective-permute-start.7
  90.2 4.8 %collective-permute-start.6 = (bf16[16,144,128]{2,1,0:T(8,128)(2,1)S(1)}, bf16[16,144,128]{2,1,0:T(8,128)(2,1)S(1)}, u32[]{:S(2)}, u32[]{:S(2)}) collective-permute-start(bf16[16,144,128]{2,1,0:T(8,128)(2,1)S(1)} %bitcast.63), channel_id=1, source_target_pairs={{0,4},{2,6},{4,0},{6,2},{1,5},{3,7},{5,1},{7,3},{8,12},{10,14},{12... | collective-permute-start | bytes 1769480 | tf_op jit(solution)/shard_map/ppermute | solution.py:38
  95.1 3.1 %collective-permute-start.5 = (bf16[16,144,128]{2,1,0:T(8,128)(2,1)S(1)}, bf16[16,144,128]{2,1,0:T(8,128)(2,1)}, u32[]{:S(2)}, u32[]{:S(2)}) collective-permute-start(bf16[16,144,128]{2,1,0:T(8,128)(2,1)S(1)} %bitcast.64), channel_id=1, source_target_pairs={{0,2},{2,0},{4,6},{6,4},{1,3},{3,1},{5,7},{7,5},{8,10},{10,8},{12,... | collective-permute-start | bytes 1769480 | tf_op jit(solution)/shard_map/ppermute | solution.py:38
  98.2 3.9 %collective-permute-start.2 = (bf16[2,2,64,256]{3,2,1,0:T(8,128)(2,1)S(1)}, bf16[2,2,64,256]{3,2,1,0:T(8,128)(2,1)S(1)}, u32[]{:S(2)}, u32[]{:S(2)}) collective-permute-start(bf16[2,2,64,256]{3,2,1,0:T(8,128)(2,1)S(1)} %pad_maximum_fusion.4), channel_id=1, source_target_pairs={{0,64},{64,0},{128,192},{192,128},{1,65},{65,1},{129,193},{193,129... | collective-permute-start | bytes 393224 | tf_op jit(solution)/shard_map/ppermute | solution.py:38
  102.1 5.0 %collective-permute-done.2 = bf16[2,2,64,256]{3,2,1,0:T(8,128)(2,1)S(1)} collective-permute-done((bf16[2,2,64,256]{3,2,1,0:T(8,128)(2,1)S(1)}, bf16[2,2,64,256]{3,2,1,0:T(8,128)(2,1)S(1)}, u32[]{:S(2)}, u32[]{:S(2)}) %collective-permute-start.2) | collective-permute-done | bytes 131104 | tf_op jit(solution)/shard_map/ppermute | solution.py:38
  108.2 4.2 %all-to-all-start.2 = ((bf16[4,4,2,64,256]{4,3,2,1,0:T(8,128)(2,1)}), bf16[4,4,2,64,256]{4,3,2,1,0:T(8,128)(2,1)S(1)}, u32[]{:S(2)}, u32[]{:S(2)}) async-start(bf16[4,4,2,64,256]{4,3,2,1,0:T(8,128)(2,1)} %broadcast_in_dim.13), calls=%async_computation.2 | async-start | bytes 2097152 | tf_op jit(solution)/shard_map/all_to_all | solution.py:30
  114.3 1.9 collective-permute-start.8
  118.2 1.9 collective-permute-start.11
  120.1 2.4 collective-permute-start.10
  122.5 1.9 collective-permute-start.9
  124.6 2.1 collective-permute-done.9.refs_5_
  126.8 6.6 %half_step.2 = bf16[4,4,2,64,256]{4,3,2,1,0:T(8,128)(2,1)} custom-call(s32[1]{0:T(128)} %bitcast.10.at_ref, bf16[4,4,2,64,256]{4,3,2,1,0:T(8,128)(2,1)S(1)} %all-to-all-done.2.x_ref, bf16[16,144,128]{2,1,0:T(8,128)(2,1)S(1)} %bitcast.66, bf16[16,144,128]{2,1,0:T(8,128)(2,1)} %collective-permute-done.5.refs_1_, ...), custom_call_target="tpu_custom_call" | custom-call | flops 1207959552 | bytes 6815744 | tf_op jit(solution)/shard_map/half_step/pallas_call | solution.py:171
  133.4 4.2 %all-to-all-start.3 = ((bf16[4,4,2,64,256]{4,3,2,1,0:T(8,128)(2,1)}), bf16[4,4,2,64,256]{4,3,2,1,0:T(8,128)(2,1)}, u32[]{:S(2)}, u32[]{:S(2)}) async-start(bf16[4,4,2,64,256]{4,3,2,1,0:T(8,128)(2,1)} %half_step.2), calls=%async_computation.3 | async-start | bytes 2097152 | tf_op jit(solution)/shard_map/all_to_all | solution.py:30
  137.6 2.5 collective-permute-start.16
  140.1 3.1 %collective-permute-start.15 = (bf16[16,144,128]{2,1,0:T(8,128)(2,1)S(1)}, bf16[16,144,128]{2,1,0:T(8,128)(2,1)}, u32[]{:S(2)}, u32[]{:S(2)}) collective-permute-start(bf16[16,144,128]{2,1,0:T(8,128)(2,1)S(1)} %bitcast.57), channel_id=1, source_target_pairs={{0,4},{2,6},{4,0},{6,2},{1,5},{3,7},{5,1},{7,3},{8,12},{10,14},{12... | collective-permute-start | bytes 1769480 | tf_op jit(solution)/shard_map/ppermute | solution.py:38
  143.2 4.3 %collective-permute-start.14 = (bf16[16,144,128]{2,1,0:T(8,128)(2,1)S(1)}, bf16[16,144,128]{2,1,0:T(8,128)(2,1)}, u32[]{:S(2)}, u32[]{:S(2)}) collective-permute-start(bf16[16,144,128]{2,1,0:T(8,128)(2,1)S(1)} %bitcast.58), channel_id=1, source_target_pairs={{0,2},{2,0},{4,6},{6,4},{1,3},{3,1},{5,7},{7,5},{8,10},{10,8},{12,... | collective-permute-start | bytes 1769480 | tf_op jit(solution)/shard_map/ppermute | solution.py:38
  147.5 5.9 %all-to-all-done.3 = bf16[4,4,2,64,256]{4,3,2,1,0:T(8,128)(2,1)} async-done(((bf16[4,4,2,64,256]{4,3,2,1,0:T(8,128)(2,1)}), bf16[4,4,2,64,256]{4,3,2,1,0:T(8,128)(2,1)}, u32[]{:S(2)}, u32[]{:S(2)}) %all-to-all-start.3) | async-done | bytes 1048608 | tf_op jit(solution)/shard_map/all_to_all | solution.py:30
  154.5 3.7 %collective-permute-start.12 = (bf16[2,2,64,256]{3,2,1,0:T(8,128)(2,1)S(1)}, bf16[2,2,64,256]{3,2,1,0:T(8,128)(2,1)S(1)}, u32[]{:S(2)}, u32[]{:S(2)}) collective-permute-start(bf16[2,2,64,256]{3,2,1,0:T(8,128)(2,1)S(1)} %slice_reduce_fusion), channel_id=1, source_target_pairs={{0,64},{64,0},{128,192},{192,128},{1,65},{65,1},{129,193},{193,129... | collective-permute-start | bytes 393224 | tf_op jit(solution)/shard_map/ppermute | solution.py:38
  159.3 5.4 %collective-permute-done.12 = bf16[2,2,64,256]{3,2,1,0:T(8,128)(2,1)S(1)} collective-permute-done((bf16[2,2,64,256]{3,2,1,0:T(8,128)(2,1)S(1)}, bf16[2,2,64,256]{3,2,1,0:T(8,128)(2,1)S(1)}, u32[]{:S(2)}, u32[]{:S(2)}) %collective-permute-start.12) | collective-permute-done | bytes 131104 | tf_op jit(solution)/shard_map/ppermute | solution.py:38
  164.8 3.1 %collective-permute-start.13 = (bf16[2,2,64,256]{3,2,1,0:T(8,128)(2,1)S(1)}, bf16[2,2,64,256]{3,2,1,0:T(8,128)(2,1)S(1)}, u32[]{:S(2)}, u32[]{:S(2)}) collective-permute-start(bf16[2,2,64,256]{3,2,1,0:T(8,128)(2,1)S(1)} %add_convert_fusion.1), channel_id=1, source_target_pairs={{0,128},{64,192},{128,0},{192,64},{1,129},{65,193},{129,1},{193,65... | collective-permute-start | bytes 393224 | tf_op jit(solution)/shard_map/ppermute | solution.py:38
  168.0 4.9 %serve.2 = (bf16[176,2048]{1,0:T(8,128)(2,1)}, bf16[176,2048]{1,0:T(8,128)(2,1)}, bf16[176,2048]{1,0:T(8,128)(2,1)}) custom-call(s32[3]{0:T(128)S(1)} %pad_add_fusion.at_ref, bf16[16,144,128]{2,1,0:T(8,128)(2,1)S(1)} %bitcast.67, bf16[16,144,128]{2,1,0:T(8,128)(2,1)} %collective-permute-done.5.refs_1_, ...), custom_call_target="tpu_custom_call" | custom-call | flops 100000000 | bytes 6881280 | tf_op jit(solution)/shard_map/serve/pallas_call | solution.py:205
  172.8 9.0 %collective-permute-done.13 = bf16[2,2,64,256]{3,2,1,0:T(8,128)(2,1)S(1)} collective-permute-done((bf16[2,2,64,256]{3,2,1,0:T(8,128)(2,1)S(1)}, bf16[2,2,64,256]{3,2,1,0:T(8,128)(2,1)S(1)}, u32[]{:S(2)}, u32[]{:S(2)}) %collective-permute-start.13) | collective-permute-done | bytes 131104 | tf_op jit(solution)/shard_map/ppermute | solution.py:38
  181.9 1.9 collective-permute-start.17
  183.9 6.2 %collective-permute-done.17 = bf16[2,2,64,256]{3,2,1,0:T(8,128)(2,1)S(1)} collective-permute-done((bf16[2,2,64,256]{3,2,1,0:T(8,128)(2,1)S(1)}, bf16[2,2,64,256]{3,2,1,0:T(8,128)(2,1)S(1)}, u32[]{:S(2)}, u32[]{:S(2)}) %collective-permute-start.17) | collective-permute-done | bytes 131104 | tf_op jit(solution)/shard_map/ppermute | solution.py:38
  191.2 3.5 %all-to-all-start.4 = ((bf16[4,4,2,64,256]{4,3,2,1,0:T(8,128)(2,1)}), bf16[4,4,2,64,256]{4,3,2,1,0:T(8,128)(2,1)S(1)}, u32[]{:S(2)}, u32[]{:S(2)}) async-start(bf16[4,4,2,64,256]{4,3,2,1,0:T(8,128)(2,1)} %broadcast_in_dim.28), calls=%async_computation.4 | async-start | bytes 2097152 | tf_op jit(solution)/shard_map/all_to_all | solution.py:30
  194.7 1.9 collective-permute-start.18
  196.7 2.4 collective-permute-start.19
  199.1 1.9 collective-permute-start.20
  201.0 2.4 collective-permute-start.21
  205.9 3.5 %all-to-all-done.4.x_ref = bf16[4,4,2,64,256]{4,3,2,1,0:T(8,128)(2,1)S(1)} async-done(((bf16[4,4,2,64,256]{4,3,2,1,0:T(8,128)(2,1)}), bf16[4,4,2,64,256]{4,3,2,1,0:T(8,128)(2,1)S(1)}, u32[]{:S(2)}, u32[]{:S(2)}) %all-to-all-start.4) | async-done | bytes 1048608 | tf_op jit(solution)/shard_map/all_to_all | solution.py:30
  211.5 6.1 %half_step.3 = bf16[4,4,2,64,256]{4,3,2,1,0:T(8,128)(2,1)} custom-call(s32[1]{0:T(128)} %bitcast.10.at_ref, bf16[4,4,2,64,256]{4,3,2,1,0:T(8,128)(2,1)S(1)} %all-to-all-done.4.x_ref, bf16[16,144,128]{2,1,0:T(8,128)(2,1)S(1)} %bitcast.60, bf16[16,144,128]{2,1,0:T(8,128)(2,1)} %collective-permute-done.14.refs_1_, ...), custom_call_target="tpu_custom_call" | custom-call | flops 1207959552 | bytes 6815744 | tf_op jit(solution)/shard_map/half_step/pallas_call | solution.py:171
  217.6 4.4 %all-to-all-start.5 = ((bf16[4,4,2,64,256]{4,3,2,1,0:T(8,128)(2,1)}), bf16[4,4,2,64,256]{4,3,2,1,0:T(8,128)(2,1)}, u32[]{:S(2)}, u32[]{:S(2)}) async-start(bf16[4,4,2,64,256]{4,3,2,1,0:T(8,128)(2,1)} %half_step.3), calls=%async_computation.5 | async-start | bytes 2097152 | tf_op jit(solution)/shard_map/all_to_all | solution.py:30
  223.0 4.5 %serve.3 = (bf16[176,2048]{1,0:T(8,128)(2,1)}, bf16[176,2048]{1,0:T(8,128)(2,1)}, bf16[176,2048]{1,0:T(8,128)(2,1)}) custom-call(s32[3]{0:T(128)S(1)} %pad_add_fusion.at_ref, bf16[16,144,128]{2,1,0:T(8,128)(2,1)S(1)} %bitcast.61, bf16[16,144,128]{2,1,0:T(8,128)(2,1)} %collective-permute-done.14.refs_1_, ...), custom_call_target="tpu_custom_call" | custom-call | flops 100000000 | bytes 6881280 | tf_op jit(solution)/shard_map/serve/pallas_call | solution.py:205
  227.5 8.3 %all-to-all-done.5 = bf16[4,4,2,64,256]{4,3,2,1,0:T(8,128)(2,1)} async-done(((bf16[4,4,2,64,256]{4,3,2,1,0:T(8,128)(2,1)}), bf16[4,4,2,64,256]{4,3,2,1,0:T(8,128)(2,1)}, u32[]{:S(2)}, u32[]{:S(2)}) %all-to-all-start.5) | async-done | bytes 1048608 | tf_op jit(solution)/shard_map/all_to_all | solution.py:30
  237.0 2.8 %collective-permute-start.22 = (bf16[2,2,64,256]{3,2,1,0:T(8,128)(2,1)S(1)}, bf16[2,2,64,256]{3,2,1,0:T(8,128)(2,1)S(1)}, u32[]{:S(2)}, u32[]{:S(2)}) collective-permute-start(bf16[2,2,64,256]{3,2,1,0:T(8,128)(2,1)S(1)} %slice_reduce_fusion.1), channel_id=1, source_target_pairs={{0,64},{64,0},{128,192},{192,128},{1,65},{65,1},{129,193},{193,129... | collective-permute-start | bytes 393224 | tf_op jit(solution)/shard_map/ppermute | solution.py:38
  240.9 3.8 %collective-permute-done.22 = bf16[2,2,64,256]{3,2,1,0:T(8,128)(2,1)S(1)} collective-permute-done((bf16[2,2,64,256]{3,2,1,0:T(8,128)(2,1)S(1)}, bf16[2,2,64,256]{3,2,1,0:T(8,128)(2,1)S(1)}, u32[]{:S(2)}, u32[]{:S(2)}) %collective-permute-start.22) | collective-permute-done | bytes 131104 | tf_op jit(solution)/shard_map/ppermute | solution.py:38
  244.8 5.3 %collective-permute-start.23 = (bf16[2,64,256]{2,1,0:T(8,128)(2,1)S(1)}, bf16[2,64,256]{2,1,0:T(8,128)(2,1)S(1)}, u32[]{:S(2)}, u32[]{:S(2)}) collective-permute-start(bf16[2,64,256]{2,1,0:T(8,128)(2,1)S(1)} %fusion.4), channel_id=1, source_target_pairs={{0,128},{64,192},{128,0},{192,64},{1,129},{65,193},{129,1},{193,65... | collective-permute-start | bytes 196616 | tf_op jit(solution)/shard_map/ppermute | solution.py:38
  250.1 5.5 %collective-permute-done.23 = bf16[2,64,256]{2,1,0:T(8,128)(2,1)S(1)} collective-permute-done((bf16[2,64,256]{2,1,0:T(8,128)(2,1)S(1)}, bf16[2,64,256]{2,1,0:T(8,128)(2,1)S(1)}, u32[]{:S(2)}, u32[]{:S(2)}) %collective-permute-start.23) | collective-permute-done | bytes 65568 | tf_op jit(solution)/shard_map/ppermute | solution.py:38
  255.6 1.9 collective-permute-start.24
  257.6 3.9 %collective-permute-done.24 = bf16[64,256]{1,0:T(8,128)(2,1)S(1)} collective-permute-done((bf16[64,256]{1,0:T(8,128)(2,1)S(1)}, bf16[64,256]{1,0:T(8,128)(2,1)S(1)}, u32[]{:S(2)}, u32[]{:S(2)}) %collective-permute-start.24) | collective-permute-done | bytes 32800 | tf_op jit(solution)/shard_map/ppermute | solution.py:38
  (69 shorter events, 20.0 us)
Async XLA Ops:
  0.6 15.4 %copy-start.8 = (bf16[512,64]{0,1:T(8,128)(2,1)S(1)}, bf16[512,64]{0,1:T(8,128)(2,1)}, u32[]{:S(2)}) copy-start(bf16[512,64]{0,1:T(8,128)(2,1)} %param.9) | copy-start | bytes 196612
  1.5 14.5 %collective-permute-start = (bf16[64,256]{1,0:T(8,128)(2,1)S(1)}, bf16[64,256]{1,0:T(8,128)(2,1)S(1)}, u32[]{:S(2)}, u32[]{:S(2)}) collective-permute-start(bf16[64,256]{1,0:T(8,128)(2,1)S(1)} %broadcast_select_fusion.1), channel_id=1, source_target_pairs={{0,32},{32,0},{1,33},{33,1},{2,34},{34,2},{3,35},{35,3},{4,36},{36... | collective-permute-start | bytes 98312 | tf_op jit(solution)/shard_map/ppermute | solution.py:38
  8.5 22.4 %all-to-all-start = ((bf16[16,32,264]{2,1,0:T(8,128)(2,1)}), bf16[16,32,264]{2,1,0:T(8,128)(2,1)S(1)}, u32[]{:S(2)}, u32[]{:S(2)}) async-start(bf16[16,32,264]{2,1,0:T(8,128)(2,1)} %pack.1), calls=%async_computation | async-start | bytes 786432 | tf_op jit(solution)/shard_map/all_to_all | solution.py:30
  16.0 14.8 %collective-permute-start.1 = (bf16[2,64,256]{2,1,0:T(8,128)(2,1)S(1)}, bf16[2,64,256]{2,1,0:T(8,128)(2,1)S(1)}, u32[]{:S(2)}, u32[]{:S(2)}) collective-permute-start(bf16[2,64,256]{2,1,0:T(8,128)(2,1)S(1)} %get-tuple-element.121), channel_id=1, source_target_pairs={{0,128},{64,192},{128,0},{192,64},{1,129},{65,193},{129,1},{193,65... | collective-permute-start | bytes 196616 | tf_op jit(solution)/shard_map/ppermute | solution.py:38
  77.6 10.5 %collective-permute-start.3 = (bf16[8,144,128]{2,1,0:T(8,128)(2,1)S(1)}, bf16[8,144,128]{2,1,0:T(8,128)(2,1)S(1)}, u32[]{:S(2)}, u32[]{:S(2)}) collective-permute-start(bf16[8,144,128]{2,1,0:T(8,128)(2,1)S(1)} %slice.55), channel_id=1, source_target_pairs={{0,32},{32,0},{1,33},{33,1},{2,34},{34,2},{3,35},{35,3},{4,36},{36... | collective-permute-start | bytes 884744 | tf_op jit(solution)/shard_map/ppermute | solution.py:38
  88.3 29.8 %collective-permute-start.7 = (bf16[16,144,128]{2,1,0:T(8,128)(2,1)S(1)}, bf16[16,144,128]{2,1,0:T(8,128)(2,1)S(1)}, u32[]{:S(2)}, u32[]{:S(2)}) collective-permute-start(bf16[16,144,128]{2,1,0:T(8,128)(2,1)S(1)} %bitcast.62), channel_id=1, source_target_pairs={{0,6},{2,4},{4,2},{6,0},{1,7},{3,5},{5,3},{7,1},{8,14},{10,12},{12... | collective-permute-start | bytes 1769480 | tf_op jit(solution)/shard_map/ppermute | solution.py:38
  90.2 29.8 %collective-permute-start.6 = (bf16[16,144,128]{2,1,0:T(8,128)(2,1)S(1)}, bf16[16,144,128]{2,1,0:T(8,128)(2,1)S(1)}, u32[]{:S(2)}, u32[]{:S(2)}) collective-permute-start(bf16[16,144,128]{2,1,0:T(8,128)(2,1)S(1)} %bitcast.63), channel_id=1, source_target_pairs={{0,4},{2,6},{4,0},{6,2},{1,5},{3,7},{5,1},{7,3},{8,12},{10,14},{12... | collective-permute-start | bytes 1769480 | tf_op jit(solution)/shard_map/ppermute | solution.py:38
  95.1 27.4 %collective-permute-start.5 = (bf16[16,144,128]{2,1,0:T(8,128)(2,1)S(1)}, bf16[16,144,128]{2,1,0:T(8,128)(2,1)}, u32[]{:S(2)}, u32[]{:S(2)}) collective-permute-start(bf16[16,144,128]{2,1,0:T(8,128)(2,1)S(1)} %bitcast.64), channel_id=1, source_target_pairs={{0,2},{2,0},{4,6},{6,4},{1,3},{3,1},{5,7},{7,5},{8,10},{10,8},{12,... | collective-permute-start | bytes 1769480 | tf_op jit(solution)/shard_map/ppermute | solution.py:38
  98.2 8.9 %collective-permute-start.2 = (bf16[2,2,64,256]{3,2,1,0:T(8,128)(2,1)S(1)}, bf16[2,2,64,256]{3,2,1,0:T(8,128)(2,1)S(1)}, u32[]{:S(2)}, u32[]{:S(2)}) collective-permute-start(bf16[2,2,64,256]{3,2,1,0:T(8,128)(2,1)S(1)} %pad_maximum_fusion.4), channel_id=1, source_target_pairs={{0,64},{64,0},{128,192},{192,128},{1,65},{65,1},{129,193},{193,129... | collective-permute-start | bytes 393224 | tf_op jit(solution)/shard_map/ppermute | solution.py:38
  108.2 16.5 %all-to-all-start.2 = ((bf16[4,4,2,64,256]{4,3,2,1,0:T(8,128)(2,1)}), bf16[4,4,2,64,256]{4,3,2,1,0:T(8,128)(2,1)S(1)}, u32[]{:S(2)}, u32[]{:S(2)}) async-start(bf16[4,4,2,64,256]{4,3,2,1,0:T(8,128)(2,1)} %broadcast_in_dim.13), calls=%async_computation.2 | async-start | bytes 2097152 | tf_op jit(solution)/shard_map/all_to_all | solution.py:30
  112.4 12.0 %collective-permute-start.4 = (bf16[8,144,128]{2,1,0:T(8,128)(2,1)S(1)}, bf16[8,144,128]{2,1,0:T(8,128)(2,1)S(1)}, u32[]{:S(2)}, u32[]{:S(2)}) collective-permute-start(bf16[8,144,128]{2,1,0:T(8,128)(2,1)S(1)} %get-tuple-element.62), channel_id=1, source_target_pairs={{0,32},{32,0},{1,33},{33,1},{2,34},{34,2},{3,35},{35,3},{4,36},{36... | collective-permute-start | bytes 884744 | tf_op jit(solution)/shard_map/ppermute | solution.py:38
  114.3 10.2 %collective-permute-start.8 = (bf16[16,144,128]{2,1,0:T(8,128)(2,1)S(1)}, bf16[16,144,128]{2,1,0:T(8,128)(2,1)}, u32[]{:S(2)}, u32[]{:S(2)}) collective-permute-start(bf16[16,144,128]{2,1,0:T(8,128)(2,1)S(1)} %bitcast.65), channel_id=1, source_target_pairs={{0,1},{1,0},{2,3},{3,2},{4,5},{5,4},{6,7},{7,6},{8,9},{9,8},{10,11... | collective-permute-start | bytes 1769480 | tf_op jit(solution)/shard_map/ppermute | solution.py:38
  118.2 6.5 %collective-permute-start.11 = (bf16[16,144,128]{2,1,0:T(8,128)(2,1)S(1)}, bf16[16,144,128]{2,1,0:T(8,128)(2,1)}, u32[]{:S(2)}, u32[]{:S(2)}) collective-permute-start(bf16[16,144,128]{2,1,0:T(8,128)(2,1)S(1)} %collective-permute-done.7.refs_3_), channel_id=1, source_target_pairs={{0,1},{1,0},{2,3},{3,2},{4,5},{5,4},{6,7},{7,6},{8,9},{9,8},{10,11... | collective-permute-start | bytes 1769480 | tf_op jit(solution)/shard_map/ppermute | solution.py:38
  120.1 4.6 %collective-permute-start.10 = (bf16[16,144,128]{2,1,0:T(8,128)(2,1)S(1)}, bf16[16,144,128]{2,1,0:T(8,128)(2,1)}, u32[]{:S(2)}, u32[]{:S(2)}) collective-permute-start(bf16[16,144,128]{2,1,0:T(8,128)(2,1)S(1)} %collective-permute-done.6.refs_2_), channel_id=1, source_target_pairs={{0,1},{1,0},{2,3},{3,2},{4,5},{5,4},{6,7},{7,6},{8,9},{9,8},{10,11... | collective-permute-start | bytes 1769480 | tf_op jit(solution)/shard_map/ppermute | solution.py:38
  122.5 4.2 %collective-permute-start.9 = (bf16[16,144,128]{2,1,0:T(8,128)(2,1)}, bf16[16,144,128]{2,1,0:T(8,128)(2,1)}, u32[]{:S(2)}, u32[]{:S(2)}) collective-permute-start(bf16[16,144,128]{2,1,0:T(8,128)(2,1)} %collective-permute-done.5.refs_1_), channel_id=1, source_target_pairs={{0,1},{1,0},{2,3},{3,2},{4,5},{5,4},{6,7},{7,6},{8,9},{9,8},{10,11... | collective-permute-start | bytes 1769480 | tf_op jit(solution)/shard_map/ppermute | solution.py:38
  133.4 20.0 %all-to-all-start.3 = ((bf16[4,4,2,64,256]{4,3,2,1,0:T(8,128)(2,1)}), bf16[4,4,2,64,256]{4,3,2,1,0:T(8,128)(2,1)}, u32[]{:S(2)}, u32[]{:S(2)}) async-start(bf16[4,4,2,64,256]{4,3,2,1,0:T(8,128)(2,1)} %half_step.2), calls=%async_computation.3 | async-start | bytes 2097152 | tf_op jit(solution)/shard_map/all_to_all | solution.py:30
  137.6 44.2 %collective-permute-start.16 = (bf16[16,144,128]{2,1,0:T(8,128)(2,1)S(1)}, bf16[16,144,128]{2,1,0:T(8,128)(2,1)S(1)}, u32[]{:S(2)}, u32[]{:S(2)}) collective-permute-start(bf16[16,144,128]{2,1,0:T(8,128)(2,1)S(1)} %bitcast.56), channel_id=1, source_target_pairs={{0,6},{2,4},{4,2},{6,0},{1,7},{3,5},{5,3},{7,1},{8,14},{10,12},{12... | collective-permute-start | bytes 1769480 | tf_op jit(solution)/shard_map/ppermute | solution.py:38
  140.1 41.8 %collective-permute-start.15 = (bf16[16,144,128]{2,1,0:T(8,128)(2,1)S(1)}, bf16[16,144,128]{2,1,0:T(8,128)(2,1)}, u32[]{:S(2)}, u32[]{:S(2)}) collective-permute-start(bf16[16,144,128]{2,1,0:T(8,128)(2,1)S(1)} %bitcast.57), channel_id=1, source_target_pairs={{0,4},{2,6},{4,0},{6,2},{1,5},{3,7},{5,1},{7,3},{8,12},{10,14},{12... | collective-permute-start | bytes 1769480 | tf_op jit(solution)/shard_map/ppermute | solution.py:38
  143.2 38.7 %collective-permute-start.14 = (bf16[16,144,128]{2,1,0:T(8,128)(2,1)S(1)}, bf16[16,144,128]{2,1,0:T(8,128)(2,1)}, u32[]{:S(2)}, u32[]{:S(2)}) collective-permute-start(bf16[16,144,128]{2,1,0:T(8,128)(2,1)S(1)} %bitcast.58), channel_id=1, source_target_pairs={{0,2},{2,0},{4,6},{6,4},{1,3},{3,1},{5,7},{7,5},{8,10},{10,8},{12,... | collective-permute-start | bytes 1769480 | tf_op jit(solution)/shard_map/ppermute | solution.py:38
  154.5 10.2 %collective-permute-start.12 = (bf16[2,2,64,256]{3,2,1,0:T(8,128)(2,1)S(1)}, bf16[2,2,64,256]{3,2,1,0:T(8,128)(2,1)S(1)}, u32[]{:S(2)}, u32[]{:S(2)}) collective-permute-start(bf16[2,2,64,256]{3,2,1,0:T(8,128)(2,1)S(1)} %slice_reduce_fusion), channel_id=1, source_target_pairs={{0,64},{64,0},{128,192},{192,128},{1,65},{65,1},{129,193},{193,129... | collective-permute-start | bytes 393224 | tf_op jit(solution)/shard_map/ppermute | solution.py:38
  164.8 17.1 %collective-permute-start.13 = (bf16[2,2,64,256]{3,2,1,0:T(8,128)(2,1)S(1)}, bf16[2,2,64,256]{3,2,1,0:T(8,128)(2,1)S(1)}, u32[]{:S(2)}, u32[]{:S(2)}) collective-permute-start(bf16[2,2,64,256]{3,2,1,0:T(8,128)(2,1)S(1)} %add_convert_fusion.1), channel_id=1, source_target_pairs={{0,128},{64,192},{128,0},{192,64},{1,129},{65,193},{129,1},{193,65... | collective-permute-start | bytes 393224 | tf_op jit(solution)/shard_map/ppermute | solution.py:38
  181.9 9.3 %copy-start.6 = (bf16[2,2,64,256]{3,2,1,0:T(8,128)(2,1)}, bf16[2,2,64,256]{3,2,1,0:T(8,128)(2,1)S(1)}, u32[]{:S(2)}) copy-start(bf16[2,2,64,256]{3,2,1,0:T(8,128)(2,1)S(1)} %add_convert_fusion) | copy-start | bytes 393220
  181.9 8.2 %collective-permute-start.17 = (bf16[2,2,64,256]{3,2,1,0:T(8,128)(2,1)S(1)}, bf16[2,2,64,256]{3,2,1,0:T(8,128)(2,1)S(1)}, u32[]{:S(2)}, u32[]{:S(2)}) collective-permute-start(bf16[2,2,64,256]{3,2,1,0:T(8,128)(2,1)S(1)} %add_convert_fusion), channel_id=1, source_target_pairs={{0,64},{64,0},{128,192},{192,128},{1,65},{65,1},{129,193},{193,129... | collective-permute-start | bytes 393224 | tf_op jit(solution)/shard_map/ppermute | solution.py:38
  191.2 18.1 %all-to-all-start.4 = ((bf16[4,4,2,64,256]{4,3,2,1,0:T(8,128)(2,1)}), bf16[4,4,2,64,256]{4,3,2,1,0:T(8,128)(2,1)S(1)}, u32[]{:S(2)}, u32[]{:S(2)}) async-start(bf16[4,4,2,64,256]{4,3,2,1,0:T(8,128)(2,1)} %broadcast_in_dim.28), calls=%async_computation.4 | async-start | bytes 2097152 | tf_op jit(solution)/shard_map/all_to_all | solution.py:30
  194.7 8.7 %collective-permute-start.18 = (bf16[16,144,128]{2,1,0:T(8,128)(2,1)S(1)}, bf16[16,144,128]{2,1,0:T(8,128)(2,1)S(1)}, u32[]{:S(2)}, u32[]{:S(2)}) collective-permute-start(bf16[16,144,128]{2,1,0:T(8,128)(2,1)S(1)} %bitcast.59), channel_id=1, source_target_pairs={{0,1},{1,0},{2,3},{3,2},{4,5},{5,4},{6,7},{7,6},{8,9},{9,8},{10,11... | collective-permute-start | bytes 1769480 | tf_op jit(solution)/shard_map/ppermute | solution.py:38
  196.7 6.8 %collective-permute-start.19 = (bf16[16,144,128]{2,1,0:T(8,128)(2,1)}, bf16[16,144,128]{2,1,0:T(8,128)(2,1)S(1)}, u32[]{:S(2)}, u32[]{:S(2)}) collective-permute-start(bf16[16,144,128]{2,1,0:T(8,128)(2,1)} %collective-permute-done.14.refs_1_), channel_id=1, source_target_pairs={{0,1},{1,0},{2,3},{3,2},{4,5},{5,4},{6,7},{7,6},{8,9},{9,8},{10,11... | collective-permute-start | bytes 1769480 | tf_op jit(solution)/shard_map/ppermute | solution.py:38
  199.1 4.4 %collective-permute-start.20 = (bf16[16,144,128]{2,1,0:T(8,128)(2,1)}, bf16[16,144,128]{2,1,0:T(8,128)(2,1)S(1)}, u32[]{:S(2)}, u32[]{:S(2)}) collective-permute-start(bf16[16,144,128]{2,1,0:T(8,128)(2,1)} %collective-permute-done.15.refs_2_), channel_id=1, source_target_pairs={{0,1},{1,0},{2,3},{3,2},{4,5},{5,4},{6,7},{7,6},{8,9},{9,8},{10,11... | collective-permute-start | bytes 1769480 | tf_op jit(solution)/shard_map/ppermute | solution.py:38
  201.0 4.0 %collective-permute-start.21 = (bf16[16,144,128]{2,1,0:T(8,128)(2,1)S(1)}, bf16[16,144,128]{2,1,0:T(8,128)(2,1)S(1)}, u32[]{:S(2)}, u32[]{:S(2)}) collective-permute-start(bf16[16,144,128]{2,1,0:T(8,128)(2,1)S(1)} %collective-permute-done.16.refs_3_), channel_id=1, source_target_pairs={{0,1},{1,0},{2,3},{3,2},{4,5},{5,4},{6,7},{7,6},{8,9},{9,8},{10,11... | collective-permute-start | bytes 1769480 | tf_op jit(solution)/shard_map/ppermute | solution.py:38
  203.5 0.8 copy-start
  205.0 0.8 copy-start.3
  209.4 1.1 copy-start.1
  210.4 1.1 copy-start.4
  217.6 4.4 %copy-start.2 = (bf16[16,144,128]{2,1,0:T(8,128)(2,1)S(1)}, bf16[16,144,128]{2,1,0:T(8,128)(2,1)}, u32[]{:S(2)}) copy-start(bf16[16,144,128]{2,1,0:T(8,128)(2,1)} %copy-done) | copy-start | bytes 1769476
  217.6 18.2 %all-to-all-start.5 = ((bf16[4,4,2,64,256]{4,3,2,1,0:T(8,128)(2,1)}), bf16[4,4,2,64,256]{4,3,2,1,0:T(8,128)(2,1)}, u32[]{:S(2)}, u32[]{:S(2)}) async-start(bf16[4,4,2,64,256]{4,3,2,1,0:T(8,128)(2,1)} %half_step.3), calls=%async_computation.5 | async-start | bytes 2097152 | tf_op jit(solution)/shard_map/all_to_all | solution.py:30
  222.0 1.1 copy-start.5
  235.8 19.8 %copy-start.7 = (bf16[2,2,64,256]{3,2,1,0:T(8,128)(2,1)S(1)}, bf16[2,2,64,256]{3,2,1,0:T(8,128)(2,1)}, u32[]{:S(2)}) copy-start(bf16[2,2,64,256]{3,2,1,0:T(8,128)(2,1)} %copy-done.6) | copy-start | bytes 393220
  237.0 7.8 %collective-permute-start.22 = (bf16[2,2,64,256]{3,2,1,0:T(8,128)(2,1)S(1)}, bf16[2,2,64,256]{3,2,1,0:T(8,128)(2,1)S(1)}, u32[]{:S(2)}, u32[]{:S(2)}) collective-permute-start(bf16[2,2,64,256]{3,2,1,0:T(8,128)(2,1)S(1)} %slice_reduce_fusion.1), channel_id=1, source_target_pairs={{0,64},{64,0},{128,192},{192,128},{1,65},{65,1},{129,193},{193,129... | collective-permute-start | bytes 393224 | tf_op jit(solution)/shard_map/ppermute | solution.py:38
  244.8 10.8 %collective-permute-start.23 = (bf16[2,64,256]{2,1,0:T(8,128)(2,1)S(1)}, bf16[2,64,256]{2,1,0:T(8,128)(2,1)S(1)}, u32[]{:S(2)}, u32[]{:S(2)}) collective-permute-start(bf16[2,64,256]{2,1,0:T(8,128)(2,1)S(1)} %fusion.4), channel_id=1, source_target_pairs={{0,128},{64,192},{128,0},{192,64},{1,129},{65,193},{129,1},{193,65... | collective-permute-start | bytes 196616 | tf_op jit(solution)/shard_map/ppermute | solution.py:38
  255.6 5.8 %collective-permute-start.24 = (bf16[64,256]{1,0:T(8,128)(2,1)S(1)}, bf16[64,256]{1,0:T(8,128)(2,1)S(1)}, u32[]{:S(2)}, u32[]{:S(2)}) collective-permute-start(bf16[64,256]{1,0:T(8,128)(2,1)S(1)} %select_bitcast_fusion.4), channel_id=1, source_target_pairs={{0,32},{32,0},{1,33},{33,1},{2,34},{34,2},{3,35},{35,3},{4,36},{36... | collective-permute-start | bytes 98312 | tf_op jit(solution)/shard_map/ppermute | solution.py:38

commit v6 on v5

--- a/solution.py
+++ b/solution.py
@@ -245,15 +245,26 @@
     return jnp.sum(by_y[:, : ZQ // 2].astype(F32), axis=0) + got.astype(F32)
 
 
-def summed(by_y):
-    kept = kept_half(by_y)
-    return kept[0] + from_peer(kept[1].astype(BF16), "zq", ZQ, 2).astype(F32)
-
-
 def summed_twice(by_y):
     kept = kept_half(by_y).astype(BF16)
     got = from_peer(kept, "zq", ZQ, 2)
     return kept.astype(F32) + got[::-1].astype(F32)
+
+
+def brought_home(by_y):
+    near, far = kept_half(by_y).astype(BF16)
+    low = lax.axis_index("b") == 0
+
+    def own(block):
+        return jnp.where(low, block[0], block[1])
+
+    def peer(block):
+        return jnp.where(low, block[1], block[0])
+
+    here = own(near).astype(F32) + from_peer(own(far), ("zq", "b"), ZL, 4).astype(F32)
+    there = from_peer(peer(near), ("zq", "b"), ZL, 1).astype(F32)
+    there += from_peer(peer(far), ("zq", "b"), ZL, 5).astype(F32)
+    return jnp.where(low, here, there), jnp.where(low, there, here)
 
 
 def stepped(tokens, total):
@@ -288,11 +299,11 @@
     pieces += over_core(pieces)
 
     partial = half_partial(share(near_zq(middle), "y", Y), pieces)
-    partial, *pieces = lax.optimization_barrier((partial, *pieces))
+    base = traded(middle[0, 0], middle[0, 1])
+    partial, base, *pieces = lax.optimization_barrier((partial, base, *pieces))
     second = served(pieces)
     by_y, *second = lax.optimization_barrier((swap(partial, "y"), *second))
-    result = stepped(middle[0], summed(by_y))
-    back = jnp.concatenate(traded(result[0], result[1]), axis=1)
+    back = jnp.concatenate([stepped(*half) for half in zip(base, brought_home(by_y))], axis=1)
     return (back.T, *first, *second)
 
 

time: 264 us -> 271 us (1.027)
  starting transfers between devices: 100 us -> 108 us
  waiting for transfers between devices: 75.2 us -> 69.2 us
  local copies, waits for them, and re-layouts: 8.76 us -> 12.8 us
    ppermute x25 -> x27, starting transfers between devices: 76.3 us -> 83.6 us  [from_peer(): return lax.ppermute(block, axis, [(i, i ^ flip) for i in range(size)])]
    unnamed x18 -> x32, local copies, waits for them, and re-layouts: 4.83 us -> 8.86 us
    all_to_all x5, waiting for transfers between devices: 17.8 us -> 13.8 us  [swap(): return lax.all_to_all(blocks, axis, split_axis=0, concat_axis=0, tiled=True)]
    ppermute x25 -> x27, waiting for transfers between devices: 57.4 us -> 55.4 us  [from_peer(): return lax.ppermute(block, axis, [(i, i ^ flip) for i in range(size)])]
  transfers between devices with their start and end apart: 30 -> 32, of which waited for: 16 -> 14; matrix products, arithmetic and copies ran while one was open for 2% -> 2% of each run, Pallas kernels for 5% -> 5%
where the time goes in v6:
time: 271 us; the launch traced here: 269 us
  starting transfers between devices  108 us (40%)
  waiting for transfers between devices  69.2 us (26%)
  blocking collectives  45 us (17%)
  Pallas kernels  25 us (9%)
  local copies, waits for them, and re-layouts  12.8 us (5%)
  other arithmetic  8.08 us (3%)
    ppermute x27, starting transfers between devices, from_peer(): return lax.ppermute(block, axis, [(i, i ^ flip) for i in range(size)])  83.6 us
    ppermute x27, waiting for transfers between devices, from_peer(): return lax.ppermute(block, axis, [(i, i ^ flip) for i in range(size)])  55.4 us
    all_to_all x1, blocking collectives, swap(): return lax.all_to_all(blocks, axis, split_axis=0, concat_axis=0, tiled=True)  45 us
    all_to_all x5, starting transfers between devices, swap(): return lax.all_to_all(blocks, axis, split_axis=0, concat_axis=0, tiled=True)  24.3 us
    all_to_all x5, waiting for transfers between devices, swap(): return lax.all_to_all(blocks, axis, split_axis=0, concat_axis=0, tiled=True)  13.8 us
    pallas_call x2, Pallas kernels, half_partial(): pl.pallas_call(half_kernel, out_shape=jax.ShapeDtypeStruct(tokens.shape,...  12.6 us
    pallas_call x2, Pallas kernels, served(): pl.pallas_call(serve_kernel, out_shape=[jax.ShapeDtypeStruct((BLOCK, D),...  9.17 us
    unnamed x32, local copies, waits for them, and re-layouts  8.86 us
  transfers between devices with their start and end apart: 32, of which 14 were waited for; matrix products, arithmetic and copies ran while one was open for 2% of the time, Pallas kernels for 5%

profile of v6, /device:TPU:6, one launch (start us, length us, event | category | flops | bytes accessed | tf_op | source)
XLA Modules:
  0.0 269.1 jit_solution(12478592572596120291)
XLA Ops:
  1.5 3.8 %collective-permute-start = (bf16[64,256]{1,0:T(8,128)(2,1)S(1)}, bf16[64,256]{1,0:T(8,128)(2,1)S(1)}, u32[]{:S(2)}, u32[]{:S(2)}) collective-permute-start(bf16[64,256]{1,0:T(8,128)(2,1)S(1)} %broadcast_select_fusion.2), channel_id=1, source_target_pairs={{0,32},{32,0},{1,33},{33,1},{2,34},{34,2},{3,35},{35,3},{4,36},{36... | collective-permute-start | bytes 98312 | tf_op jit(solution)/shard_map/ppermute | solution.py:38
  5.3 3.2 %pack.1 = bf16[16,32,264]{2,1,0:T(8,128)(2,1)} custom-call(f32[1,32]{1,0:T(1,128)} %bitcast.68, f32[1,32]{1,0:T(1,128)} %bitcast.69, f32[32,704]{1,0:T(8,128)} %refs_0_.1, f32[32,704]{1,0:T(8,128)} %refs_1_.1, f32[32,704]{1,0:T(8,128)} %refs_2_.1, f32[32,704]{1,0:T(8,128)} %refs_3_.1, f32[32,704]{1,0:T(8,128)} %refs_4_.1, f32[32,704]{1,0:T(8,128)} %refs_5_.1), custom_call_target="tpu_custom_call" | custom-call | flops 1000000 | bytes 1000000 | tf_op jit(solution)/shard_map/pack/pallas_call | solution.py:73
  8.5 7.4 %all-to-all-start = ((bf16[16,32,264]{2,1,0:T(8,128)(2,1)}), bf16[16,32,264]{2,1,0:T(8,128)(2,1)S(1)}, u32[]{:S(2)}, u32[]{:S(2)}) async-start(bf16[16,32,264]{2,1,0:T(8,128)(2,1)} %pack.1), calls=%async_computation | async-start | bytes 786432 | tf_op jit(solution)/shard_map/all_to_all | solution.py:30
  16.0 9.1 %collective-permute-start.1 = (bf16[2,64,256]{2,1,0:T(8,128)(2,1)S(1)}, bf16[2,64,256]{2,1,0:T(8,128)(2,1)S(1)}, u32[]{:S(2)}, u32[]{:S(2)}) collective-permute-start(bf16[2,64,256]{2,1,0:T(8,128)(2,1)S(1)} %get-tuple-element.130), channel_id=1, source_target_pairs={{0,128},{64,192},{128,0},{192,64},{1,129},{65,193},{129,1},{193,65... | collective-permute-start | bytes 196616 | tf_op jit(solution)/shard_map/ppermute | solution.py:38
  25.1 5.7 %collective-permute-done.1 = bf16[2,64,256]{2,1,0:T(8,128)(2,1)S(1)} collective-permute-done((bf16[2,64,256]{2,1,0:T(8,128)(2,1)S(1)}, bf16[2,64,256]{2,1,0:T(8,128)(2,1)S(1)}, u32[]{:S(2)}, u32[]{:S(2)}) %collective-permute-start.1) | collective-permute-done | bytes 65568 | tf_op jit(solution)/shard_map/ppermute | solution.py:38
  32.6 45.0 %all_to_all.30 = bf16[8,288,128]{2,1,0:T(8,128)(2,1)S(1)} all-to-all(bf16[8,288,128]{2,1,0:T(8,128)(2,1)S(1)} %bitcast.62), channel_id=1, replica_groups=mesh['gr'=2,'zq'=4,'b'=2,'y'=4,'x'=4,'core'=2] {'gr','zq'}, dimensions={0} | all-to-all | bytes 1179648 | tf_op jit(solution)/shard_map/all_to_all | solution.py:30
  77.6 2.4 collective-permute-start.3
  80.0 8.1 %collective-permute-done.3 = bf16[8,144,128]{2,1,0:T(8,128)(2,1)S(1)} collective-permute-done((bf16[8,144,128]{2,1,0:T(8,128)(2,1)S(1)}, bf16[8,144,128]{2,1,0:T(8,128)(2,1)S(1)}, u32[]{:S(2)}, u32[]{:S(2)}) %collective-permute-start.3) | collective-permute-done | bytes 294944 | tf_op jit(solution)/shard_map/ppermute | solution.py:38
  88.3 1.9 collective-permute-start.7
  90.3 4.8 %collective-permute-start.6 = (bf16[16,144,128]{2,1,0:T(8,128)(2,1)S(1)}, bf16[16,144,128]{2,1,0:T(8,128)(2,1)S(1)}, u32[]{:S(2)}, u32[]{:S(2)}) collective-permute-start(bf16[16,144,128]{2,1,0:T(8,128)(2,1)S(1)} %bitcast.56), channel_id=1, source_target_pairs={{0,4},{2,6},{4,0},{6,2},{1,5},{3,7},{5,1},{7,3},{8,12},{10,14},{12... | collective-permute-start | bytes 1769480 | tf_op jit(solution)/shard_map/ppermute | solution.py:38
  95.1 3.1 %collective-permute-start.5 = (bf16[16,144,128]{2,1,0:T(8,128)(2,1)S(1)}, bf16[16,144,128]{2,1,0:T(8,128)(2,1)}, u32[]{:S(2)}, u32[]{:S(2)}) collective-permute-start(bf16[16,144,128]{2,1,0:T(8,128)(2,1)S(1)} %bitcast.57), channel_id=1, source_target_pairs={{0,2},{2,0},{4,6},{6,4},{1,3},{3,1},{5,7},{7,5},{8,10},{10,8},{12,... | collective-permute-start | bytes 1769480 | tf_op jit(solution)/shard_map/ppermute | solution.py:38
  98.2 3.9 %collective-permute-start.2 = (bf16[2,2,64,256]{3,2,1,0:T(8,128)(2,1)S(1)}, bf16[2,2,64,256]{3,2,1,0:T(8,128)(2,1)S(1)}, u32[]{:S(2)}, u32[]{:S(2)}) collective-permute-start(bf16[2,2,64,256]{3,2,1,0:T(8,128)(2,1)S(1)} %pad_maximum_fusion.4), channel_id=1, source_target_pairs={{0,64},{64,0},{128,192},{192,128},{1,65},{65,1},{129,193},{193,129... | collective-permute-start | bytes 393224 | tf_op jit(solution)/shard_map/ppermute | solution.py:38
  102.1 5.0 %collective-permute-done.2 = bf16[2,2,64,256]{3,2,1,0:T(8,128)(2,1)S(1)} collective-permute-done((bf16[2,2,64,256]{3,2,1,0:T(8,128)(2,1)S(1)}, bf16[2,2,64,256]{3,2,1,0:T(8,128)(2,1)S(1)}, u32[]{:S(2)}, u32[]{:S(2)}) %collective-permute-start.2) | collective-permute-done | bytes 131104 | tf_op jit(solution)/shard_map/ppermute | solution.py:38
  108.2 4.2 %all-to-all-start.2 = ((bf16[4,4,2,64,256]{4,3,2,1,0:T(8,128)(2,1)}), bf16[4,4,2,64,256]{4,3,2,1,0:T(8,128)(2,1)S(1)}, u32[]{:S(2)}, u32[]{:S(2)}) async-start(bf16[4,4,2,64,256]{4,3,2,1,0:T(8,128)(2,1)} %broadcast_in_dim.13), calls=%async_computation.2 | async-start | bytes 2097152 | tf_op jit(solution)/shard_map/all_to_all | solution.py:30
  114.4 1.9 collective-permute-start.8
  120.1 2.4 collective-permute-start.10
  122.5 1.9 collective-permute-start.9
  124.7 2.1 collective-permute-done.9.refs_5_
  126.8 6.6 %half_step.2 = bf16[4,4,2,64,256]{4,3,2,1,0:T(8,128)(2,1)} custom-call(s32[1]{0:T(128)} %bitcast.at_ref, bf16[4,4,2,64,256]{4,3,2,1,0:T(8,128)(2,1)S(1)} %all-to-all-done.2.x_ref, bf16[16,144,128]{2,1,0:T(8,128)(2,1)S(1)} %bitcast.59, bf16[16,144,128]{2,1,0:T(8,128)(2,1)} %collective-permute-done.5.refs_1_, ...), custom_call_target="tpu_custom_call" | custom-call | flops 1207959552 | bytes 6815744 | tf_op jit(solution)/shard_map/half_step/pallas_call | solution.py:171
  133.4 4.2 %all-to-all-start.3 = ((bf16[4,4,2,64,256]{4,3,2,1,0:T(8,128)(2,1)}), bf16[4,4,2,64,256]{4,3,2,1,0:T(8,128)(2,1)}, u32[]{:S(2)}, u32[]{:S(2)}) async-start(bf16[4,4,2,64,256]{4,3,2,1,0:T(8,128)(2,1)} %half_step.2), calls=%async_computation.3 | async-start | bytes 2097152 | tf_op jit(solution)/shard_map/all_to_all | solution.py:30
  137.7 2.4 collective-permute-start.16
  140.1 3.1 %collective-permute-start.15 = (bf16[16,144,128]{2,1,0:T(8,128)(2,1)S(1)}, bf16[16,144,128]{2,1,0:T(8,128)(2,1)S(1)}, u32[]{:S(2)}, u32[]{:S(2)}) collective-permute-start(bf16[16,144,128]{2,1,0:T(8,128)(2,1)S(1)} %bitcast.50), channel_id=1, source_target_pairs={{0,4},{2,6},{4,0},{6,2},{1,5},{3,7},{5,1},{7,3},{8,12},{10,14},{12... | collective-permute-start | bytes 1769480 | tf_op jit(solution)/shard_map/ppermute | solution.py:38
  143.2 4.3 %collective-permute-start.14 = (bf16[16,144,128]{2,1,0:T(8,128)(2,1)S(1)}, bf16[16,144,128]{2,1,0:T(8,128)(2,1)}, u32[]{:S(2)}, u32[]{:S(2)}) collective-permute-start(bf16[16,144,128]{2,1,0:T(8,128)(2,1)S(1)} %bitcast.51), channel_id=1, source_target_pairs={{0,2},{2,0},{4,6},{6,4},{1,3},{3,1},{5,7},{7,5},{8,10},{10,8},{12,... | collective-permute-start | bytes 1769480 | tf_op jit(solution)/shard_map/ppermute | solution.py:38
  147.5 5.9 %all-to-all-done.3 = bf16[4,4,2,64,256]{4,3,2,1,0:T(8,128)(2,1)} async-done(((bf16[4,4,2,64,256]{4,3,2,1,0:T(8,128)(2,1)}), bf16[4,4,2,64,256]{4,3,2,1,0:T(8,128)(2,1)}, u32[]{:S(2)}, u32[]{:S(2)}) %all-to-all-start.3) | async-done | bytes 1048608 | tf_op jit(solution)/shard_map/all_to_all | solution.py:30
  154.5 3.7 %collective-permute-start.12 = (bf16[2,2,64,256]{3,2,1,0:T(8,128)(2,1)S(1)}, bf16[2,2,64,256]{3,2,1,0:T(8,128)(2,1)S(1)}, u32[]{:S(2)}, u32[]{:S(2)}) collective-permute-start(bf16[2,2,64,256]{3,2,1,0:T(8,128)(2,1)S(1)} %slice_reduce_fusion), channel_id=1, source_target_pairs={{0,64},{64,0},{128,192},{192,128},{1,65},{65,1},{129,193},{193,129... | collective-permute-start | bytes 393224 | tf_op jit(solution)/shard_map/ppermute | solution.py:38
  159.3 5.4 %collective-permute-done.12 = bf16[2,2,64,256]{3,2,1,0:T(8,128)(2,1)S(1)} collective-permute-done((bf16[2,2,64,256]{3,2,1,0:T(8,128)(2,1)S(1)}, bf16[2,2,64,256]{3,2,1,0:T(8,128)(2,1)S(1)}, u32[]{:S(2)}, u32[]{:S(2)}) %collective-permute-start.12) | collective-permute-done | bytes 131104 | tf_op jit(solution)/shard_map/ppermute | solution.py:38
  164.8 3.1 %collective-permute-start.13 = (bf16[2,2,64,256]{3,2,1,0:T(8,128)(2,1)S(1)}, bf16[2,2,64,256]{3,2,1,0:T(8,128)(2,1)}, u32[]{:S(2)}, u32[]{:S(2)}) collective-permute-start(bf16[2,2,64,256]{3,2,1,0:T(8,128)(2,1)S(1)} %add_convert_fusion.2), channel_id=1, source_target_pairs={{0,128},{64,192},{128,0},{192,64},{1,129},{65,193},{129,1},{193,65... | collective-permute-start | bytes 393224 | tf_op jit(solution)/shard_map/ppermute | solution.py:38
  169.1 4.9 %serve.2 = (bf16[176,2048]{1,0:T(8,128)(2,1)}, bf16[176,2048]{1,0:T(8,128)(2,1)}, bf16[176,2048]{1,0:T(8,128)(2,1)}) custom-call(s32[3]{0:T(128)S(1)} %pad_add_fusion.at_ref, bf16[16,144,128]{2,1,0:T(8,128)(2,1)S(1)} %bitcast.60, bf16[16,144,128]{2,1,0:T(8,128)(2,1)} %collective-permute-done.5.refs_1_, bf16[16,144,128]{2,1,0:T(8,128)(2,1)S(1)} %copy-done.1, ...), custom_call_target="tpu_custom_call" | custom-call | flops 100000000 | bytes 6881280 | tf_op jit(solution)/shard_map/serve/pallas_call | solution.py:205
  174.0 8.0 %collective-permute-done.13 = bf16[2,2,64,256]{3,2,1,0:T(8,128)(2,1)} collective-permute-done((bf16[2,2,64,256]{3,2,1,0:T(8,128)(2,1)S(1)}, bf16[2,2,64,256]{3,2,1,0:T(8,128)(2,1)}, u32[]{:S(2)}, u32[]{:S(2)}) %collective-permute-start.13) | collective-permute-done | bytes 131104 | tf_op jit(solution)/shard_map/ppermute | solution.py:38
  182.9 1.9 collective-permute-start.17
  184.9 6.3 %collective-permute-done.17 = bf16[2,2,64,256]{3,2,1,0:T(8,128)(2,1)S(1)} collective-permute-done((bf16[2,2,64,256]{3,2,1,0:T(8,128)(2,1)S(1)}, bf16[2,2,64,256]{3,2,1,0:T(8,128)(2,1)S(1)}, u32[]{:S(2)}, u32[]{:S(2)}) %collective-permute-start.17) | collective-permute-done | bytes 131104 | tf_op jit(solution)/shard_map/ppermute | solution.py:38
  192.3 3.5 %all-to-all-start.4 = ((bf16[4,4,2,64,256]{4,3,2,1,0:T(8,128)(2,1)}), bf16[4,4,2,64,256]{4,3,2,1,0:T(8,128)(2,1)S(1)}, u32[]{:S(2)}, u32[]{:S(2)}) async-start(bf16[4,4,2,64,256]{4,3,2,1,0:T(8,128)(2,1)} %broadcast_in_dim.28), calls=%async_computation.4 | async-start | bytes 2097152 | tf_op jit(solution)/shard_map/all_to_all | solution.py:30
  195.8 1.9 collective-permute-start.18
  197.7 2.4 collective-permute-start.19
  200.2 1.9 collective-permute-start.20
  202.1 2.4 collective-permute-start.21
  204.5 1.9 collective-permute-start.22
  206.4 3.9 %collective-permute-done.22 = bf16[64,256]{1,0:T(8,128)(2,1)S(1)} collective-permute-done((bf16[64,256]{1,0:T(8,128)(2,1)S(1)}, bf16[64,256]{1,0:T(8,128)(2,1)S(1)}, u32[]{:S(2)}, u32[]{:S(2)}) %collective-permute-start.22) | collective-permute-done | bytes 32800 | tf_op jit(solution)/shard_map/ppermute | solution.py:38
  216.6 5.9 %half_step.3 = bf16[4,4,2,64,256]{4,3,2,1,0:T(8,128)(2,1)} custom-call(s32[1]{0:T(128)} %bitcast.at_ref, bf16[4,4,2,64,256]{4,3,2,1,0:T(8,128)(2,1)S(1)} %all-to-all-done.4.x_ref, bf16[16,144,128]{2,1,0:T(8,128)(2,1)S(1)} %bitcast.53, bf16[16,144,128]{2,1,0:T(8,128)(2,1)} %collective-permute-done.14.refs_1_, ...), custom_call_target="tpu_custom_call" | custom-call | flops 1207959552 | bytes 6815744 | tf_op jit(solution)/shard_map/half_step/pallas_call | solution.py:171
  222.5 4.9 %all-to-all-start.5 = ((bf16[4,4,2,64,256]{4,3,2,1,0:T(8,128)(2,1)}), bf16[4,4,2,64,256]{4,3,2,1,0:T(8,128)(2,1)}, u32[]{:S(2)}, u32[]{:S(2)}) async-start(bf16[4,4,2,64,256]{4,3,2,1,0:T(8,128)(2,1)} %half_step.3), calls=%async_computation.5 | async-start | bytes 2097152 | tf_op jit(solution)/shard_map/all_to_all | solution.py:30
  229.5 4.3 %serve.3 = (bf16[176,2048]{1,0:T(8,128)(2,1)}, bf16[176,2048]{1,0:T(8,128)(2,1)}, bf16[176,2048]{1,0:T(8,128)(2,1)}) custom-call(s32[3]{0:T(128)S(1)} %pad_add_fusion.at_ref, bf16[16,144,128]{2,1,0:T(8,128)(2,1)S(1)} %bitcast.54, bf16[16,144,128]{2,1,0:T(8,128)(2,1)} %collective-permute-done.14.refs_1_, ...), custom_call_target="tpu_custom_call" | custom-call | flops 100000000 | bytes 6881280 | tf_op jit(solution)/shard_map/serve/pallas_call | solution.py:205
  233.9 7.8 %all-to-all-done.5 = bf16[4,4,2,64,256]{4,3,2,1,0:T(8,128)(2,1)} async-done(((bf16[4,4,2,64,256]{4,3,2,1,0:T(8,128)(2,1)}), bf16[4,4,2,64,256]{4,3,2,1,0:T(8,128)(2,1)}, u32[]{:S(2)}, u32[]{:S(2)}) %all-to-all-start.5) | async-done | bytes 1048608 | tf_op jit(solution)/shard_map/all_to_all | solution.py:30
  242.8 2.2 collective-permute-start.23
  246.2 5.5 %collective-permute-done.23 = bf16[2,2,64,256]{3,2,1,0:T(8,128)(2,1)S(1)} collective-permute-done((bf16[2,2,64,256]{3,2,1,0:T(8,128)(2,1)S(1)}, bf16[2,2,64,256]{3,2,1,0:T(8,128)(2,1)S(1)}, u32[]{:S(2)}, u32[]{:S(2)}) %collective-permute-start.23) | collective-permute-done | bytes 131104 | tf_op jit(solution)/shard_map/ppermute | solution.py:38
  251.7 4.2 %collective-permute-start.24 = (bf16[64,256]{1,0:T(8,128)(2,1)S(1)}, bf16[64,256]{1,0:T(8,128)(2,1)S(1)}, u32[]{:S(2)}, u32[]{:S(2)}) collective-permute-start(bf16[64,256]{1,0:T(8,128)(2,1)S(1)} %get-tuple-element.124), channel_id=1, source_target_pairs={{0,128},{32,160},{64,192},{96,224},{128,0},{160,32},{192,64},{224,... | collective-permute-start | bytes 98312 | tf_op jit(solution)/shard_map/ppermute | solution.py:38
  255.9 1.9 collective-permute-start.25
  257.8 7.0 %collective-permute-start.26 = (bf16[64,256]{1,0:T(8,128)(2,1)S(1)}, bf16[64,256]{1,0:T(8,128)(2,1)S(1)}, u32[]{:S(2)}, u32[]{:S(2)}) collective-permute-start(bf16[64,256]{1,0:T(8,128)(2,1)S(1)} %get-tuple-element.126), channel_id=1, source_target_pairs={{0,160},{32,128},{64,224},{96,192},{128,32},{160,0},{192,96},{224,... | collective-permute-start | bytes 98312 | tf_op jit(solution)/shard_map/ppermute | solution.py:38
  264.9 3.5 %collective-permute-done.26 = bf16[64,256]{1,0:T(8,128)(2,1)S(1)} collective-permute-done((bf16[64,256]{1,0:T(8,128)(2,1)S(1)}, bf16[64,256]{1,0:T(8,128)(2,1)S(1)}, u32[]{:S(2)}, u32[]{:S(2)}) %collective-permute-start.26) | collective-permute-done | bytes 32800 | tf_op jit(solution)/shard_map/ppermute | solution.py:38
  (87 shorter events, 26.7 us)
Async XLA Ops:
  0.6 15.4 %copy-start.13 = (bf16[512,64]{0,1:T(8,128)(2,1)S(1)}, bf16[512,64]{0,1:T(8,128)(2,1)}, u32[]{:S(2)}) copy-start(bf16[512,64]{0,1:T(8,128)(2,1)} %param.9) | copy-start | bytes 196612
  1.5 14.5 %collective-permute-start = (bf16[64,256]{1,0:T(8,128)(2,1)S(1)}, bf16[64,256]{1,0:T(8,128)(2,1)S(1)}, u32[]{:S(2)}, u32[]{:S(2)}) collective-permute-start(bf16[64,256]{1,0:T(8,128)(2,1)S(1)} %broadcast_select_fusion.2), channel_id=1, source_target_pairs={{0,32},{32,0},{1,33},{33,1},{2,34},{34,2},{3,35},{35,3},{4,36},{36... | collective-permute-start | bytes 98312 | tf_op jit(solution)/shard_map/ppermute | solution.py:38
  8.5 22.4 %all-to-all-start = ((bf16[16,32,264]{2,1,0:T(8,128)(2,1)}), bf16[16,32,264]{2,1,0:T(8,128)(2,1)S(1)}, u32[]{:S(2)}, u32[]{:S(2)}) async-start(bf16[16,32,264]{2,1,0:T(8,128)(2,1)} %pack.1), calls=%async_computation | async-start | bytes 786432 | tf_op jit(solution)/shard_map/all_to_all | solution.py:30
  16.0 14.8 %collective-permute-start.1 = (bf16[2,64,256]{2,1,0:T(8,128)(2,1)S(1)}, bf16[2,64,256]{2,1,0:T(8,128)(2,1)S(1)}, u32[]{:S(2)}, u32[]{:S(2)}) collective-permute-start(bf16[2,64,256]{2,1,0:T(8,128)(2,1)S(1)} %get-tuple-element.130), channel_id=1, source_target_pairs={{0,128},{64,192},{128,0},{192,64},{1,129},{65,193},{129,1},{193,65... | collective-permute-start | bytes 196616 | tf_op jit(solution)/shard_map/ppermute | solution.py:38
  30.9 76.2 %copy-start.11 = (bf16[2,2,64,256]{3,2,1,0:T(8,128)(2,1)}, bf16[2,2,64,256]{3,2,1,0:T(8,128)(2,1)S(1)}, u32[]{:S(2)}) copy-start(bf16[2,2,64,256]{3,2,1,0:T(8,128)(2,1)S(1)} %pad_maximum_fusion.4) | copy-start | bytes 393220
  77.6 10.5 %collective-permute-start.3 = (bf16[8,144,128]{2,1,0:T(8,128)(2,1)S(1)}, bf16[8,144,128]{2,1,0:T(8,128)(2,1)S(1)}, u32[]{:S(2)}, u32[]{:S(2)}) collective-permute-start(bf16[8,144,128]{2,1,0:T(8,128)(2,1)S(1)} %slice.70), channel_id=1, source_target_pairs={{0,32},{32,0},{1,33},{33,1},{2,34},{34,2},{3,35},{35,3},{4,36},{36... | collective-permute-start | bytes 884744 | tf_op jit(solution)/shard_map/ppermute | solution.py:38
  88.3 29.8 %collective-permute-start.7 = (bf16[16,144,128]{2,1,0:T(8,128)(2,1)S(1)}, bf16[16,144,128]{2,1,0:T(8,128)(2,1)S(1)}, u32[]{:S(2)}, u32[]{:S(2)}) collective-permute-start(bf16[16,144,128]{2,1,0:T(8,128)(2,1)S(1)} %bitcast.55), channel_id=1, source_target_pairs={{0,6},{2,4},{4,2},{6,0},{1,7},{3,5},{5,3},{7,1},{8,14},{10,12},{12... | collective-permute-start | bytes 1769480 | tf_op jit(solution)/shard_map/ppermute | solution.py:38
  90.3 29.8 %collective-permute-start.6 = (bf16[16,144,128]{2,1,0:T(8,128)(2,1)S(1)}, bf16[16,144,128]{2,1,0:T(8,128)(2,1)S(1)}, u32[]{:S(2)}, u32[]{:S(2)}) collective-permute-start(bf16[16,144,128]{2,1,0:T(8,128)(2,1)S(1)} %bitcast.56), channel_id=1, source_target_pairs={{0,4},{2,6},{4,0},{6,2},{1,5},{3,7},{5,1},{7,3},{8,12},{10,14},{12... | collective-permute-start | bytes 1769480 | tf_op jit(solution)/shard_map/ppermute | solution.py:38
  95.1 27.4 %collective-permute-start.5 = (bf16[16,144,128]{2,1,0:T(8,128)(2,1)S(1)}, bf16[16,144,128]{2,1,0:T(8,128)(2,1)}, u32[]{:S(2)}, u32[]{:S(2)}) collective-permute-start(bf16[16,144,128]{2,1,0:T(8,128)(2,1)S(1)} %bitcast.57), channel_id=1, source_target_pairs={{0,2},{2,0},{4,6},{6,4},{1,3},{3,1},{5,7},{7,5},{8,10},{10,8},{12,... | collective-permute-start | bytes 1769480 | tf_op jit(solution)/shard_map/ppermute | solution.py:38
  98.2 8.9 %collective-permute-start.2 = (bf16[2,2,64,256]{3,2,1,0:T(8,128)(2,1)S(1)}, bf16[2,2,64,256]{3,2,1,0:T(8,128)(2,1)S(1)}, u32[]{:S(2)}, u32[]{:S(2)}) collective-permute-start(bf16[2,2,64,256]{3,2,1,0:T(8,128)(2,1)S(1)} %pad_maximum_fusion.4), channel_id=1, source_target_pairs={{0,64},{64,0},{128,192},{192,128},{1,65},{65,1},{129,193},{193,129... | collective-permute-start | bytes 393224 | tf_op jit(solution)/shard_map/ppermute | solution.py:38
  108.2 16.5 %all-to-all-start.2 = ((bf16[4,4,2,64,256]{4,3,2,1,0:T(8,128)(2,1)}), bf16[4,4,2,64,256]{4,3,2,1,0:T(8,128)(2,1)S(1)}, u32[]{:S(2)}, u32[]{:S(2)}) async-start(bf16[4,4,2,64,256]{4,3,2,1,0:T(8,128)(2,1)} %broadcast_in_dim.13), calls=%async_computation.2 | async-start | bytes 2097152 | tf_op jit(solution)/shard_map/all_to_all | solution.py:30
  112.5 12.0 %collective-permute-start.4 = (bf16[8,144,128]{2,1,0:T(8,128)(2,1)S(1)}, bf16[8,144,128]{2,1,0:T(8,128)(2,1)S(1)}, u32[]{:S(2)}, u32[]{:S(2)}) collective-permute-start(bf16[8,144,128]{2,1,0:T(8,128)(2,1)S(1)} %get-tuple-element.64), channel_id=1, source_target_pairs={{0,32},{32,0},{1,33},{33,1},{2,34},{34,2},{3,35},{35,3},{4,36},{36... | collective-permute-start | bytes 884744 | tf_op jit(solution)/shard_map/ppermute | solution.py:38
  114.4 10.2 %collective-permute-start.8 = (bf16[16,144,128]{2,1,0:T(8,128)(2,1)S(1)}, bf16[16,144,128]{2,1,0:T(8,128)(2,1)}, u32[]{:S(2)}, u32[]{:S(2)}) collective-permute-start(bf16[16,144,128]{2,1,0:T(8,128)(2,1)S(1)} %bitcast.58), channel_id=1, source_target_pairs={{0,1},{1,0},{2,3},{3,2},{4,5},{5,4},{6,7},{7,6},{8,9},{9,8},{10,11... | collective-permute-start | bytes 1769480 | tf_op jit(solution)/shard_map/ppermute | solution.py:38
  118.2 6.5 %collective-permute-start.11 = (bf16[16,144,128]{2,1,0:T(8,128)(2,1)S(1)}, bf16[16,144,128]{2,1,0:T(8,128)(2,1)}, u32[]{:S(2)}, u32[]{:S(2)}) collective-permute-start(bf16[16,144,128]{2,1,0:T(8,128)(2,1)S(1)} %collective-permute-done.7.refs_3_), channel_id=1, source_target_pairs={{0,1},{1,0},{2,3},{3,2},{4,5},{5,4},{6,7},{7,6},{8,9},{9,8},{10,11... | collective-permute-start | bytes 1769480 | tf_op jit(solution)/shard_map/ppermute | solution.py:38
  120.1 6.7 %copy-start = (bf16[16,144,128]{2,1,0:T(8,128)(2,1)}, bf16[16,144,128]{2,1,0:T(8,128)(2,1)S(1)}, u32[]{:S(2)}) copy-start(bf16[16,144,128]{2,1,0:T(8,128)(2,1)S(1)} %collective-permute-done.6.refs_2_) | copy-start | bytes 1769476
  120.1 4.6 %collective-permute-start.10 = (bf16[16,144,128]{2,1,0:T(8,128)(2,1)S(1)}, bf16[16,144,128]{2,1,0:T(8,128)(2,1)}, u32[]{:S(2)}, u32[]{:S(2)}) collective-permute-start(bf16[16,144,128]{2,1,0:T(8,128)(2,1)S(1)} %collective-permute-done.6.refs_2_), channel_id=1, source_target_pairs={{0,1},{1,0},{2,3},{3,2},{4,5},{5,4},{6,7},{7,6},{8,9},{9,8},{10,11... | collective-permute-start | bytes 1769480 | tf_op jit(solution)/shard_map/ppermute | solution.py:38
  122.5 4.2 %collective-permute-start.9 = (bf16[16,144,128]{2,1,0:T(8,128)(2,1)}, bf16[16,144,128]{2,1,0:T(8,128)(2,1)}, u32[]{:S(2)}, u32[]{:S(2)}) collective-permute-start(bf16[16,144,128]{2,1,0:T(8,128)(2,1)} %collective-permute-done.5.refs_1_), channel_id=1, source_target_pairs={{0,1},{1,0},{2,3},{3,2},{4,5},{5,4},{6,7},{7,6},{8,9},{9,8},{10,11... | collective-permute-start | bytes 1769480 | tf_op jit(solution)/shard_map/ppermute | solution.py:38
  133.4 20.0 %all-to-all-start.3 = ((bf16[4,4,2,64,256]{4,3,2,1,0:T(8,128)(2,1)}), bf16[4,4,2,64,256]{4,3,2,1,0:T(8,128)(2,1)}, u32[]{:S(2)}, u32[]{:S(2)}) async-start(bf16[4,4,2,64,256]{4,3,2,1,0:T(8,128)(2,1)} %half_step.2), calls=%async_computation.3 | async-start | bytes 2097152 | tf_op jit(solution)/shard_map/all_to_all | solution.py:30
  137.7 45.2 %collective-permute-start.16 = (bf16[16,144,128]{2,1,0:T(8,128)(2,1)S(1)}, bf16[16,144,128]{2,1,0:T(8,128)(2,1)S(1)}, u32[]{:S(2)}, u32[]{:S(2)}) collective-permute-start(bf16[16,144,128]{2,1,0:T(8,128)(2,1)S(1)} %bitcast.49), channel_id=1, source_target_pairs={{0,6},{2,4},{4,2},{6,0},{1,7},{3,5},{5,3},{7,1},{8,14},{10,12},{12... | collective-permute-start | bytes 1769480 | tf_op jit(solution)/shard_map/ppermute | solution.py:38
  140.1 42.7 %collective-permute-start.15 = (bf16[16,144,128]{2,1,0:T(8,128)(2,1)S(1)}, bf16[16,144,128]{2,1,0:T(8,128)(2,1)S(1)}, u32[]{:S(2)}, u32[]{:S(2)}) collective-permute-start(bf16[16,144,128]{2,1,0:T(8,128)(2,1)S(1)} %bitcast.50), channel_id=1, source_target_pairs={{0,4},{2,6},{4,0},{6,2},{1,5},{3,7},{5,1},{7,3},{8,12},{10,14},{12... | collective-permute-start | bytes 1769480 | tf_op jit(solution)/shard_map/ppermute | solution.py:38
  143.2 39.6 %collective-permute-start.14 = (bf16[16,144,128]{2,1,0:T(8,128)(2,1)S(1)}, bf16[16,144,128]{2,1,0:T(8,128)(2,1)}, u32[]{:S(2)}, u32[]{:S(2)}) collective-permute-start(bf16[16,144,128]{2,1,0:T(8,128)(2,1)S(1)} %bitcast.51), channel_id=1, source_target_pairs={{0,2},{2,0},{4,6},{6,4},{1,3},{3,1},{5,7},{7,5},{8,10},{10,8},{12,... | collective-permute-start | bytes 1769480 | tf_op jit(solution)/shard_map/ppermute | solution.py:38
  154.5 10.2 %collective-permute-start.12 = (bf16[2,2,64,256]{3,2,1,0:T(8,128)(2,1)S(1)}, bf16[2,2,64,256]{3,2,1,0:T(8,128)(2,1)S(1)}, u32[]{:S(2)}, u32[]{:S(2)}) collective-permute-start(bf16[2,2,64,256]{3,2,1,0:T(8,128)(2,1)S(1)} %slice_reduce_fusion), channel_id=1, source_target_pairs={{0,64},{64,0},{128,192},{192,128},{1,65},{65,1},{129,193},{193,129... | collective-permute-start | bytes 393224 | tf_op jit(solution)/shard_map/ppermute | solution.py:38
  164.8 17.1 %collective-permute-start.13 = (bf16[2,2,64,256]{3,2,1,0:T(8,128)(2,1)S(1)}, bf16[2,2,64,256]{3,2,1,0:T(8,128)(2,1)}, u32[]{:S(2)}, u32[]{:S(2)}) collective-permute-start(bf16[2,2,64,256]{3,2,1,0:T(8,128)(2,1)S(1)} %add_convert_fusion.2), channel_id=1, source_target_pairs={{0,128},{64,192},{128,0},{192,64},{1,129},{65,193},{129,1},{193,65... | collective-permute-start | bytes 393224 | tf_op jit(solution)/shard_map/ppermute | solution.py:38
  168.0 1.1 copy-start.1
  169.1 13.8 %copy-start.12 = (bf16[2,2,64,256]{3,2,1,0:T(8,128)(2,1)S(1)}, bf16[2,2,64,256]{3,2,1,0:T(8,128)(2,1)}, u32[]{:S(2)}) copy-start(bf16[2,2,64,256]{3,2,1,0:T(8,128)(2,1)} %copy-done.11) | copy-start | bytes 393220
  182.9 8.2 %collective-permute-start.17 = (bf16[2,2,64,256]{3,2,1,0:T(8,128)(2,1)S(1)}, bf16[2,2,64,256]{3,2,1,0:T(8,128)(2,1)S(1)}, u32[]{:S(2)}, u32[]{:S(2)}) collective-permute-start(bf16[2,2,64,256]{3,2,1,0:T(8,128)(2,1)S(1)} %add_convert_fusion.1), channel_id=1, source_target_pairs={{0,64},{64,0},{128,192},{192,128},{1,65},{65,1},{129,193},{193,129... | collective-permute-start | bytes 393224 | tf_op jit(solution)/shard_map/ppermute | solution.py:38
  192.3 21.1 %all-to-all-start.4 = ((bf16[4,4,2,64,256]{4,3,2,1,0:T(8,128)(2,1)}), bf16[4,4,2,64,256]{4,3,2,1,0:T(8,128)(2,1)S(1)}, u32[]{:S(2)}, u32[]{:S(2)}) async-start(bf16[4,4,2,64,256]{4,3,2,1,0:T(8,128)(2,1)} %broadcast_in_dim.28), calls=%async_computation.4 | async-start | bytes 2097152 | tf_op jit(solution)/shard_map/all_to_all | solution.py:30
  195.8 15.1 %collective-permute-start.18 = (bf16[16,144,128]{2,1,0:T(8,128)(2,1)S(1)}, bf16[16,144,128]{2,1,0:T(8,128)(2,1)S(1)}, u32[]{:S(2)}, u32[]{:S(2)}) collective-permute-start(bf16[16,144,128]{2,1,0:T(8,128)(2,1)S(1)} %bitcast.52), channel_id=1, source_target_pairs={{0,1},{1,0},{2,3},{3,2},{4,5},{5,4},{6,7},{7,6},{8,9},{9,8},{10,11... | collective-permute-start | bytes 1769480 | tf_op jit(solution)/shard_map/ppermute | solution.py:38
  197.7 13.2 %collective-permute-start.19 = (bf16[16,144,128]{2,1,0:T(8,128)(2,1)}, bf16[16,144,128]{2,1,0:T(8,128)(2,1)S(1)}, u32[]{:S(2)}, u32[]{:S(2)}) collective-permute-start(bf16[16,144,128]{2,1,0:T(8,128)(2,1)} %collective-permute-done.14.refs_1_), channel_id=1, source_target_pairs={{0,1},{1,0},{2,3},{3,2},{4,5},{5,4},{6,7},{7,6},{8,9},{9,8},{10,11... | collective-permute-start | bytes 1769480 | tf_op jit(solution)/shard_map/ppermute | solution.py:38
  200.2 11.6 %collective-permute-start.20 = (bf16[16,144,128]{2,1,0:T(8,128)(2,1)S(1)}, bf16[16,144,128]{2,1,0:T(8,128)(2,1)S(1)}, u32[]{:S(2)}, u32[]{:S(2)}) collective-permute-start(bf16[16,144,128]{2,1,0:T(8,128)(2,1)S(1)} %collective-permute-done.15.refs_2_), channel_id=1, source_target_pairs={{0,1},{1,0},{2,3},{3,2},{4,5},{5,4},{6,7},{7,6},{8,9},{9,8},{10,11... | collective-permute-start | bytes 1769480 | tf_op jit(solution)/shard_map/ppermute | solution.py:38
  202.1 10.5 %collective-permute-start.21 = (bf16[16,144,128]{2,1,0:T(8,128)(2,1)S(1)}, bf16[16,144,128]{2,1,0:T(8,128)(2,1)S(1)}, u32[]{:S(2)}, u32[]{:S(2)}) collective-permute-start(bf16[16,144,128]{2,1,0:T(8,128)(2,1)S(1)} %collective-permute-done.16.refs_3_), channel_id=1, source_target_pairs={{0,1},{1,0},{2,3},{3,2},{4,5},{5,4},{6,7},{7,6},{8,9},{9,8},{10,11... | collective-permute-start | bytes 1769480 | tf_op jit(solution)/shard_map/ppermute | solution.py:38
  204.5 5.8 %collective-permute-start.22 = (bf16[64,256]{1,0:T(8,128)(2,1)S(1)}, bf16[64,256]{1,0:T(8,128)(2,1)S(1)}, u32[]{:S(2)}, u32[]{:S(2)}) collective-permute-start(bf16[64,256]{1,0:T(8,128)(2,1)S(1)} %select_bitcast_fusion.7), channel_id=1, source_target_pairs={{0,32},{32,0},{1,33},{33,1},{2,34},{34,2},{3,35},{35,3},{4,36},{36... | collective-permute-start | bytes 98312 | tf_op jit(solution)/shard_map/ppermute | solution.py:38
  211.0 0.8 copy-start.2
  211.8 0.8 copy-start.5
  212.6 0.8 copy-start.8
  213.4 1.1 copy-start.3
  214.5 1.1 copy-start.6
  215.5 1.1 copy-start.9
  222.5 4.9 %copy-start.4 = (bf16[16,144,128]{2,1,0:T(8,128)(2,1)S(1)}, bf16[16,144,128]{2,1,0:T(8,128)(2,1)}, u32[]{:S(2)}) copy-start(bf16[16,144,128]{2,1,0:T(8,128)(2,1)} %copy-done.2) | copy-start | bytes 1769476
  222.5 19.1 %all-to-all-start.5 = ((bf16[4,4,2,64,256]{4,3,2,1,0:T(8,128)(2,1)}), bf16[4,4,2,64,256]{4,3,2,1,0:T(8,128)(2,1)}, u32[]{:S(2)}, u32[]{:S(2)}) async-start(bf16[4,4,2,64,256]{4,3,2,1,0:T(8,128)(2,1)} %half_step.3), calls=%async_computation.5 | async-start | bytes 2097152 | tf_op jit(solution)/shard_map/all_to_all | solution.py:30
  227.4 1.1 copy-start.7
  228.5 1.1 copy-start.10
  241.7 26.8 %copy-start.14 = (bf16[64,256]{1,0:T(8,128)(2,1)S(1)}, bf16[64,256]{1,0:T(8,128)(2,1)}, u32[]{:S(2)}) copy-start(bf16[64,256]{1,0:T(8,128)(2,1)} %get-tuple-element.108) | copy-start | bytes 98308
  241.7 26.8 %copy-start.15 = (bf16[64,256]{1,0:T(8,128)(2,1)S(1)}, bf16[64,256]{1,0:T(8,128)(2,1)}, u32[]{:S(2)}) copy-start(bf16[64,256]{1,0:T(8,128)(2,1)} %get-tuple-element.94) | copy-start | bytes 98308
  242.8 8.9 %collective-permute-start.23 = (bf16[2,2,64,256]{3,2,1,0:T(8,128)(2,1)S(1)}, bf16[2,2,64,256]{3,2,1,0:T(8,128)(2,1)S(1)}, u32[]{:S(2)}, u32[]{:S(2)}) collective-permute-start(bf16[2,2,64,256]{3,2,1,0:T(8,128)(2,1)S(1)} %slice_reduce_fusion.1), channel_id=1, source_target_pairs={{0,64},{64,0},{128,192},{192,128},{1,65},{65,1},{129,193},{193,129... | collective-permute-start | bytes 393224 | tf_op jit(solution)/shard_map/ppermute | solution.py:38
  251.7 13.1 %collective-permute-start.24 = (bf16[64,256]{1,0:T(8,128)(2,1)S(1)}, bf16[64,256]{1,0:T(8,128)(2,1)S(1)}, u32[]{:S(2)}, u32[]{:S(2)}) collective-permute-start(bf16[64,256]{1,0:T(8,128)(2,1)S(1)} %get-tuple-element.124), channel_id=1, source_target_pairs={{0,128},{32,160},{64,192},{96,224},{128,0},{160,32},{192,64},{224,... | collective-permute-start | bytes 98312 | tf_op jit(solution)/shard_map/ppermute | solution.py:38
  255.9 9.0 %collective-permute-start.25 = (bf16[64,256]{1,0:T(8,128)(2,1)S(1)}, bf16[64,256]{1,0:T(8,128)(2,1)S(1)}, u32[]{:S(2)}, u32[]{:S(2)}) collective-permute-start(bf16[64,256]{1,0:T(8,128)(2,1)S(1)} %get-tuple-element.125), channel_id=1, source_target_pairs={{0,32},{32,0},{64,96},{96,64},{128,160},{160,128},{192,224},{224,1... | collective-permute-start | bytes 98312 | tf_op jit(solution)/shard_map/ppermute | solution.py:38
  257.8 10.6 %collective-permute-start.26 = (bf16[64,256]{1,0:T(8,128)(2,1)S(1)}, bf16[64,256]{1,0:T(8,128)(2,1)S(1)}, u32[]{:S(2)}, u32[]{:S(2)}) collective-permute-start(bf16[64,256]{1,0:T(8,128)(2,1)S(1)} %get-tuple-element.126), channel_id=1, source_target_pairs={{0,160},{32,128},{64,224},{96,192},{128,32},{160,0},{192,96},{224,... | collective-permute-start | bytes 98312 | tf_op jit(solution)/shard_map/ppermute | solution.py:38
